TPU v7x, 256 devices: a whole 4x4x8 slice. The times are simulated.
256 devices in a mesh: ep: 64 (over z, y, core), tp: 4 (over x).
Axes of the slice: x: 4, y: 4, z: 8, core: 2. Of those that a mesh axis runs over, the one named last changes fastest.
Arguments:
- tokens: bfloat16 [1536, 1024], P('ep'), may hold values from -1.796875 to 1.796875
- attn_gain: float32 [1024], replicated, may hold values from 0.1 to 1.9
- w_query: bfloat16 [1024, 1024], P(None, 'tp'), may hold values from -0.1875 to 0.1875
- w_key: bfloat16 [1024, 256], P(None, 'tp'), may hold values from -0.1875 to 0.1875
- w_value: bfloat16 [1024, 256], P(None, 'tp'), may hold values from -0.1875 to 0.1875
- w_forget: bfloat16 [1024, 4], P(None, 'tp'), may hold values from -0.1875 to 0.1875
- forget_bias: float32 [4], P('tp'), may hold values from -1 to 2
- query_gain: float32 [64], replicated, may hold values from 0.1 to 1.9
- key_gain: float32 [64], replicated, may hold values from 0.1 to 1.9
- cache_pairs: bfloat16 [1536, 4, 1024, 128], P('ep', 'tp'), may hold values from -6 to 206
- cache_cum: float32 [1536, 4, 1024], P('ep', 'tp'), may hold values from -1024 to 0, as said below
- lengths: int32 [1536], P('ep'), may hold values from 64 to 1024, as said below
- w_output: bfloat16 [1024, 1024], P('tp'), may hold values from -0.1875 to 0.1875
- ffn_gain: float32 [1024], replicated, may hold values from 0.1 to 1.9
- expert_ids: int32 [1536, 2], replicated, may hold values from 0 to 63, all different within a row; in each aligned block of 24 rows (0 to 23, 24 to 47, ...) at most 2 rows name the same one
- route_weight: float32 [1536, 2], replicated, may hold values from 0.2 to 1
- w_exp_gate: bfloat16 [64, 1024, 3584], P('ep', None, 'tp'), may hold values from -0.1875 to 0.1875
- w_exp_up: bfloat16 [64, 1024, 3584], P('ep', None, 'tp'), may hold values from -0.1875 to 0.1875
- w_exp_down: bfloat16 [64, 3584, 1024], P('ep', 'tp'), may hold values from -0.09375 to 0.09375
- shared_gate: bfloat16 [1024], replicated, may hold values from -0.1875 to 0.1875
- w_dense_gate: bfloat16 [4096, 1024], P('ep'), may hold values from -0.1875 to 0.1875
- w_dense_up: bfloat16 [4096, 1024], P('ep'), may hold values from -0.1875 to 0.1875
- w_dense_down: bfloat16 [4096, 1024], P('ep', 'tp'), may hold values from -0.09375 to 0.09375
Outputs:
- layer_out: bfloat16 [1536, 1024], P('ep', 'tp')
Inputs may be any that keep to these rules, and one draw needn't show every extreme that they name: The cache of sequence b holds positions 0 to lengths[b] - 1; some sequence has 1024. `expert_ids`: each row names 2 different experts; in each aligned block of 24 rows no expert is named by more than 2 rows. cache_cum[b, g, s] never rises with s.
All inputs are finite; a program needn't handle non-finite values.
Results may differ from a plain program's by a relative error of at most 0.02.
Values may be sent and summed in bfloat16 or wider, within the bound.
No kernel may reach another device: no remote copies, remote signals or barrier semaphores. Data moves between devices by JAX's collectives and lax.ppermute only.
A program may use at most 64 MiB of HBM per device.

v0:
```python
import jax
import jax.numpy as jnp
from jax import lax
from jax.sharding import Mesh
from jax.sharding import PartitionSpec as P

EP = ("ep_0", "ep_1", "ep_2")


EPSILON = 1e-06


def from_everyone(x, axis):
    count = lax.axis_size(axis)
    return lax.all_to_all(jnp.broadcast_to(x[None], (count, *x.shape)), axis, 0, 0, tiled=True)


def taken_together(x, axis):
    return from_everyone(x, axis).astype(jnp.float32).sum(axis=0)


def in_order(parts, dim):
    shape = list(parts.shape[1:])
    shape[dim] *= parts.shape[0]
    return jnp.moveaxis(parts, 0, dim).reshape(shape)


def whole_of(x, axes, dim):
    far, near = axes
    parts = from_everyone(from_everyone(x, far), near)
    return in_order(parts.swapaxes(0, 1).reshape(-1, *x.shape), dim)


def in_blocks(x, dim, count):
    shape = x.shape
    parts = x.reshape(*shape[:dim], count, shape[dim] // count, *shape[dim + 1 :])
    return jnp.moveaxis(parts, dim, 0)


def sent_and_summed(x, axis, dim):
    count = lax.axis_size(axis)
    parts = lax.all_to_all(in_blocks(x, dim, count), axis, 0, 0, tiled=True)
    return jnp.sum(parts.astype(jnp.float32), axis=0)


def sum_in_two_steps(x, axes, dim):
    far, near = axes
    parts = in_blocks(x, dim, lax.axis_size(far))
    nearer = sent_and_summed(parts, near, dim + 1)
    arrived = lax.all_to_all(
        nearer.astype(jnp.bfloat16), far, split_axis=0, concat_axis=0, tiled=True
    )
    return arrived.astype(jnp.float32).sum(axis=0)


def rms_scale(values, gain_row):
    mean_square = jnp.mean(values * values, axis=-1, keepdims=True)
    return values * lax.rsqrt(mean_square + EPSILON) * gain_row


def shards(
    tokens,
    attn_gain,
    w_query,
    w_key,
    w_value,
    w_forget,
    forget_bias,
    query_gain,
    key_gain,
    cache_pairs,
    cache_cum,
    lengths,
    w_output,
    ffn_gain,
    expert_ids,
    route_weight,
    w_exp_gate,
    w_exp_up,
    w_exp_down,
    shared_gate,
    w_dense_gate,
    w_dense_up,
    w_dense_down,
):
    seq_rows, width = tokens.shape
    head_size = query_gain.shape[0]
    kv_here = cache_pairs.shape[1]
    cache_len = cache_pairs.shape[2]
    tokens_f = tokens.astype(jnp.float32)
    normed = rms_scale(tokens_f, attn_gain).astype(jnp.bfloat16)
    query_raw = jnp.dot(normed, w_query, preferred_element_type=jnp.float32)
    heads_here = query_raw.shape[1] // head_size
    group_size = heads_here // kv_here
    query_rows = rms_scale(
        query_raw.reshape(seq_rows, kv_here, group_size, head_size), query_gain
    ).astype(jnp.bfloat16)
    key_raw = jnp.dot(normed, w_key, preferred_element_type=jnp.float32).reshape(
        seq_rows, kv_here, head_size
    )
    fresh_key = rms_scale(key_raw, key_gain).astype(jnp.bfloat16)
    value_new = jnp.dot(normed, w_value, preferred_element_type=jnp.float32).astype(jnp.bfloat16)
    value_new = value_new.reshape(seq_rows, kv_here, head_size)
    log_gate = jax.nn.log_sigmoid(
        jnp.dot(normed, w_forget, preferred_element_type=jnp.float32) + forget_bias
    )
    position = lax.broadcasted_iota(jnp.int32, (1, 1, cache_len), 2)
    is_live = position < lengths[:, None, None]
    last_cum = jnp.sum(jnp.where(position == lengths[:, None, None] - 1, cache_cum, 0.0), axis=2)
    now_cum = last_cum + log_gate
    cached_keys = cache_pairs[..., :head_size]
    cached_values = cache_pairs[..., head_size:]
    score_multiplier = head_size ** (-0.5)
    past_score = (
        jnp.einsum("bkgd,bkld->bkgl", query_rows, cached_keys, preferred_element_type=jnp.float32)
        * score_multiplier
    )
    past_score = past_score + (now_cum[:, :, None] - cache_cum)[:, :, None, :]
    past_score = jnp.where(is_live[:, :, None, :], past_score, -jnp.inf)
    current_score = (
        jnp.einsum("nlte,nle->nlt", query_rows, fresh_key, preferred_element_type=jnp.float32)
        * score_multiplier
    )
    row_peak = jnp.maximum(jnp.max(past_score, axis=3), current_score)
    past_exp = jnp.exp(past_score - row_peak[..., None])
    own_exp = jnp.exp(current_score - row_peak)
    denom_sum = jnp.sum(past_exp, axis=3) + own_exp
    past_prob = (past_exp / denom_sum[..., None]).astype(jnp.bfloat16)
    own_prob = (own_exp / denom_sum).astype(jnp.bfloat16)
    head_mix = jnp.einsum(
        "bkgl,bkld->bkgd", past_prob, cached_values, preferred_element_type=jnp.float32
    )
    head_mix = head_mix + own_prob[..., None].astype(jnp.float32) * value_new[:, :, None, :].astype(
        jnp.float32
    )
    head_mix = head_mix.astype(jnp.bfloat16).reshape(seq_rows, heads_here * head_size)
    partial_value = jnp.dot(head_mix, w_output, preferred_element_type=jnp.float32)
    attn_out = taken_together(partial_value.astype(jnp.bfloat16), "tp").astype(jnp.float32)
    residual = (tokens_f + attn_out).astype(jnp.bfloat16)
    residual_f = residual.astype(jnp.float32)
    normed_two = rms_scale(residual_f, ffn_gain).astype(jnp.bfloat16)
    all_rows = whole_of(normed_two, (("ep_0", "ep_1"), "ep_2"), 0)
    batch_rows = all_rows.shape[0]
    num_groups = lax.axis_size(EP)
    capacity = max(2, min(seq_rows, 128 // num_groups))
    chosen = expert_ids == lax.axis_index(EP)
    is_hit = jnp.sum(chosen.astype(jnp.int32), axis=1).reshape(num_groups, seq_rows)
    weight_here = jnp.sum(jnp.where(chosen, route_weight, 0.0), axis=1)
    slot_rank = jnp.cumsum(is_hit, axis=1)
    slot_ids = lax.broadcasted_iota(jnp.int32, (1, capacity, 1), 1) + 1
    picker = ((slot_rank[:, None, :] == slot_ids) & (is_hit[:, None, :] == 1)).astype(jnp.bfloat16)
    grouped = all_rows.reshape(num_groups, seq_rows, width)
    picked = jnp.einsum("scn,snd->scd", picker, grouped, preferred_element_type=jnp.float32)
    picked = picked.astype(jnp.bfloat16).reshape(num_groups * capacity, width)
    gate_part = jnp.dot(picked, w_exp_gate[0], preferred_element_type=jnp.float32)
    up_part = jnp.dot(picked, w_exp_up[0], preferred_element_type=jnp.float32)
    hidden = (jax.nn.silu(gate_part) * up_part).astype(jnp.bfloat16)
    expert_part = jnp.dot(hidden, w_exp_down[0], preferred_element_type=jnp.float32)
    expert_rows = sent_and_summed(expert_part.astype(jnp.bfloat16), "tp", 1).astype(jnp.bfloat16)
    feature_span = expert_rows.shape[1]
    placed = jnp.einsum(
        "scn,scd->snd",
        picker,
        expert_rows.reshape(num_groups, capacity, feature_span),
        preferred_element_type=jnp.float32,
    ).reshape(batch_rows, feature_span)
    expert_term = placed * weight_here[:, None]
    contract = (((1,), (1,)), ((), ()))
    dense_gate_raw = lax.dot_general(
        all_rows, w_dense_gate, contract, preferred_element_type=jnp.float32
    )
    dense_up_raw = lax.dot_general(
        all_rows, w_dense_up, contract, preferred_element_type=jnp.float32
    )
    dense_hidden = (jax.nn.silu(dense_gate_raw) * dense_up_raw).astype(jnp.bfloat16)
    mix_gate = jax.nn.sigmoid(jnp.dot(all_rows, shared_gate, preferred_element_type=jnp.float32))
    dense_rows = jnp.dot(dense_hidden, w_dense_down, preferred_element_type=jnp.float32)
    summed = sum_in_two_steps(
        (mix_gate[:, None] * dense_rows + expert_term).astype(jnp.bfloat16),
        (("ep_0", "ep_1"), "ep_2"),
        0,
    )
    column = lax.axis_index("tp") * feature_span
    own_residual = lax.dynamic_slice_in_dim(residual_f, column, feature_span, 1)
    return (own_residual + summed).astype(jnp.bfloat16)


def solution(mesh):
    split = Mesh(mesh.devices.reshape(8, 4, 2, mesh.shape["tp"]), ("ep_0", "ep_1", "ep_2", "tp"))
    return jax.shard_map(
        shards,
        mesh=split,
        in_specs=(
            P(EP, None),
            P(),
            P(None, "tp"),
            P(None, "tp"),
            P(None, "tp"),
            P(None, "tp"),
            P("tp"),
            P(),
            P(),
            P(EP, "tp", None, None),
            P(EP, "tp", None),
            P(EP),
            P("tp", None),
            P(),
            P(),
            P(),
            P(EP, None, "tp"),
            P(EP, None, "tp"),
            P(EP, "tp", None),
            P(),
            P(EP, None),
            P(EP, None),
            P(EP, "tp"),
        ),
        out_specs=P(EP, "tp"),
        check_vma=False,
    )
```

profile of v0, /device:TPU:32, one launch (start us, length us, event | category | flops | bytes accessed | tf_op | source)
XLA Modules:
  0.0 138.7 jit_solution(6740849996699019402)
XLA Ops:
  2.5 1.3 fusion.88
  4.1 1.3 multiply_reduce_fusion.1
  6.1 1.3 fusion.63
  7.3 1.0 fusion.78
  8.4 1.0 broadcast_subtract_fusion
  10.5 4.8 %fusion.89 = (f32[24,4]{1,0:T(8,128)S(1)}, f32[24,4,1024]{2,1,0:T(4,128)S(1)}) fusion(f32[24,1024]{1,0:T(8,128)S(1)} %bitcast.98, bf16[24,4,64]{2,1,0:T(4,128)(2,1)S(1)} %multiply_convert_fusion.1, bf16[24,1,1024,128]{3,2,1,0:T(8,128)(2,1)} %param.32, pred[24,1024]{1,0:T(8,128)(4,1)S(1)} %iota_compare_fusion), kind=kOutput, calls=%fused_computation.109 | convolution fusion | flops 12976032 | bytes 6820224 | tf_op jit(solution)/shard_map/bkgd,bkld->bkgl/dot_general | solution.py:115
  15.8 2.0 %fusion.35 = bf16[24,4,64]{2,1,0:T(4,128)(2,1)S(1)} fusion(bf16[24,1,1024,128]{3,2,1,0:T(8,128)(2,1)S(1)} %copy-done.13, f32[24,4,1024]{2,1,0:T(4,128)S(1)} %get-tuple-element.14, f32[24,4]{1,0:T(8,128)S(1)} %get-tuple-element.8, f32[24,4]{1,0:T(8,128)S(1)} %multiply_maximum_fusion, f32[24,64]{1,0:T(8,128)S(1)} %fusion.41, f32[24,4]{1,0:T(8,128)S(1)} %get-tuple-element.7), kind=kOutput, calls=%fused_computation.26 | convolution fusion | flops 12896256 | bytes 6704256 | tf_op jit(solution)/shard_map/bkgl,bkld->bkgd/dot_general | solution.py:130
  18.1 10.4 %all_to_all.30 = bf16[4,24,1024]{2,1,0:T(8,128)(2,1)S(1)} all-to-all(bf16[4,24,1024]{2,1,0:T(8,128)(2,1)S(1)} %broadcast_in_dim.28), channel_id=1, replica_groups=mesh['ep_0'=8,'ep_1'=4,'ep_2'=2,'tp'=4] {'tp'}, dimensions={0} | all-to-all | bytes 393216 | tf_op jit(solution)/shard_map/all_to_all | solution.py:15
  28.8 1.3 broadcast_in_dim.29
  30.2 11.5 %all-to-all-start.1 = ((bf16[32,24,1024]{2,1,0:T(8,128)(2,1)}), bf16[32,24,1024]{2,1,0:T(8,128)(2,1)S(1)}, u32[]{:S(2)}, u32[]{:S(2)}) async-start(bf16[32,24,1024]{2,1,0:T(8,128)(2,1)} %broadcast_in_dim.29), calls=%async_computation.1 | async-start | bytes 3145728 | tf_op jit(solution)/shard_map/all_to_all | solution.py:15
  43.9 1.3 select_reduce_fusion
  45.9 32.7 %all-to-all-done.1 = bf16[32,24,1024]{2,1,0:T(8,128)(2,1)S(1)} async-done(((bf16[32,24,1024]{2,1,0:T(8,128)(2,1)}), bf16[32,24,1024]{2,1,0:T(8,128)(2,1)S(1)}, u32[]{:S(2)}, u32[]{:S(2)}) %all-to-all-start.1) | async-done | bytes 1572896 | tf_op jit(solution)/shard_map/all_to_all | solution.py:15
  79.1 6.3 %all_to_all.31 = bf16[2,32,24,1024]{3,2,1,0:T(8,128)(2,1)S(1)} all-to-all(bf16[2,32,24,1024]{3,2,1,0:T(8,128)(2,1)S(1)} %broadcast_in_dim.30), channel_id=1, replica_groups=mesh['ep_0'=8,'ep_1'=4,'ep_2'=2,'tp'=4] {'ep_2'}, dimensions={0} | all-to-all | bytes 6291456 | tf_op jit(solution)/shard_map/all_to_all | solution.py:15
  85.8 1.7 %copy-done.1 = bf16[2,32,24,1024]{3,2,0,1:T(8,128)(2,1)} copy-done((bf16[2,32,24,1024]{3,2,0,1:T(8,128)(2,1)}, bf16[2,32,24,1024]{3,2,0,1:T(8,128)(2,1)S(1)}, u32[]{:S(2)}) %copy-start.1) | copy-done | bytes 3145752
  88.4 1.9 %fusion.13 = f32[128,896]{1,0:T(8,128)S(1)} fusion(bf16[128,1024]{1,0:T(8,128)(2,1)S(1)} %reshape.261, bf16[1,1024,896]{2,1,0:T(8,128)(2,1)} %param.39), kind=kOutput, calls=%fused_computation.15 | convolution fusion | flops 234881024 | bytes 2555904 | tf_op jit(solution)/shard_map/dot_general | solution.py:155
  90.4 2.3 %fusion.18 = bf16[128,1024]{1,0:T(8,128)(2,1)S(1)} fusion(bf16[1,896,1024]{2,1,0:T(8,128)(2,1)S(1)} %copy-done, bf16[128,1024]{1,0:T(8,128)(2,1)S(1)} %reshape.261, bf16[1,1024,896]{2,1,0:T(8,128)(2,1)} %param.40, f32[128,896]{1,0:T(8,128)S(1)} %fusion.13), kind=kOutput, calls=%fused_computation.19 | convolution fusion | flops 470581248 | bytes 4653056 | tf_op jit(solution)/shard_map/dot_general | solution.py:158
  93.5 3.4 %all-to-all-start.3 = ((bf16[4,128,256]{2,1,0:T(8,128)(2,1)}), bf16[4,128,256]{2,1,0:T(8,128)(2,1)S(1)}, u32[]{:S(2)}, u32[]{:S(2)}) async-start(bf16[4,128,256]{2,1,0:T(8,128)(2,1)} %bitcast.88), calls=%async_computation.3 | async-start | bytes 524288 | tf_op jit(solution)/shard_map/all_to_all | solution.py:42
  96.9 3.9 %fusion.90 = f32[1536,64]{0,1:T(8,128)} fusion(bf16[1536,1024]{1,0:T(8,128)(2,1)} %bitcast.92, bf16[64,1024]{1,0:T(8,128)(2,1)S(1)} %copy-done.5), kind=kOutput, calls=%fused_computation.110 | convolution fusion | flops 201326592 | bytes 3670016 | tf_op jit(solution)/shard_map/dot_general | solution.py:169
  101.7 2.4 %all-to-all-done.3 = bf16[4,128,256]{2,1,0:T(8,128)(2,1)S(1)} async-done(((bf16[4,128,256]{2,1,0:T(8,128)(2,1)}), bf16[4,128,256]{2,1,0:T(8,128)(2,1)S(1)}, u32[]{:S(2)}, u32[]{:S(2)}) %all-to-all-start.3) | async-done | bytes 262176 | tf_op jit(solution)/shard_map/all_to_all | solution.py:42
  105.7 4.3 %fusion.7 = bf16[1536,256]{1,0:T(8,128)(2,1)} fusion(f32[1536,256]{1,0:T(8,128)S(1)} %bitcast_multiply_fusion, bf16[64,256]{1,0:T(8,128)(2,1)S(1)} %copy-done.7, bf16[1536,1024]{1,0:T(8,128)(2,1)} %bitcast.93, bf16[64,1024]{1,0:T(8,128)(2,1)} %param.44, f32[1536]{0:T(1024)S(1)} %add_divide_fusion, f32[1536,64]{0,1:T(8,128)} %fusion.90), kind=kOutput, calls=%fused_computation.8 | convolution fusion | flops 253427712 | bytes 6068224 | tf_op jit(solution)/shard_map/dot_general | solution.py:177
  110.0 1.2 copy.54
  111.2 4.4 %all_to_all.32 = bf16[2,32,24,256]{3,2,1,0:T(8,128)(2,1)S(1)} all-to-all(bf16[2,32,24,256]{3,2,1,0:T(8,128)(2,1)S(1)} %bitcast.95), channel_id=1, replica_groups=mesh['ep_0'=8,'ep_1'=4,'ep_2'=2,'tp'=4] {'ep_2'}, dimensions={0} | all-to-all | bytes 1572864 | tf_op jit(solution)/shard_map/all_to_all | solution.py:42
  116.5 6.5 %all-to-all-start.5 = ((bf16[32,24,256]{2,1,0:T(8,128)(2,1)}), bf16[32,24,256]{2,1,0:T(8,128)(2,1)S(1)}, u32[]{:S(2)}, u32[]{:S(2)}) async-start(bf16[32,24,256]{2,1,0:T(8,128)(2,1)} %reduce_sum.124), calls=%async_computation.5 | async-start | bytes 786432 | tf_op jit(solution)/shard_map/all_to_all | solution.py:50
  123.0 15.0 %all-to-all-done.5 = bf16[32,24,256]{2,1,0:T(8,128)(2,1)S(1)} async-done(((bf16[32,24,256]{2,1,0:T(8,128)(2,1)}), bf16[32,24,256]{2,1,0:T(8,128)(2,1)S(1)}, u32[]{:S(2)}, u32[]{:S(2)}) %all-to-all-start.5) | async-done | bytes 393248 | tf_op jit(solution)/shard_map/all_to_all | solution.py:50
  (73 shorter events, 14.4 us)
Async XLA Ops:
  0.0 90.4 %copy-start = (bf16[1,896,1024]{2,1,0:T(8,128)(2,1)S(1)}, bf16[1,896,1024]{2,1,0:T(8,128)(2,1)}, u32[]{:S(2)}) copy-start(bf16[1,896,1024]{2,1,0:T(8,128)(2,1)} %param.41) | copy-start | bytes 5505028
  0.0 10.2 %copy-start.12 = (f32[64]{0:T(128)S(1)}, f32[64]{0:T(128)}, u32[]{:S(2)}) copy-start(f32[64]{0:T(128)} %param.31) | copy-start | bytes 772
  10.4 5.1 %copy-start.4 = (bf16[24,1024]{1,0:T(8,128)(2,1)S(1)}, bf16[24,1024]{1,0:T(8,128)(2,1)}, u32[]{:S(2)}) copy-start(bf16[24,1024]{1,0:T(8,128)(2,1)} %param.23) | copy-start | bytes 147460
  10.4 5.1 %copy-start.8 = (f32[1024]{0:T(1024)S(1)}, f32[1024]{0:T(1024)}, u32[]{:S(2)}) copy-start(f32[1024]{0:T(1024)} %param.24) | copy-start | bytes 12292
  10.4 5.1 %copy-start.14 = (bf16[1024,64]{0,1:T(8,128)(2,1)S(1)}, bf16[1024,64]{0,1:T(8,128)(2,1)}, u32[]{:S(2)}) copy-start(bf16[1024,64]{0,1:T(8,128)(2,1)} %param.27) | copy-start | bytes 393220
  10.5 5.3 %copy-start.13 = (bf16[24,1,1024,128]{3,2,1,0:T(8,128)(2,1)S(1)}, bf16[24,1,1024,128]{3,2,1,0:T(8,128)(2,1)}, u32[]{:S(2)}) copy-start(bf16[24,1,1024,128]{3,2,1,0:T(8,128)(2,1)} %param.32) | copy-start | bytes 18874372
  15.8 2.1 %copy-start.3 = (bf16[256,1024]{1,0:T(8,128)(2,1)S(1)}, bf16[256,1024]{1,0:T(8,128)(2,1)}, u32[]{:S(2)}) copy-start(bf16[256,1024]{1,0:T(8,128)(2,1)} %param.35) | copy-start | bytes 1572868
  15.8 12.9 %copy-start.9 = (f32[1024]{0:T(1024)S(1)}, f32[1024]{0:T(1024)}, u32[]{:S(2)}) copy-start(f32[1024]{0:T(1024)} %param.36) | copy-start | bytes 12292
  30.2 11.5 %copy-start.6 = (s32[1536,2]{0,1:T(2,128)S(1)}, s32[1536,2]{0,1:T(2,128)}, u32[]{:S(2)}) copy-start(s32[1536,2]{0,1:T(2,128)} %param.37) | copy-start | bytes 36868
  30.2 12.2 %copy-start.11 = (bf16[1024]{0:T(1024)(128)(2,1)S(1)}, bf16[1024]{0:T(1024)(128)(2,1)}, u32[]{:S(2)}) copy-start(bf16[1024]{0:T(1024)(128)(2,1)} %param.42) | copy-start | bytes 6148
  30.2 48.5 %all-to-all-start.1 = ((bf16[32,24,1024]{2,1,0:T(8,128)(2,1)}), bf16[32,24,1024]{2,1,0:T(8,128)(2,1)S(1)}, u32[]{:S(2)}, u32[]{:S(2)}) async-start(bf16[32,24,1024]{2,1,0:T(8,128)(2,1)} %broadcast_in_dim.29), calls=%async_computation.1 | async-start | bytes 3145728 | tf_op jit(solution)/shard_map/all_to_all | solution.py:15
  85.4 2.1 %copy-start.10 = (s32[2]{0:T(128)S(1)}, s32[2]{0:T(128)}, u32[]{:S(2)}) copy-start(s32[2]{0:T(128)} %iota_add_fusion) | copy-start | bytes 28
  85.8 1.7 %copy-start.1 = (bf16[2,32,24,1024]{3,2,0,1:T(8,128)(2,1)}, bf16[2,32,24,1024]{3,2,0,1:T(8,128)(2,1)S(1)}, u32[]{:S(2)}) copy-start(bf16[2,32,24,1024]{3,2,0,1:T(8,128)(2,1)S(1)} %copy.40) | copy-start | bytes 9437188
  90.4 6.5 %copy-start.5 = (bf16[64,1024]{1,0:T(8,128)(2,1)S(1)}, bf16[64,1024]{1,0:T(8,128)(2,1)}, u32[]{:S(2)}) copy-start(bf16[64,1024]{1,0:T(8,128)(2,1)} %param.43) | copy-start | bytes 393220
  93.5 10.6 %all-to-all-start.3 = ((bf16[4,128,256]{2,1,0:T(8,128)(2,1)}), bf16[4,128,256]{2,1,0:T(8,128)(2,1)S(1)}, u32[]{:S(2)}, u32[]{:S(2)}) async-start(bf16[4,128,256]{2,1,0:T(8,128)(2,1)} %bitcast.88), calls=%async_computation.3 | async-start | bytes 524288 | tf_op jit(solution)/shard_map/all_to_all | solution.py:42
  96.9 3.9 %copy-start.2 = (bf16[2,32,24,1024]{3,2,0,1:T(8,128)(2,1)S(1)}, bf16[2,32,24,1024]{3,2,0,1:T(8,128)(2,1)}, u32[]{:S(2)}) copy-start(bf16[2,32,24,1024]{3,2,0,1:T(8,128)(2,1)} %copy-done.1) | copy-start | bytes 9437188
  104.7 1.0 copy-start.7
  116.5 21.4 %all-to-all-start.5 = ((bf16[32,24,256]{2,1,0:T(8,128)(2,1)}), bf16[32,24,256]{2,1,0:T(8,128)(2,1)S(1)}, u32[]{:S(2)}, u32[]{:S(2)}) async-start(bf16[32,24,256]{2,1,0:T(8,128)(2,1)} %reduce_sum.124), calls=%async_computation.5 | async-start | bytes 786432 | tf_op jit(solution)/shard_map/all_to_all | solution.py:50
where the time goes:
time: 140 us; the launch traced here: 139 us
  waiting for transfers between devices  50.1 us (36%)
  matrix products  25.6 us (18%)
  starting transfers between devices  21.3 us (15%)
  blocking collectives  21 us (15%)
  other arithmetic  12.5 us (9%)
  local copies, waits for them, and re-layouts  7.02 us (5%)
    all_to_all x1, waiting for transfers between devices, from_everyone(): lax.all_to_all(jnp.broadcast_to(x[None], (count, *x.shape)), axis, 0, 0,...  32.7 us
    all_to_all x2, blocking collectives, from_everyone(): lax.all_to_all(jnp.broadcast_to(x[None], (count, *x.shape)), axis, 0, 0,...  16.7 us
    all_to_all x1, waiting for transfers between devices, sum_in_two_steps(): lax.all_to_all(nearer.astype(jnp.bfloat16), far, split_axis=0, concat_axi...  15 us
    all_to_all x1, starting transfers between devices, from_everyone(): lax.all_to_all(jnp.broadcast_to(x[None], (count, *x.shape)), axis, 0, 0,...  11.5 us
    all_to_all x1, starting transfers between devices, sum_in_two_steps(): lax.all_to_all(nearer.astype(jnp.bfloat16), far, split_axis=0, concat_axi...  6.45 us
    dot_general x1, matrix products, shards(): jnp.einsum('bkgd,bkld->bkgl', query_rows, cached_keys, preferred_element_...  4.76 us
    all_to_all x1, blocking collectives, sent_and_summed(): parts = lax.all_to_all(in_blocks(x, dim, count), axis, 0, 0, tiled=True)  4.37 us
    dot_general x1, matrix products, shards(): jnp.dot(dense_hidden, w_dense_down, preferred_element_type=jnp.float32)  4.33 us
  transfers between devices with their start and end apart: 3, of which 3 were waited for; matrix products, arithmetic and copies ran while one was open for 7% of the time, Pallas kernels for 0%

commit v1 on v0

--- a/solution.py
+++ b/solution.py
@@ -5,6 +5,7 @@
 from jax.sharding import PartitionSpec as P
 
 EP = ("ep_0", "ep_1", "ep_2")
+FAR = ("ep_0", "ep_1")
 
 
 EPSILON = 1e-06
@@ -83,6 +84,11 @@
     w_dense_up,
     w_dense_down,
 ):
+    def other(w):
+        return lax.ppermute(w, "ep_2", [(0, 1), (1, 0)])
+
+    gate_other, up_other, down_other = other(w_exp_gate[0]), other(w_exp_up[0]), other(w_exp_down[0])
+    dense_gate_other, dense_up_other, dense_down_other = other(w_dense_gate), other(w_dense_up), other(w_dense_down)
     seq_rows, width = tokens.shape
     head_size = query_gain.shape[0]
     kv_here = cache_pairs.shape[1]
@@ -139,49 +145,96 @@
     residual = (tokens_f + attn_out).astype(jnp.bfloat16)
     residual_f = residual.astype(jnp.float32)
     normed_two = rms_scale(residual_f, ffn_gain).astype(jnp.bfloat16)
-    all_rows = whole_of(normed_two, (("ep_0", "ep_1"), "ep_2"), 0)
-    batch_rows = all_rows.shape[0]
-    num_groups = lax.axis_size(EP)
-    capacity = max(2, min(seq_rows, 128 // num_groups))
-    chosen = expert_ids == lax.axis_index(EP)
-    is_hit = jnp.sum(chosen.astype(jnp.int32), axis=1).reshape(num_groups, seq_rows)
-    weight_here = jnp.sum(jnp.where(chosen, route_weight, 0.0), axis=1)
-    slot_rank = jnp.cumsum(is_hit, axis=1)
-    slot_ids = lax.broadcasted_iota(jnp.int32, (1, capacity, 1), 1) + 1
-    picker = ((slot_rank[:, None, :] == slot_ids) & (is_hit[:, None, :] == 1)).astype(jnp.bfloat16)
-    grouped = all_rows.reshape(num_groups, seq_rows, width)
-    picked = jnp.einsum("scn,snd->scd", picker, grouped, preferred_element_type=jnp.float32)
-    picked = picked.astype(jnp.bfloat16).reshape(num_groups * capacity, width)
-    gate_part = jnp.dot(picked, w_exp_gate[0], preferred_element_type=jnp.float32)
-    up_part = jnp.dot(picked, w_exp_up[0], preferred_element_type=jnp.float32)
-    hidden = (jax.nn.silu(gate_part) * up_part).astype(jnp.bfloat16)
-    expert_part = jnp.dot(hidden, w_exp_down[0], preferred_element_type=jnp.float32)
-    expert_rows = sent_and_summed(expert_part.astype(jnp.bfloat16), "tp", 1).astype(jnp.bfloat16)
-    feature_span = expert_rows.shape[1]
-    placed = jnp.einsum(
+
+    tp_at, core_at = lax.axis_index("tp"), lax.axis_index("ep_2")
+    n_tp, n_core = lax.axis_size("tp"), lax.axis_size("ep_2")
+    chips = lax.axis_size(FAR)
+    chip_at = lax.axis_index(FAR)
+    cap = 2
+    share = seq_rows // n_tp
+
+    ids = expert_ids.reshape(chips, n_core, seq_rows, -1)
+    ids_plane = lax.dynamic_index_in_dim(ids, core_at, 1, keepdims=False)
+    ids_own = lax.dynamic_index_in_dim(ids_plane, chip_at, 0, keepdims=False)
+    cores = jnp.stack([core_at, 1 - core_at])
+    dest = jnp.arange(chips)[:, None] * n_core + cores[None, :]
+    hit = jnp.any(ids_own[None, None] == dest[:, :, None, None], axis=3)
+    rank = jnp.cumsum(hit.astype(jnp.int32), axis=2)
+    slot = jnp.arange(1, cap + 1)
+    pick = (hit[:, :, None, :] & (rank[:, :, None, :] == slot[None, None, :, None])).astype(jnp.bfloat16)
+    sent = jnp.dot(
+        pick.reshape(-1, seq_rows), normed_two, preferred_element_type=jnp.float32
+    ).astype(jnp.bfloat16)
+    slots = n_core * cap
+    mine = lax.dynamic_slice_in_dim(normed_two, tp_at * share, share, 0)
+    message = jnp.concatenate(
+        [
+            sent.reshape(chips, slots, width),
+            jnp.broadcast_to(mine[None], (chips, share, width)),
+        ],
+        axis=1,
+    )
+    message = message.reshape(chips, -1, 128)
+    arrived = lax.all_to_all(message, FAR, 0, 0, tiled=True)
+    arrived = arrived.reshape(chips, slots + share, width)
+    to_expert = arrived[:, :slots].reshape(chips, n_core, cap, width)
+    to_dense = arrived[:, slots:].reshape(chips * share, width)
+
+    def expert(rows, gate_w, up_w, down_w):
+        gate_part = jnp.dot(rows, gate_w, preferred_element_type=jnp.float32)
+        up_part = jnp.dot(rows, up_w, preferred_element_type=jnp.float32)
+        hidden = (jax.nn.silu(gate_part) * up_part).astype(jnp.bfloat16)
+        return jnp.dot(hidden, down_w, preferred_element_type=jnp.float32).astype(jnp.bfloat16)
+
+    part_own = expert(to_expert[:, 0].reshape(-1, width), w_exp_gate[0], w_exp_up[0], w_exp_down[0])
+    part_other = expert(to_expert[:, 1].reshape(-1, width), gate_other, up_other, down_other)
+    expert_part = jnp.stack(
+        [part_own.reshape(chips, cap, width), part_other.reshape(chips, cap, width)], axis=1
+    ).reshape(chips * slots, width)
+
+    contract = (((1,), (1,)), ((), ()))
+    dense_gate_w = jnp.concatenate([w_dense_gate, dense_gate_other], axis=0)
+    dense_up_w = jnp.concatenate([w_dense_up, dense_up_other], axis=0)
+    dense_down_w = jnp.concatenate([w_dense_down, dense_down_other], axis=0)
+    dense_gate_raw = lax.dot_general(to_dense, dense_gate_w, contract, preferred_element_type=jnp.float32)
+    dense_up_raw = lax.dot_general(to_dense, dense_up_w, contract, preferred_element_type=jnp.float32)
+    mix_gate = jax.nn.sigmoid(jnp.dot(to_dense, shared_gate, preferred_element_type=jnp.float32))
+    dense_hidden = (mix_gate[:, None] * (jax.nn.silu(dense_gate_raw) * dense_up_raw)).astype(jnp.bfloat16)
+    span = width // n_tp
+    hidden_size = dense_hidden.shape[1]
+    blocks = jnp.concatenate(
+        [
+            in_blocks(expert_part, 1, n_tp),
+            jnp.broadcast_to(dense_hidden.reshape(1, -1, span), (n_tp, dense_hidden.size // span, span)),
+        ],
+        axis=1,
+    )
+    crossed = lax.all_to_all(blocks, "tp", 0, 0, tiled=True)
+    expert_rows = crossed[:, : chips * slots].astype(jnp.float32).sum(axis=0).astype(jnp.bfloat16)
+    hidden_all = crossed[:, chips * slots :].reshape(n_tp, chips, share, hidden_size)
+    hidden_all = hidden_all.swapaxes(0, 1).reshape(chips * seq_rows, hidden_size)
+    dense_rows = jnp.dot(hidden_all, dense_down_w, preferred_element_type=jnp.float32)
+
+    weights_plane = lax.dynamic_index_in_dim(
+        route_weight.reshape(chips, n_core, seq_rows, -1), core_at, 1, keepdims=False
+    )
+    here = chip_at * n_core + cores
+    chosen = ids_plane[:, None] == here[None, :, None, None]
+    hit_here = jnp.any(chosen, axis=3)
+    weight_here = jnp.sum(jnp.where(chosen, weights_plane[:, None], 0.0), axis=3)
+    rank_here = jnp.cumsum(hit_here.astype(jnp.int32), axis=2)
+    place = hit_here[:, :, None, :] & (rank_here[:, :, None, :] == slot[None, None, :, None])
+    place = jnp.where(place, weight_here[:, :, None, :], 0.0).reshape(chips, slots, seq_rows)
+    expert_term = jnp.einsum(
         "scn,scd->snd",
-        picker,
-        expert_rows.reshape(num_groups, capacity, feature_span),
+        place,
+        expert_rows.reshape(chips, slots, span).astype(jnp.float32),
+        precision=lax.Precision.HIGHEST,
         preferred_element_type=jnp.float32,
-    ).reshape(batch_rows, feature_span)
-    expert_term = placed * weight_here[:, None]
-    contract = (((1,), (1,)), ((), ()))
-    dense_gate_raw = lax.dot_general(
-        all_rows, w_dense_gate, contract, preferred_element_type=jnp.float32
-    )
-    dense_up_raw = lax.dot_general(
-        all_rows, w_dense_up, contract, preferred_element_type=jnp.float32
-    )
-    dense_hidden = (jax.nn.silu(dense_gate_raw) * dense_up_raw).astype(jnp.bfloat16)
-    mix_gate = jax.nn.sigmoid(jnp.dot(all_rows, shared_gate, preferred_element_type=jnp.float32))
-    dense_rows = jnp.dot(dense_hidden, w_dense_down, preferred_element_type=jnp.float32)
-    summed = sum_in_two_steps(
-        (mix_gate[:, None] * dense_rows + expert_term).astype(jnp.bfloat16),
-        (("ep_0", "ep_1"), "ep_2"),
-        0,
-    )
-    column = lax.axis_index("tp") * feature_span
-    own_residual = lax.dynamic_slice_in_dim(residual_f, column, feature_span, 1)
+    )
+    total = (dense_rows.reshape(chips, seq_rows, span) + expert_term).astype(jnp.bfloat16)
+    summed = lax.all_to_all(total, FAR, 0, 0, tiled=True).astype(jnp.float32).sum(axis=0)
+    own_residual = lax.dynamic_slice_in_dim(residual_f, tp_at * span, span, 1)
     return (own_residual + summed).astype(jnp.bfloat16)
 
 

time: 140 us -> 113 us (0.81)
  blocking collectives: 21 us -> 0 us
  waiting for transfers between devices: 50.1 us -> 45 us
  starting transfers between devices: 21.3 us -> 25.9 us
  other arithmetic: 12.5 us -> 9.16 us
  matrix products: 25.6 us -> 23.9 us
    all_to_all x1, waiting for transfers between devices: 32.7 us -> 5.04 us  [from_everyone(): lax.all_to_all(jnp.broadcast_to(x[None], (count, *x.shape)), axis, 0, 0,...]
    all_to_all x2 -> x3, waiting for transfers between devices: 17.4 us -> 40 us  [the longest x1 17 us: shards(): arrived = lax.all_to_all(message, FAR, 0, 0, tiled=True)]
    all_to_all x3 -> x0, blocking collectives: 21 us -> none  [the longest x2 16.7 us: from_everyone(): lax.all_to_all(jnp.broadcast_to(x[None], (count, *x.shape)), axis, 0, 0,...]
    all_to_all x2 -> x3, starting transfers between devices: 9.85 us -> 20.2 us  [the longest x1 11.4 us: shards(): arrived = lax.all_to_all(message, FAR, 0, 0, tiled=True)]
    all_to_all x1, starting transfers between devices: 11.5 us -> 4.29 us  [from_everyone(): lax.all_to_all(jnp.broadcast_to(x[None], (count, *x.shape)), axis, 0, 0,...]
    reduce_sum x5 -> x3, other arithmetic: 2.43 us -> 0.18 us  [the longest x1 0.08 us: shards(): jnp.sum(jnp.where(chosen, weights_plane[:, None], 0.0), axis=3)]
    dot_general x7 -> x10, matrix products: 14.7 us -> 13 us  [the longest x2 5.65 us: expert(): jnp.dot(hidden, down_w, preferred_element_type=jnp.float32)]
    unnamed x32 -> x28, local copies, waits for them, and re-layouts: 1.76 us -> 0.2 us
  transfers between devices with their start and end apart: 3 -> 10, of which waited for: 3 -> 4; matrix products, arithmetic and copies ran while one was open for 7% -> 16% of each run, Pallas kernels for 0% -> 0%
where the time goes in v1:
time: 113 us; the launch traced here: 112 us
  waiting for transfers between devices  45 us (40%)
  starting transfers between devices  25.9 us (23%)
  matrix products  23.9 us (21%)
  other arithmetic  9.16 us (8%)
  local copies, waits for them, and re-layouts  6.48 us (6%)
  between operations  1.36 us (1%)
    all_to_all x1, waiting for transfers between devices, shards(): arrived = lax.all_to_all(message, FAR, 0, 0, tiled=True)  17 us
    all_to_all x1, waiting for transfers between devices, shards(): lax.all_to_all(total, FAR, 0, 0, tiled=True).astype(jnp.float32).sum(axis=0)  14.5 us
    all_to_all x1, starting transfers between devices, shards(): arrived = lax.all_to_all(message, FAR, 0, 0, tiled=True)  11.4 us
    all_to_all x1, waiting for transfers between devices, shards(): crossed = lax.all_to_all(blocks, 'tp', 0, 0, tiled=True)  8.49 us
    dot_general x2, matrix products, expert(): jnp.dot(hidden, down_w, preferred_element_type=jnp.float32)  5.65 us
    all_to_all x1, starting transfers between devices, shards(): lax.all_to_all(total, FAR, 0, 0, tiled=True).astype(jnp.float32).sum(axis=0)  5.37 us
    all_to_all x1, waiting for transfers between devices, from_everyone(): lax.all_to_all(jnp.broadcast_to(x[None], (count, *x.shape)), axis, 0, 0,...  5.04 us
    dot_general x1, matrix products, shards(): jnp.einsum('bkgd,bkld->bkgl', query_rows, cached_keys, preferred_element_...  4.76 us
  transfers between devices with their start and end apart: 10, of which 4 were waited for; matrix products, arithmetic and copies ran while one was open for 16% of the time, Pallas kernels for 0%

profile of v1, /device:TPU:32, one launch (start us, length us, event | category | flops | bytes accessed | tf_op | source)
XLA Modules:
  0.0 111.8 jit_solution(11834050285751282260)
XLA Ops:
  2.1 0.9 fusion.45
  3.1 1.3 %fusion.49 = f32[24]{0:T(128)S(1)} fusion(f32[24,1,1024]{2,1,0:T(1,128)} %param.33, s32[24]{0:T(128)S(1)} %broadcast_add_fusion.2), kind=kLoop, calls=%fused_computation.65 | loop fusion | flops 73704 | bytes 98496 | tf_op jit(solution)/shard_map/reduce_sum | solution.py:115
  4.3 1.0 fusion.64
  5.4 1.0 broadcast_subtract_fusion
  6.5 1.3 %fusion.85 = (f32[24,256]{1,0:T(8,128)S(1)}, f32[24,256]{1,0:T(8,128)S(1)}) fusion(bf16[1024,256]{1,0:T(8,128)(2,1)} %param.25, bf16[24,1024]{1,0:T(8,128)(2,1)} %param.23, f32[1024]{0:T(1024)} %param.24, f32[24]{0:T(128)S(1)} %add_rsqrt_fusion.3), kind=kOutput, calls=%fused_computation.123 | convolution fusion | flops 12687360 | bytes 626784 | tf_op jit(solution)/shard_map/dot_general | solution.py:98
  8.1 1.3 %multiply_reduce_fusion.1 = (f32[24]{0:T(128)S(1)}, f32[24,64]{1,0:T(8,128)S(1)}) fusion(bf16[1024,64]{0,1:T(8,128)(2,1)} %param.26, bf16[24,1024]{1,0:T(8,128)(2,1)} %param.23, f32[1024]{0:T(1024)} %param.24, f32[24]{0:T(128)S(1)} %add_rsqrt_fusion.3), kind=kOutput, calls=%fused_computation.86 | convolution fusion | flops 3247080 | bytes 190656 | tf_op jit(solution)/shard_map/dot_general | solution.py:104
  10.4 4.8 %fusion.86 = (f32[24,4]{1,0:T(8,128)S(1)}, f32[24,4,1024]{2,1,0:T(4,128)S(1)}) fusion(f32[24,1024]{1,0:T(8,128)S(1)} %bitcast.106, bf16[24,4,64]{2,1,0:T(4,128)(2,1)S(1)} %multiply_convert_fusion.4, bf16[24,1,1024,128]{3,2,1,0:T(8,128)(2,1)} %param.32, pred[24,1024]{1,0:T(8,128)(4,1)S(1)} %iota_compare_fusion), kind=kOutput, calls=%fused_computation.124 | convolution fusion | flops 12976032 | bytes 6820224 | tf_op jit(solution)/shard_map/bkgd,bkld->bkgl/dot_general | solution.py:121
  15.7 2.0 %fusion.17 = bf16[24,4,64]{2,1,0:T(4,128)(2,1)S(1)} fusion(bf16[24,1,1024,128]{3,2,1,0:T(8,128)(2,1)S(1)} %copy-done.9, f32[24,4,1024]{2,1,0:T(4,128)S(1)} %get-tuple-element.18, f32[24,4]{1,0:T(8,128)S(1)} %get-tuple-element.12, f32[24,4]{1,0:T(8,128)S(1)} %multiply_maximum_fusion, f32[24,64]{1,0:T(8,128)S(1)} %fusion.23, f32[24,4]{1,0:T(8,128)S(1)} %get-tuple-element.11), kind=kOutput, calls=%fused_computation.17 | convolution fusion | flops 12896256 | bytes 6704256 | tf_op jit(solution)/shard_map/bkgl,bkld->bkgd/dot_general | solution.py:136
  18.7 4.3 %all-to-all-start = ((bf16[4,24,1024]{2,1,0:T(8,128)(2,1)}), bf16[4,24,1024]{2,1,0:T(8,128)(2,1)S(1)}, u32[]{:S(2)}, u32[]{:S(2)}) async-start(bf16[4,24,1024]{2,1,0:T(8,128)(2,1)} %broadcast_in_dim.47), calls=%async_computation | async-start | bytes 393216 | tf_op jit(solution)/shard_map/all_to_all | solution.py:16
  24.3 5.0 %all-to-all-done = bf16[4,24,1024]{2,1,0:T(8,128)(2,1)S(1)} async-done(((bf16[4,24,1024]{2,1,0:T(8,128)(2,1)}), bf16[4,24,1024]{2,1,0:T(8,128)(2,1)S(1)}, u32[]{:S(2)}, u32[]{:S(2)}) %all-to-all-start) | async-done | bytes 196640 | tf_op jit(solution)/shard_map/all_to_all | solution.py:16
  30.6 1.3 %reshape.342 = bf16[32,80,128]{2,1,0:T(8,128)(2,1)} reshape(bf16[32,10,1024]{2,1,0:T(8,128)(2,1)S(1)} %pad_maximum_fusion) | data formatting | bytes 1310720 | tf_op jit(solution)/shard_map/reshape | solution.py:177
  31.8 11.4 %all-to-all-start.1 = ((bf16[32,80,128]{2,1,0:T(8,128)(2,1)}), bf16[32,80,128]{2,1,0:T(8,128)(2,1)S(1)}, u32[]{:S(2)}, u32[]{:S(2)}) async-start(bf16[32,80,128]{2,1,0:T(8,128)(2,1)} %reshape.342), calls=%async_computation.1 | async-start | bytes 1310720 | tf_op jit(solution)/shard_map/all_to_all | solution.py:178
  44.6 17.0 %all-to-all-done.1 = bf16[32,80,128]{2,1,0:T(8,128)(2,1)S(1)} async-done(((bf16[32,80,128]{2,1,0:T(8,128)(2,1)}), bf16[32,80,128]{2,1,0:T(8,128)(2,1)S(1)}, u32[]{:S(2)}, u32[]{:S(2)}) %all-to-all-start.1) | async-done | bytes 655392 | tf_op jit(solution)/shard_map/all_to_all | solution.py:178
  62.9 1.2 %fusion.27 = f32[192,128]{1,0:T(8,128)S(1)} fusion(bf16[192,1024]{1,0:T(8,128)(2,1)S(1)} %reshape.345, bf16[64,1024]{1,0:T(8,128)(2,1)} %collective-permute-done.3, bf16[64,1024]{1,0:T(8,128)(2,1)S(1)} %copy-done.11), kind=kOutput, calls=%fused_computation.34 | convolution fusion | flops 50855936 | bytes 753664 | tf_op jit(solution)/shard_map/dot_general | solution.py:199
  64.8 1.9 %fusion.73 = f32[64,896]{1,0:T(8,128)S(1)} fusion(bf16[64,1024]{1,0:T(8,128)(2,1)S(1)} %reshape_squeeze.6, bf16[1,1024,896]{2,1,0:T(8,128)(2,1)} %param.39), kind=kOutput, calls=%fused_computation.116 | convolution fusion | flops 117440512 | bytes 2195456 | tf_op jit(solution)/shard_map/dot_general | solution.py:184
  66.8 2.8 %convolution_convert_fusion.2 = bf16[64,1024]{1,0:T(8,128)(2,1)S(1)} fusion(bf16[64,1024]{1,0:T(8,128)(2,1)S(1)} %reshape_squeeze.6, f32[64,896]{1,0:T(8,128)S(1)} %fusion.73, bf16[1,896,1024]{2,1,0:T(8,128)(2,1)} %param.41, bf16[1,1024,896]{2,1,0:T(8,128)(2,1)} %param.40), kind=kOutput, calls=%fused_computation.13 | convolution fusion | flops 235290624 | bytes 4161536 | tf_op jit(solution)/shard_map/dot_general | solution.py:187
  69.7 1.9 %fusion.89 = f32[64,896]{1,0:T(8,128)S(1)} fusion(bf16[64,1024]{1,0:T(8,128)(2,1)S(1)} %reshape_squeeze.7, bf16[1024,896]{1,0:T(8,128)(2,1)} %collective-permute-done), kind=kOutput, calls=%fused_computation.126 | convolution fusion | flops 117440512 | bytes 2195456 | tf_op jit(solution)/shard_map/dot_general | solution.py:184
  71.6 2.8 %convolution_convert_fusion.1 = bf16[64,1024]{1,0:T(8,128)(2,1)S(1)} fusion(bf16[896,1024]{1,0:T(8,128)(2,1)} %collective-permute-done.2, f32[64,896]{1,0:T(8,128)S(1)} %fusion.89, bf16[64,1024]{1,0:T(8,128)(2,1)S(1)} %reshape_squeeze.7, bf16[1024,896]{1,0:T(8,128)(2,1)} %collective-permute-done.1), kind=kOutput, calls=%fused_computation.12 | convolution fusion | flops 235290624 | bytes 4161536 | tf_op jit(solution)/shard_map/dot_general | solution.py:187
  75.4 0.8 copy.73
  76.3 3.5 %all-to-all-start.2 = ((bf16[4,224,256]{2,1,0:T(8,128)(2,1)}), bf16[4,224,256]{2,1,0:T(8,128)(2,1)S(1)}, u32[]{:S(2)}, u32[]{:S(2)}) async-start(bf16[4,224,256]{2,1,0:T(8,128)(2,1)} %copy.73), calls=%async_computation.2 | async-start | bytes 917504 | tf_op jit(solution)/shard_map/all_to_all | solution.py:212
  80.9 8.5 %all-to-all-done.2 = bf16[4,224,256]{2,1,0:T(8,128)(2,1)S(1)} async-done(((bf16[4,224,256]{2,1,0:T(8,128)(2,1)}), bf16[4,224,256]{2,1,0:T(8,128)(2,1)S(1)}, u32[]{:S(2)}, u32[]{:S(2)}) %all-to-all-start.2) | async-done | bytes 458784 | tf_op jit(solution)/shard_map/all_to_all | solution.py:212
  90.2 1.0 fusion.6
  91.2 5.4 %all-to-all-start.3 = ((bf16[32,24,256]{2,1,0:T(8,128)(2,1)}), bf16[32,24,256]{2,1,0:T(8,128)(2,1)S(1)}, u32[]{:S(2)}, u32[]{:S(2)}) async-start(bf16[32,24,256]{2,1,0:T(8,128)(2,1)} %fusion.6), calls=%async_computation.3 | async-start | bytes 786432 | tf_op jit(solution)/shard_map/all_to_all | solution.py:236
  96.6 14.5 %all-to-all-done.3 = bf16[32,24,256]{2,1,0:T(8,128)(2,1)S(1)} async-done(((bf16[32,24,256]{2,1,0:T(8,128)(2,1)}), bf16[32,24,256]{2,1,0:T(8,128)(2,1)S(1)}, u32[]{:S(2)}, u32[]{:S(2)}) %all-to-all-start.3) | async-done | bytes 393248 | tf_op jit(solution)/shard_map/all_to_all | solution.py:236
  (125 shorter events, 13.5 us)
Async XLA Ops:
  0.0 17.9 %copy-start = (bf16[256,1024]{1,0:T(8,128)(2,1)S(1)}, bf16[256,1024]{1,0:T(8,128)(2,1)}, u32[]{:S(2)}) copy-start(bf16[256,1024]{1,0:T(8,128)(2,1)} %param.35) | copy-start | bytes 1572868
  0.0 10.1 %copy-start.8 = (f32[64]{0:T(128)S(1)}, f32[64]{0:T(128)}, u32[]{:S(2)}) copy-start(f32[64]{0:T(128)} %param.31) | copy-start | bytes 772
  10.3 5.1 %copy-start.1 = (bf16[24,1024]{1,0:T(8,128)(2,1)S(1)}, bf16[24,1024]{1,0:T(8,128)(2,1)}, u32[]{:S(2)}) copy-start(bf16[24,1024]{1,0:T(8,128)(2,1)} %param.23) | copy-start | bytes 147460
  10.4 5.1 %copy-start.5 = (f32[1024]{0:T(1024)S(1)}, f32[1024]{0:T(1024)}, u32[]{:S(2)}) copy-start(f32[1024]{0:T(1024)} %param.24) | copy-start | bytes 12292
  10.4 5.1 %copy-start.10 = (bf16[1024,64]{0,1:T(8,128)(2,1)S(1)}, bf16[1024,64]{0,1:T(8,128)(2,1)}, u32[]{:S(2)}) copy-start(bf16[1024,64]{0,1:T(8,128)(2,1)} %param.27) | copy-start | bytes 393220
  10.4 5.3 %copy-start.9 = (bf16[24,1,1024,128]{3,2,1,0:T(8,128)(2,1)S(1)}, bf16[24,1,1024,128]{3,2,1,0:T(8,128)(2,1)}, u32[]{:S(2)}) copy-start(bf16[24,1,1024,128]{3,2,1,0:T(8,128)(2,1)} %param.32) | copy-start | bytes 18874372
  15.7 7.3 %copy-start.3 = (s32[1536,2]{0,1:T(2,128)S(1)}, s32[1536,2]{0,1:T(2,128)}, u32[]{:S(2)}) copy-start(s32[1536,2]{0,1:T(2,128)} %param.37) | copy-start | bytes 36868
  17.7 11.8 %copy-start.6 = (f32[1024]{0:T(1024)S(1)}, f32[1024]{0:T(1024)}, u32[]{:S(2)}) copy-start(f32[1024]{0:T(1024)} %param.36) | copy-start | bytes 12292
  18.7 10.6 %all-to-all-start = ((bf16[4,24,1024]{2,1,0:T(8,128)(2,1)}), bf16[4,24,1024]{2,1,0:T(8,128)(2,1)S(1)}, u32[]{:S(2)}, u32[]{:S(2)}) async-start(bf16[4,24,1024]{2,1,0:T(8,128)(2,1)} %broadcast_in_dim.47), calls=%async_computation | async-start | bytes 393216 | tf_op jit(solution)/shard_map/all_to_all | solution.py:16
  30.5 12.8 %copy-start.11 = (bf16[64,1024]{1,0:T(8,128)(2,1)S(1)}, bf16[64,1024]{1,0:T(8,128)(2,1)}, u32[]{:S(2)}) copy-start(bf16[64,1024]{1,0:T(8,128)(2,1)} %param.43) | copy-start | bytes 393220
  30.5 13.3 %copy-start.12 = (bf16[64,1024]{1,0:T(8,128)(2,1)S(1)}, bf16[64,1024]{1,0:T(8,128)(2,1)}, u32[]{:S(2)}) copy-start(bf16[64,1024]{1,0:T(8,128)(2,1)} %param.44) | copy-start | bytes 393220
  30.5 13.9 %copy-start.4 = (f32[1536,2]{0,1:T(2,128)S(1)}, f32[1536,2]{0,1:T(2,128)}, u32[]{:S(2)}) copy-start(f32[1536,2]{0,1:T(2,128)} %param.38) | copy-start | bytes 36868
  30.5 14.0 %copy-start.7 = (bf16[1024]{0:T(1024)(128)(2,1)S(1)}, bf16[1024]{0:T(1024)(128)(2,1)}, u32[]{:S(2)}) copy-start(bf16[1024]{0:T(1024)(128)(2,1)} %param.42) | copy-start | bytes 6148
  31.8 29.8 %all-to-all-start.1 = ((bf16[32,80,128]{2,1,0:T(8,128)(2,1)}), bf16[32,80,128]{2,1,0:T(8,128)(2,1)S(1)}, u32[]{:S(2)}, u32[]{:S(2)}) async-start(bf16[32,80,128]{2,1,0:T(8,128)(2,1)} %reshape.342), calls=%async_computation.1 | async-start | bytes 1310720 | tf_op jit(solution)/shard_map/all_to_all | solution.py:178
  43.2 26.5 %collective-permute-start = (bf16[1024,896]{1,0:T(8,128)(2,1)}, bf16[1024,896]{1,0:T(8,128)(2,1)}, u32[]{:S(2)}, u32[]{:S(2)}) collective-permute-start(bf16[1024,896]{1,0:T(8,128)(2,1)} %bitcast.11), channel_id=1, source_target_pairs={{0,4},{4,0},{1,5},{5,1},{2,6},{6,2},{3,7},{7,3},{8,12},{12,8},{9,1... | collective-permute-start | bytes 5505032 | tf_op jit(solution)/shard_map/ppermute | solution.py:88
  43.3 19.3 %collective-permute-start.3 = (bf16[64,1024]{1,0:T(8,128)(2,1)S(1)}, bf16[64,1024]{1,0:T(8,128)(2,1)}, u32[]{:S(2)}, u32[]{:S(2)}) collective-permute-start(bf16[64,1024]{1,0:T(8,128)(2,1)S(1)} %copy-done.11), channel_id=1, source_target_pairs={{0,4},{4,0},{1,5},{5,1},{2,6},{6,2},{3,7},{7,3},{8,12},{12,8},{9,1... | collective-permute-start | bytes 393224 | tf_op jit(solution)/shard_map/ppermute | solution.py:88
  43.8 20.3 %collective-permute-start.4 = (bf16[64,1024]{1,0:T(8,128)(2,1)S(1)}, bf16[64,1024]{1,0:T(8,128)(2,1)S(1)}, u32[]{:S(2)}, u32[]{:S(2)}) collective-permute-start(bf16[64,1024]{1,0:T(8,128)(2,1)S(1)} %copy-done.12), channel_id=1, source_target_pairs={{0,4},{4,0},{1,5},{5,1},{2,6},{6,2},{3,7},{7,3},{8,12},{12,8},{9,1... | collective-permute-start | bytes 393224 | tf_op jit(solution)/shard_map/ppermute | solution.py:88
  43.9 27.7 %collective-permute-start.2 = (bf16[896,1024]{1,0:T(8,128)(2,1)}, bf16[896,1024]{1,0:T(8,128)(2,1)}, u32[]{:S(2)}, u32[]{:S(2)}) collective-permute-start(bf16[896,1024]{1,0:T(8,128)(2,1)} %bitcast.13), channel_id=1, source_target_pairs={{0,4},{4,0},{1,5},{5,1},{2,6},{6,2},{3,7},{7,3},{8,12},{12,8},{9,1... | collective-permute-start | bytes 5505032 | tf_op jit(solution)/shard_map/ppermute | solution.py:88
  44.3 27.3 %collective-permute-start.1 = (bf16[1024,896]{1,0:T(8,128)(2,1)}, bf16[1024,896]{1,0:T(8,128)(2,1)}, u32[]{:S(2)}, u32[]{:S(2)}) collective-permute-start(bf16[1024,896]{1,0:T(8,128)(2,1)} %bitcast.12), channel_id=1, source_target_pairs={{0,4},{4,0},{1,5},{5,1},{2,6},{6,2},{3,7},{7,3},{8,12},{12,8},{9,1... | collective-permute-start | bytes 5505032 | tf_op jit(solution)/shard_map/ppermute | solution.py:88
  62.0 0.8 copy-start.2
  62.7 27.5 %collective-permute-start.5 = (bf16[64,256]{1,0:T(8,128)(2,1)S(1)}, bf16[64,256]{1,0:T(8,128)(2,1)S(1)}, u32[]{:S(2)}, u32[]{:S(2)}) collective-permute-start(bf16[64,256]{1,0:T(8,128)(2,1)S(1)} %copy-done.2), channel_id=1, source_target_pairs={{0,4},{4,0},{1,5},{5,1},{2,6},{6,2},{3,7},{7,3},{8,12},{12,8},{9,1... | collective-permute-start | bytes 98312 | tf_op jit(solution)/shard_map/ppermute | solution.py:88
  76.3 13.2 %all-to-all-start.2 = ((bf16[4,224,256]{2,1,0:T(8,128)(2,1)}), bf16[4,224,256]{2,1,0:T(8,128)(2,1)S(1)}, u32[]{:S(2)}, u32[]{:S(2)}) async-start(bf16[4,224,256]{2,1,0:T(8,128)(2,1)} %copy.73), calls=%async_computation.2 | async-start | bytes 917504 | tf_op jit(solution)/shard_map/all_to_all | solution.py:212
  91.2 19.9 %all-to-all-start.3 = ((bf16[32,24,256]{2,1,0:T(8,128)(2,1)}), bf16[32,24,256]{2,1,0:T(8,128)(2,1)S(1)}, u32[]{:S(2)}, u32[]{:S(2)}) async-start(bf16[32,24,256]{2,1,0:T(8,128)(2,1)} %fusion.6), calls=%async_computation.3 | async-start | bytes 786432 | tf_op jit(solution)/shard_map/all_to_all | solution.py:236

commit v2 on v0

v2 whole, which is shorter than its diff:
```python
import functools

import jax
import jax.numpy as jnp
from jax import lax
from jax.experimental import pallas as pl
from jax.experimental.pallas import tpu as pltpu
from jax.sharding import Mesh
from jax.sharding import PartitionSpec as P

EP = ("ep_0", "ep_1", "ep_2")
FAR = ("ep_0", "ep_1")
EPSILON = 1e-06
F32, BF16 = jnp.float32, jnp.bfloat16
CAP = 2
LANES = 128
MIB = 1 << 20
ANY = pl.BlockSpec(memory_space=pl.ANY)
IN_VMEM = pl.BlockSpec(memory_space=pltpu.VMEM)
IN_SMEM = pl.BlockSpec(memory_space=pltpu.SMEM)
NT = (((1,), (1,)), ((), ()))


def at_hbm(x):
    return pltpu.with_memory_space_constraint(x, pltpu.HBM)


def at_vmem(x):
    return pltpu.with_memory_space_constraint(x, pltpu.VMEM)


def normal_rows(values, gain_row):
    mean_square = jnp.mean(values * values, axis=-1, keepdims=True)
    return values * lax.rsqrt(mean_square + EPSILON) * gain_row


def dot(a, b):
    return jnp.dot(a, b, preferred_element_type=F32)


def dot_nt(a, b):
    return lax.dot_general(a, b, NT, preferred_element_type=F32)


def rows_of(shape):
    return lax.broadcasted_iota(jnp.int32, shape, 0)


def lanes_of(shape):
    return lax.broadcasted_iota(jnp.int32, shape, 1)


def route_tables(ids, weights, taken_ref, place_ref):
    n_tp, n_core = lax.axis_size("tp"), lax.axis_size("ep_2")
    core_at, chip_at = lax.axis_index("ep_2"), lax.axis_index(FAR)
    rows, wide = taken_ref.shape[1:]
    batch = ids.shape[1]
    seqs = wide // n_tp
    cores = (core_at, 1 - core_at)
    ids = ids[...]

    lane = lanes_of((wide, batch))
    own = lane == (chip_at * n_core + core_at) * seqs + rows_of((wide, batch)) % seqs
    own = jnp.where(own, 1.0, 0.0).astype(BF16)
    padded = jnp.concatenate([ids.astype(F32), jnp.zeros((6, batch), F32)], axis=0).astype(BF16)
    own_ids = dot_nt(padded, own).astype(jnp.int32)
    row, lane = rows_of((rows, wide)), lanes_of((rows, wide))
    piece_fits = lane // seqs == row % n_tp
    slot = (row % (2 * n_tp)) // n_tp
    first, second = rows_of((wide, wide)), lanes_of((wide, wide))
    ahead = (first // seqs == second // seqs) & (first <= second)
    ahead = jnp.where(ahead, 1.0, 0.0).astype(BF16)
    for o in range(2):
        expert = (row // (2 * n_tp)) * n_core + cores[o]
        hit = (expert == own_ids[0:1, :]) | (expert == own_ids[1:2, :])
        rank = dot(jnp.where(hit, 1.0, 0.0).astype(BF16), ahead).astype(jnp.int32)
        taken = hit & (rank == slot + 1) & piece_fits
        taken_ref[o] = jnp.where(taken, 1.0, 0.0).astype(BF16)

    half = place_ref.shape[2] // 2
    lane = lanes_of((1, batch))
    in_plane = (lane // seqs) % n_core == core_at
    mine = lanes_of((seqs, batch)) % seqs == rows_of((seqs, batch))
    stacked = []
    for o in range(2):
        expert = chip_at * n_core + cores[o]
        hits = (ids == expert) & in_plane
        weight = jnp.sum(jnp.where(hits, weights[...], 0.0), axis=0, keepdims=True)
        high = weight.astype(BF16).astype(F32)
        hit = jnp.sum(jnp.where(hits, 1.0, 0.0), axis=0, keepdims=True)
        stacked += [jnp.where(mine, part, 0.0) for part in (hit, high, weight - high)]
    stacked = jnp.concatenate(stacked, axis=0).astype(BF16)
    group = lanes_of((half, batch)) // (seqs * n_core) == rows_of((half, batch)) // CAP
    table = dot_nt(stacked, jnp.where(group, 1.0, 0.0).astype(BF16))
    before = rows_of((seqs, seqs)) >= lanes_of((seqs, seqs))
    before = jnp.where(before, 1.0, 0.0).astype(BF16)
    slot = lanes_of((seqs, half)) % CAP + 1
    for o in range(2):
        hit, high, low = (table[(3 * o + i) * seqs : (3 * o + i + 1) * seqs] for i in range(3))
        rank = dot(before, hit.astype(BF16)).astype(jnp.int32)
        put = (hit > 0.5) & (rank == slot)
        place_ref[0, :, o * half : (o + 1) * half] = jnp.where(put, high, 0.0).astype(BF16)
        place_ref[1, :, o * half : (o + 1) * half] = jnp.where(put, low, 0.0).astype(BF16)


def attend_kernel(chunks, lens, forget_bias, *refs):
    sources, (out_ref, taken_ref, place_ref), rest = refs[:13], refs[13:16], refs[16:]
    held, (queries, keys, values, shift, scores, mixed, sems) = rest[:13], rest[13:]
    ids, weights, tok, gain, wq, wk, wv, wf, qg, kg, cum, wo, cache = held
    seqs, slots, pair = cache.shape
    head = qg.shape[1]
    group = wq.shape[1] // head
    copies = [pltpu.make_async_copy(sources[i], held[i], sems.at[i]) for i in range(12)]
    step = seqs // chunks
    parts = [
        pltpu.make_async_copy(
            sources[12].at[pl.ds(i * step, step)], cache.at[pl.ds(i * step, step)], sems.at[12 + i]
        )
        for i in range(chunks)
    ]
    for copy in copies[:11]:
        copy.start()
    for part in parts:
        part.start()
    copies[11].start()
    for copy in copies[:2]:
        copy.wait()
    route_tables(ids, weights, taken_ref, place_ref)
    for copy in copies[2:10]:
        copy.wait()

    normed = normal_rows(tok[...].astype(F32), gain[...]).astype(BF16)
    query_raw = dot(normed, wq[...])
    key_new = normal_rows(dot_nt(normed, wk[...]), kg[...]).astype(BF16).astype(F32)
    value_new = dot_nt(normed, wv[...]).astype(BF16).astype(F32)
    blank = jnp.zeros((seqs, pair - head), F32)
    key_new = jnp.concatenate([key_new, blank], axis=1)
    value_new = jnp.concatenate([blank, value_new], axis=1)
    for h in range(group):
        query = normal_rows(query_raw[:, h * head : (h + 1) * head], qg[...])
        query = jnp.concatenate([query.astype(BF16).astype(F32), blank], axis=1)
        queries[pl.ds(h, seqs, stride=group), :] = query
        keys[pl.ds(h, seqs, stride=group), :] = key_new
        values[pl.ds(h, seqs, stride=group), :] = value_new
    forget = jnp.sum(normed.astype(F32) * wf[...].astype(F32), axis=1, keepdims=True) + forget_bias[0]
    log_gate = jnp.minimum(forget, 0.0) - jnp.log1p(jnp.exp(-jnp.abs(forget)))

    row = rows_of((seqs, 1))
    length = jnp.zeros((seqs, 1), jnp.int32)
    for s in range(seqs):
        length = jnp.where(row == s, lens[s], length)
    copies[10].wait()
    position = lanes_of((seqs, slots))
    summed = cum[...].reshape(seqs, slots)
    last = jnp.sum(jnp.where(position == length - 1, summed, 0.0), axis=1, keepdims=True)
    shift[...] = jnp.where(position < length, (last + log_gate) - summed, -jnp.inf)

    multiplier = head ** (-0.5)
    own_score = jnp.sum(queries[...] * keys[...], axis=1, keepdims=True) * multiplier
    tall = 2 * group
    upper = rows_of((tall, 1)) < group
    for p in range(seqs // 2):
        if (2 * p) % step == 0:
            parts[2 * p // step].wait()
        query = queries[tall * p : tall * (p + 1), :].astype(BF16)
        score = jnp.where(upper, dot_nt(query, cache[2 * p]), dot_nt(query, cache[2 * p + 1]))
        moved = jnp.where(upper, shift[2 * p : 2 * p + 1, :], shift[2 * p + 1 : 2 * p + 2, :])
        scores[tall * p : tall * (p + 1), :] = score * multiplier + moved
    score = scores[...]
    peak = jnp.maximum(jnp.max(score, axis=1, keepdims=True), own_score)
    past = jnp.exp(score - peak)
    own = jnp.exp(own_score - peak)
    whole = 1.0 / (jnp.sum(past, axis=1, keepdims=True) + own)
    scores[...] = past * whole
    own_prob = (own * whole).astype(BF16).astype(F32)
    for p in range(seqs // 2):
        prob = scores[tall * p : tall * (p + 1), :].astype(BF16)
        mixed[tall * p : tall * (p + 1), :] = jnp.where(
            upper, dot(prob, cache[2 * p]), dot(prob, cache[2 * p + 1])
        )
    mixed[...] = mixed[...] + own_prob * values[...]
    copies[11].wait()
    total = jnp.zeros((seqs, wo.shape[1]), F32)
    for h in range(group):
        mix = mixed[pl.ds(h, seqs, stride=group), :][:, pair - head :].astype(BF16)
        total = total + dot(mix, wo[h * head : (h + 1) * head, :])
    partial = total.astype(BF16)
    for t in range(out_ref.shape[0]):
        out_ref[t] = partial


def attend(n_tp, chips, lens, forget_bias, *arrays):
    chunks = 6
    tok, wq, qg, cache = arrays[2], arrays[4], arrays[8], arrays[12]
    seqs, slots, pair = cache.shape
    heads = wq.shape[1] // qg.shape[1]
    rows = seqs * heads
    scratch = [pltpu.VMEM(a.shape, a.dtype) for a in arrays]
    scratch += [pltpu.VMEM((rows, pair), F32)] * 3
    scratch += [pltpu.VMEM((seqs, slots), F32), pltpu.VMEM((rows, slots), F32), pltpu.VMEM((rows, pair), F32)]
    scratch += [pltpu.SemaphoreType.DMA((12 + chunks,))]
    return pl.pallas_call(
        functools.partial(attend_kernel, chunks),
        name="attend",
        out_shape=(
            pltpu.VMEM((n_tp, *tok.shape), BF16),
            pltpu.VMEM((2, chips * 2 * n_tp, n_tp * seqs), BF16),
            pltpu.VMEM((2, seqs, chips * 2 * CAP), BF16),
        ),
        in_specs=[IN_SMEM, IN_SMEM] + [ANY] * 13,
        out_specs=(IN_VMEM,) * 3,
        scratch_shapes=scratch,
        compiler_params=pltpu.CompilerParams(vmem_limit_bytes=16 * MIB),
    )(lens, forget_bias, *[at_hbm(a) for a in arrays])


def send_kernel(crossed, tok, gain, taken_ref, *refs):
    message, own_residual = refs[-2:]
    n_tp = crossed.shape[0]
    seqs, width = tok.shape
    rows = message.shape[0]
    span = width // n_tp
    share = seqs // n_tp
    tp_at = lax.axis_index("tp")
    attn_out = crossed[0].astype(F32)
    for t in range(1, n_tp):
        attn_out = attn_out + crossed[t].astype(F32)
    residual = (tok[...].astype(F32) + attn_out).astype(BF16)
    residual_f = residual.astype(F32)
    kept = residual[:, :span]
    for t in range(1, n_tp):
        kept = jnp.where(tp_at == t, residual[:, t * span : (t + 1) * span], kept)
    own_residual[...] = kept
    normed = normal_rows(residual_f, gain[...])
    pieces = jnp.concatenate([normed[:, q * span : (q + 1) * span] for q in range(n_tp)], axis=0)
    pieces = pieces.astype(BF16)
    wide = n_tp * seqs
    for o in range(2):
        message[:, o * span : (o + 1) * span] = dot(taken_ref[o], pieces).astype(BF16)
    each = 2 * n_tp
    row, lane = rows_of((each, wide)), lanes_of((each, wide))
    for two in range(share // 2):
        token = tp_at * share + two * 2 + row // n_tp
        taken = (lane // seqs == row % n_tp) & (lane % seqs == token)
        block = dot(jnp.where(taken, 1.0, 0.0).astype(BF16), pieces).astype(BF16)
        block = jnp.broadcast_to(block[None], (rows // each, each, span)).reshape(rows, span)
        message[:, (2 + two) * span : (3 + two) * span] = block


def send(crossed, tok, gain, taken, chips, swapped):
    n_tp, seqs, width = crossed.shape
    span = width // n_tp
    rows = chips * 2 * n_tp
    return pl.pallas_call(
        send_kernel,
        name="send",
        out_shape=(
            pltpu.VMEM((rows, (2 + seqs // n_tp // 2) * span), BF16),
            pltpu.VMEM((seqs, span), BF16),
        ),
        in_specs=[IN_VMEM] * 4 + [ANY] * len(swapped),
        out_specs=(IN_VMEM, IN_VMEM),
        compiler_params=pltpu.CompilerParams(vmem_limit_bytes=8 * MIB),
    )(at_vmem(crossed), tok, gain, at_vmem(taken), *[at_hbm(w) for w in swapped])


def experts_kernel(n_tp, arrived, shared, *refs):
    weights, out_ref, spread, held, sems = refs[:10], refs[10], refs[11], refs[12:-1], refs[-1]
    matrices, (dense_gate, dense_up) = held[:6], held[6:]
    units = weights[6].shape[0]
    into = (dense_gate.at[:units], dense_gate.at[units:], dense_up.at[:units], dense_up.at[units:])
    into = matrices + into
    copies = [pltpu.make_async_copy(weights[i], into[i], sems.at[i]) for i in range(10)]
    for copy in copies[6:] + copies[:6]:
        copy.start()
    rows, span = arrived.shape[0], out_ref.shape[2]
    each = 2 * n_tp
    chips = rows // each
    for j in range(spread.shape[0]):
        spread[j] = arrived[:, j * LANES : (j + 1) * LANES].astype(F32)

    def gathered(start, stride, count, column):
        return jnp.concatenate(
            [
                spread[column // LANES + j, pl.ds(start + q, count, stride=stride), :]
                for q in range(n_tp)
                for j in range(span // LANES)
            ],
            axis=1,
        )

    blocks = []
    for two in range(arrived.shape[1] // span - 2):
        for k in range(2):
            blocks.append(gathered(k * n_tp, each, chips, (2 + two) * span))
    tokens = jnp.concatenate(blocks, axis=0).astype(BF16)
    gate_row = shared[...].astype(F32)
    gate_row = jnp.concatenate([gate_row[i : i + 1] for i in range(gate_row.shape[0])], axis=1)
    gate_rows = jnp.broadcast_to(gate_row, (8, gate_row.shape[1])).astype(BF16)
    mix_gate = dot_nt(tokens, gate_rows)[:, :1]
    mix_gate = 1.0 / (1.0 + jnp.exp(-mix_gate))
    for copy in copies[6:]:
        copy.wait()
    gate = dot_nt(tokens, dense_gate[...])
    up = dot_nt(tokens, dense_up[...])
    hidden = (mix_gate * (gate / (1.0 + jnp.exp(-gate)) * up)).astype(BF16)
    half = hidden.shape[0] // 2
    taken = chips * 2 * CAP
    for t in range(n_tp):
        out_ref[t, taken:, : span // 2] = hidden[:half]
        out_ref[t, taken:, span // 2 :] = hidden[half:]
    for o in range(2):
        tokens = gathered(0, n_tp, chips * CAP, o * span).astype(BF16)
        gate_w, up_w, down_w = matrices[3 * o : 3 * o + 3]
        copies[3 * o].wait()
        gate = dot(tokens, gate_w[...])
        copies[3 * o + 1].wait()
        up = dot(tokens, up_w[...])
        hidden = (gate / (1.0 + jnp.exp(-gate)) * up).astype(BF16)
        copies[3 * o + 2].wait()
        part = dot(hidden, down_w[...]).astype(BF16)
        for t in range(n_tp):
            out_ref[t, o * chips * CAP : (o + 1) * chips * CAP, :] = part[:, t * span : (t + 1) * span]


def experts(n_tp, span, arrived, shared, matrices, dense):
    rows = arrived.shape[0]
    chips = rows // (2 * n_tp)
    many = (arrived.shape[1] // span - 2) * 2 * chips
    units, width = dense[0].shape
    return pl.pallas_call(
        functools.partial(experts_kernel, n_tp),
        name="experts",
        out_shape=pltpu.VMEM((n_tp, chips * 2 * CAP + many // 2, span), BF16),
        in_specs=[IN_VMEM] * 2 + [ANY] * 10,
        out_specs=IN_VMEM,
        scratch_shapes=[pltpu.VMEM((arrived.shape[1] // LANES, rows, LANES), F32)]
        + [pltpu.VMEM(w.shape, w.dtype) for w in matrices]
        + [pltpu.VMEM((2 * units, width), BF16)] * 2
        + [pltpu.SemaphoreType.DMA((10,))],
        compiler_params=pltpu.CompilerParams(vmem_limit_bytes=24 * MIB),
    )(at_vmem(arrived), shared, *[at_hbm(w) for w in matrices], *[at_hbm(w) for w in dense])


def combine_kernel(crossed, place, down_own, down_other, out_ref, dense):
    n_tp, _, span = crossed.shape
    chips, seqs, _ = out_ref.shape
    taken = chips * 2 * CAP
    share = seqs // n_tp
    total = crossed[0, :taken].astype(F32)
    for t in range(1, n_tp):
        total = total + crossed[t, :taken].astype(F32)
    total = total.astype(BF16)
    down = jnp.concatenate([down_own[...], down_other[...]], axis=0)
    for t in range(n_tp):
        both = crossed[t, taken:]
        hidden = jnp.concatenate([both[:, : span // 2], both[:, span // 2 :]], axis=0)
        part = dot(hidden, down)
        for c in range(share):
            for j in range(dense.shape[0]):
                dense[j, pl.ds(t * share + c, chips, stride=seqs), :] = part[
                    c * chips : (c + 1) * chips, j * LANES : (j + 1) * LANES
                ]
    lane = lanes_of((seqs, taken))
    owner = (lane % (chips * CAP)) // CAP
    spread = jnp.zeros((chips * seqs, span), F32)
    for i in range(2):
        weight = place[i].astype(F32)
        weight = jnp.concatenate([jnp.where(owner == s, weight, 0.0) for s in range(chips)], axis=0)
        spread = spread + dot(weight.astype(BF16), total)
    for j in range(dense.shape[0]):
        column = spread[:, j * LANES : (j + 1) * LANES]
        out_ref[:, :, j * LANES : (j + 1) * LANES] = (dense[j] + column).astype(BF16).reshape(chips, seqs, LANES)


def combine(crossed, place, down_own, down_other, chips, seqs):
    span = crossed.shape[2]
    return pl.pallas_call(
        combine_kernel,
        name="combine",
        out_shape=pltpu.VMEM((chips, seqs, span), BF16),
        in_specs=[IN_VMEM] * 4,
        out_specs=IN_VMEM,
        scratch_shapes=[pltpu.VMEM((span // LANES, chips * seqs, LANES), F32)],
        compiler_params=pltpu.CompilerParams(vmem_limit_bytes=8 * MIB),
    )(at_vmem(crossed), at_vmem(place), at_vmem(down_own), at_vmem(down_other))


def shards(
    tokens,
    attn_gain,
    w_query,
    w_key,
    w_value,
    w_forget,
    forget_bias,
    query_gain,
    key_gain,
    cache_pairs,
    cache_cum,
    lengths,
    w_output,
    ffn_gain,
    expert_ids,
    route_weight,
    w_exp_gate,
    w_exp_up,
    w_exp_down,
    shared_gate,
    w_dense_gate,
    w_dense_up,
    w_dense_down,
):
    seqs, width = tokens.shape
    n_tp, chips = lax.axis_size("tp"), lax.axis_size(FAR)
    span = width // n_tp

    def other(w):
        return lax.ppermute(w, "ep_2", [(0, 1), (1, 0)])

    matrices = [w_exp_gate[0], w_exp_up[0], w_exp_down[0]]
    matrices = matrices + [other(w) for w in matrices]
    dense = [w_dense_gate, other(w_dense_gate), w_dense_up, other(w_dense_up)]
    down_other = other(w_dense_down)

    partial, taken, place = attend(
        n_tp,
        chips,
        lengths,
        forget_bias,
        expert_ids.T,
        route_weight.T,
        tokens,
        attn_gain[None],
        w_query,
        w_key.T,
        w_value.T,
        w_forget.T,
        query_gain[None],
        key_gain[None],
        cache_cum,
        w_output,
        cache_pairs[:, 0],
    )
    crossed = lax.all_to_all(partial, "tp", 0, 0, tiled=True)
    message, own_residual = send(
        crossed, tokens, ffn_gain[None], taken, chips, [*matrices[3:], dense[1], dense[3], down_other]
    )
    arrived = lax.all_to_all(message.reshape(chips, -1, message.shape[1]), FAR, 0, 0, tiled=True)
    blocks = experts(n_tp, span, arrived.reshape(message.shape), shared_gate.reshape(-1, LANES), matrices, dense)
    crossed = lax.all_to_all(blocks, "tp", 0, 0, tiled=True)
    total = combine(crossed, place, w_dense_down, down_other, chips, seqs)
    summed = lax.all_to_all(total, FAR, 0, 0, tiled=True).astype(F32).sum(axis=0)
    return (own_residual.astype(F32) + summed).astype(BF16)


def solution(mesh):
    split = Mesh(mesh.devices.reshape(8, 4, 2, mesh.shape["tp"]), ("ep_0", "ep_1", "ep_2", "tp"))
    return jax.shard_map(
        shards,
        mesh=split,
        in_specs=(
            P(EP, None),
            P(),
            P(None, "tp"),
            P(None, "tp"),
            P(None, "tp"),
            P(None, "tp"),
            P("tp"),
            P(),
            P(),
            P(EP, "tp", None, None),
            P(EP, "tp", None),
            P(EP),
            P("tp", None),
            P(),
            P(),
            P(),
            P(EP, None, "tp"),
            P(EP, None, "tp"),
            P(EP, "tp", None),
            P(),
            P(EP, None),
            P(EP, None),
            P(EP, "tp"),
        ),
        out_specs=P(EP, "tp"),
        check_vma=False,
    )
```

time: 140 us -> 86.8 us (0.62)
  waiting for transfers between devices: 50.1 us -> 5.73 us
  blocking collectives: 21 us -> 58.3 us
  matrix products: 25.6 us -> 0 us
  starting transfers between devices: 21.3 us -> 5.89 us
  Pallas kernels: 0 us -> 13.2 us
  other arithmetic: 12.5 us -> 0.68 us
  local copies, waits for them, and re-layouts: 7.02 us -> 1.91 us
    all_to_all x3 -> x1, waiting for transfers between devices: 50.1 us -> 4.74 us  [shards(): crossed = lax.all_to_all(partial, 'tp', 0, 0, tiled=True)]
    all_to_all x3, blocking collectives: 21 us -> 58.3 us  [the longest x1 29.7 us: shards(): lax.all_to_all(message.reshape(chips, -1, message.shape[1]), FAR, 0, 0, t...]
    dot_general x15 -> x0, matrix products: 25.6 us -> none  [the longest x1 4.76 us: shards(): jnp.einsum('bkgd,bkld->bkgl', query_rows, cached_keys, preferred_element_...]
    all_to_all x3 -> x1, starting transfers between devices: 21.3 us -> 4.3 us  [shards(): crossed = lax.all_to_all(partial, 'tp', 0, 0, tiled=True)]
    pallas_call x0 -> x4, Pallas kernels: none -> 13.2 us  [the longest x1 7.24 us: attend(): pl.pallas_call(functools.partial(attend_kernel, chunks), name='attend', o...]
    reduce_sum x11 -> x1, other arithmetic: 5.17 us -> 0.07 us  [shards(): lax.all_to_all(total, FAR, 0, 0, tiled=True).astype(F32).sum(axis=0)]
    another operation x2 -> x0, local copies, waits for them, and re-layouts: 1.87 us -> none  [the longest x1 1.18 us: in_blocks(): x.reshape(*shape[:dim], count, shape[dim] // count, *shape[dim + 1:])]
    sub x2 -> x0, other arithmetic: 1.83 us -> none  [the longest x1 1.03 us: shards(): past_score = past_score + (now_cum[:, :, None] - cache_cum)[:, :, None, :]]
  transfers between devices with their start and end apart: 3 -> 7, of which waited for: 3 -> 3; matrix products, arithmetic and copies ran while one was open for 7% -> 0% of each run, Pallas kernels for 0% -> 8%
where the time goes in v2:
time: 86.8 us; the launch traced here: 86.5 us
  blocking collectives  58.3 us (67%)
  Pallas kernels  13.2 us (15%)
  starting transfers between devices  5.89 us (7%)
  waiting for transfers between devices  5.73 us (7%)
  local copies, waits for them, and re-layouts  1.91 us (2%)
    all_to_all x1, blocking collectives, shards(): lax.all_to_all(message.reshape(chips, -1, message.shape[1]), FAR, 0, 0, t...  29.7 us
    all_to_all x1, blocking collectives, shards(): lax.all_to_all(total, FAR, 0, 0, tiled=True).astype(F32).sum(axis=0)  18.5 us
    all_to_all x1, blocking collectives, shards(): crossed = lax.all_to_all(blocks, 'tp', 0, 0, tiled=True)  10.1 us
    pallas_call x1, Pallas kernels, attend(): pl.pallas_call(functools.partial(attend_kernel, chunks), name='attend', o...  7.24 us
    pallas_call x1, Pallas kernels, experts(): pl.pallas_call(functools.partial(experts_kernel, n_tp), name='experts', o...  5.12 us
    all_to_all x1, waiting for transfers between devices, shards(): crossed = lax.all_to_all(partial, 'tp', 0, 0, tiled=True)  4.74 us
    all_to_all x1, starting transfers between devices, shards(): crossed = lax.all_to_all(partial, 'tp', 0, 0, tiled=True)  4.3 us
    unnamed x24, local copies, waits for them, and re-layouts  1.91 us
  transfers between devices with their start and end apart: 7, of which 3 were waited for; matrix products, arithmetic and copies ran while one was open for 0% of the time, Pallas kernels for 8%

profile of v2, /device:TPU:32, one launch (start us, length us, event | category | flops | bytes accessed | tf_op | source)
XLA Modules:
  0.0 86.5 jit_solution(6683190945131058886)
XLA Ops:
  0.0 0.0 collective-permute-start
  0.0 0.5 collective-permute-start.1
  0.5 0.0 collective-permute-start.2
  0.5 0.5 collective-permute-start.5
  1.7 0.6 copy-done.6
  2.3 7.2 %attend.1 = (bf16[4,24,1024]{2,1,0:T(8,128)(2,1)}, bf16[2,256,96]{2,1,0:T(8,128)(2,1)S(1)}, bf16[2,24,128]{2,1,0:T(8,128)(2,1)S(1)}) custom-call(s32[24]{0:T(128)S(1)} %copy-done.6, f32[1]{0:T(128)S(6)} %copy.24.forget_bias, s32[2,1536]{1,0:T(2,128)} %bitcast.29, f32[2,1536]{1,0:T(2,128)} %bitcast.30, bf16[24,1024]{1,0:T(8,128)(2,1)} %tok.1, ...), custom_call_target="tpu_custom_call" | custom-call | tf_op jit(solution)/shard_map/attend/pallas_call | solution.py:202
  9.6 4.3 %all-to-all-start = ((bf16[4,24,1024]{2,1,0:T(8,128)(2,1)}), bf16[4,24,1024]{2,1,0:T(8,128)(2,1)S(1)}, u32[]{:S(2)}, u32[]{:S(2)}) async-start(bf16[4,24,1024]{2,1,0:T(8,128)(2,1)} %get-tuple-element.10), calls=%async_computation | async-start | bytes 393216 | tf_op jit(solution)/shard_map/all_to_all | solution.py:445
  13.9 0.0 collective-permute-start.3
  13.9 0.0 collective-permute-done.5.refs_5_.down_other
  13.9 0.6 collective-permute-start.4
  14.5 0.7 collective-permute-done.3.refs_3_.refs_7_
  15.2 0.2 collective-permute-done.4.refs_4_.refs_9_
  15.5 4.7 %all-to-all-done.crossed = bf16[4,24,1024]{2,1,0:T(8,128)(2,1)S(1)} async-done(((bf16[4,24,1024]{2,1,0:T(8,128)(2,1)}), bf16[4,24,1024]{2,1,0:T(8,128)(2,1)S(1)}, u32[]{:S(2)}, u32[]{:S(2)}) %all-to-all-start) | async-done | bytes 196640 | tf_op jit(solution)/shard_map/all_to_all | solution.py:445
  20.2 0.0 collective-permute-done.refs_0_.refs_3_
  20.2 0.0 collective-permute-done.2.refs_2_.refs_5_
  20.3 1.2 %copy-done.7 = bf16[1024,896]{1,0:T(8,128)(2,1)} copy-done((bf16[1024,896]{1,0:T(8,128)(2,1)}, bf16[1024,896]{1,0:T(8,128)(2,1)S(1)}, u32[]{:S(2)}) %copy-start.7) | copy-done | bytes 1835032
  21.5 0.4 send.1
  21.9 29.7 %all_to_all.20 = bf16[32,8,1280]{2,1,0:T(8,128)(2,1)S(1)} all-to-all(bf16[32,8,1280]{2,1,0:T(8,128)(2,1)S(1)} %bitcast.17), channel_id=1, replica_groups=mesh['ep_0'=8,'ep_1'=4,'ep_2'=2,'tp'=4] {'ep_0','ep_1'}, dimensions={0} | all-to-all | bytes 1310720 | tf_op jit(solution)/shard_map/all_to_all | solution.py:449
  51.6 5.1 %experts.1 = bf16[4,224,256]{2,1,0:T(8,128)(2,1)S(1)} custom-call(bf16[256,1280]{1,0:T(8,128)(2,1)S(1)} %bitcast.16, bf16[8,128]{1,0:T(8,128)(2,1)S(1)} %bitcast.19, bf16[1024,896]{1,0:T(8,128)(2,1)} %bitcast.22, bf16[1024,896]{1,0:T(8,128)(2,1)} %bitcast.24, bf16[896,1024]{1,0:T(8,128)(2,1)} %bitcast.26, bf16[1024,896]{1,0:T(8,128)(2,1)} %copy-done.7, ...), custom_call_target="tpu_custom_call" | custom-call | tf_op jit(solution)/shard_map/experts/pallas_call | solution.py:331
  56.7 10.1 %all_to_all.21.crossed = bf16[4,224,256]{2,1,0:T(8,128)(2,1)S(1)} all-to-all(bf16[4,224,256]{2,1,0:T(8,128)(2,1)S(1)} %experts.1), channel_id=1, replica_groups=mesh['ep_0'=8,'ep_1'=4,'ep_2'=2,'tp'=4] {'tp'}, dimensions={0} | all-to-all | bytes 917504 | tf_op jit(solution)/shard_map/all_to_all | solution.py:451
  66.9 0.5 combine.1
  67.3 18.5 %all_to_all.22 = bf16[32,24,256]{2,1,0:T(8,128)(2,1)S(1)} all-to-all(bf16[32,24,256]{2,1,0:T(8,128)(2,1)S(1)} %combine.1), channel_id=1, replica_groups=mesh['ep_0'=8,'ep_1'=4,'ep_2'=2,'tp'=4] {'ep_0','ep_1'}, dimensions={0} | all-to-all | bytes 786432 | tf_op jit(solution)/shard_map/all_to_all | solution.py:453
  85.8 0.1 convert_reduce_fusion
  85.9 0.6 add_convert_fusion
  (23 shorter events, 0.0 us)
Async XLA Ops:
  0.0 20.2 %collective-permute-start = (bf16[1024,896]{1,0:T(8,128)(2,1)}, bf16[1024,896]{1,0:T(8,128)(2,1)S(1)}, u32[]{:S(2)}, u32[]{:S(2)}) collective-permute-start(bf16[1024,896]{1,0:T(8,128)(2,1)} %bitcast.21), channel_id=1, source_target_pairs={{0,4},{4,0},{1,5},{5,1},{2,6},{6,2},{3,7},{7,3},{8,12},{12,8},{9,1... | collective-permute-start | bytes 5505032 | tf_op jit(solution)/shard_map/ppermute | solution.py:419
  0.0 20.2 %collective-permute-start.1 = (bf16[1024,896]{1,0:T(8,128)(2,1)}, bf16[1024,896]{1,0:T(8,128)(2,1)}, u32[]{:S(2)}, u32[]{:S(2)}) collective-permute-start(bf16[1024,896]{1,0:T(8,128)(2,1)} %bitcast.23), channel_id=1, source_target_pairs={{0,4},{4,0},{1,5},{5,1},{2,6},{6,2},{3,7},{7,3},{8,12},{12,8},{9,1... | collective-permute-start | bytes 5505032 | tf_op jit(solution)/shard_map/ppermute | solution.py:419
  0.5 19.7 %collective-permute-start.2 = (bf16[896,1024]{1,0:T(8,128)(2,1)}, bf16[896,1024]{1,0:T(8,128)(2,1)}, u32[]{:S(2)}, u32[]{:S(2)}) collective-permute-start(bf16[896,1024]{1,0:T(8,128)(2,1)} %bitcast.25), channel_id=1, source_target_pairs={{0,4},{4,0},{1,5},{5,1},{2,6},{6,2},{3,7},{7,3},{8,12},{12,8},{9,1... | collective-permute-start | bytes 5505032 | tf_op jit(solution)/shard_map/ppermute | solution.py:419
  0.5 13.4 %collective-permute-start.5 = (bf16[64,256]{1,0:T(8,128)(2,1)}, bf16[64,256]{1,0:T(8,128)(2,1)S(1)}, u32[]{:S(2)}, u32[]{:S(2)}) collective-permute-start(bf16[64,256]{1,0:T(8,128)(2,1)} %down_own.1), channel_id=1, source_target_pairs={{0,4},{4,0},{1,5},{5,1},{2,6},{6,2},{3,7},{7,3},{8,12},{12,8},{9,1... | collective-permute-start | bytes 98312 | tf_op jit(solution)/shard_map/ppermute | solution.py:419
  1.7 0.7 copy-start.6
  2.3 11.6 %copy-start.10 = (bf16[64,1024]{1,0:T(8,128)(2,1)S(1)}, bf16[64,1024]{1,0:T(8,128)(2,1)}, u32[]{:S(2)}) copy-start(bf16[64,1024]{1,0:T(8,128)(2,1)} %refs_6_.1) | copy-start | bytes 393220
  2.3 11.6 %copy-start.11 = (bf16[64,1024]{1,0:T(8,128)(2,1)S(1)}, bf16[64,1024]{1,0:T(8,128)(2,1)}, u32[]{:S(2)}) copy-start(bf16[64,1024]{1,0:T(8,128)(2,1)} %refs_8_.1) | copy-start | bytes 393220
  2.3 19.2 %copy-start = (bf16[24,1024]{1,0:T(8,128)(2,1)S(1)}, bf16[24,1024]{1,0:T(8,128)(2,1)}, u32[]{:S(2)}) copy-start(bf16[24,1024]{1,0:T(8,128)(2,1)} %tok.1) | copy-start | bytes 147460
  2.3 19.2 %copy-start.4 = (f32[1024]{0:T(1024)S(1)}, f32[1024]{0:T(1024)}, u32[]{:S(2)}) copy-start(f32[1024]{0:T(1024)} %param.36) | copy-start | bytes 12292
  9.6 10.6 %all-to-all-start = ((bf16[4,24,1024]{2,1,0:T(8,128)(2,1)}), bf16[4,24,1024]{2,1,0:T(8,128)(2,1)S(1)}, u32[]{:S(2)}, u32[]{:S(2)}) async-start(bf16[4,24,1024]{2,1,0:T(8,128)(2,1)} %get-tuple-element.10), calls=%async_computation | async-start | bytes 393216 | tf_op jit(solution)/shard_map/all_to_all | solution.py:445
  13.9 1.3 %collective-permute-start.3 = (bf16[64,1024]{1,0:T(8,128)(2,1)S(1)}, bf16[64,1024]{1,0:T(8,128)(2,1)S(1)}, u32[]{:S(2)}, u32[]{:S(2)}) collective-permute-start(bf16[64,1024]{1,0:T(8,128)(2,1)S(1)} %copy-done.10), channel_id=1, source_target_pairs={{0,4},{4,0},{1,5},{5,1},{2,6},{6,2},{3,7},{7,3},{8,12},{12,8},{9,1... | collective-permute-start | bytes 393224 | tf_op jit(solution)/shard_map/ppermute | solution.py:419
  13.9 6.3 %copy-start.1 = (bf16[64,256]{1,0:T(8,128)(2,1)}, bf16[64,256]{1,0:T(8,128)(2,1)S(1)}, u32[]{:S(2)}) copy-start(bf16[64,256]{1,0:T(8,128)(2,1)S(1)} %collective-permute-done.5.refs_5_.down_other) | copy-start | bytes 98308
  13.9 1.6 %collective-permute-start.4 = (bf16[64,1024]{1,0:T(8,128)(2,1)S(1)}, bf16[64,1024]{1,0:T(8,128)(2,1)S(1)}, u32[]{:S(2)}, u32[]{:S(2)}) collective-permute-start(bf16[64,1024]{1,0:T(8,128)(2,1)S(1)} %copy-done.11), channel_id=1, source_target_pairs={{0,4},{4,0},{1,5},{5,1},{2,6},{6,2},{3,7},{7,3},{8,12},{12,8},{9,1... | collective-permute-start | bytes 393224 | tf_op jit(solution)/shard_map/ppermute | solution.py:419
  15.2 5.0 %copy-start.8 = (bf16[64,1024]{1,0:T(8,128)(2,1)}, bf16[64,1024]{1,0:T(8,128)(2,1)S(1)}, u32[]{:S(2)}) copy-start(bf16[64,1024]{1,0:T(8,128)(2,1)S(1)} %collective-permute-done.3.refs_3_.refs_7_) | copy-start | bytes 393220
  15.5 4.8 %copy-start.9 = (bf16[64,1024]{1,0:T(8,128)(2,1)}, bf16[64,1024]{1,0:T(8,128)(2,1)S(1)}, u32[]{:S(2)}) copy-start(bf16[64,1024]{1,0:T(8,128)(2,1)S(1)} %collective-permute-done.4.refs_4_.refs_9_) | copy-start | bytes 393220
  20.2 1.3 %copy-start.7 = (bf16[1024,896]{1,0:T(8,128)(2,1)}, bf16[1024,896]{1,0:T(8,128)(2,1)S(1)}, u32[]{:S(2)}) copy-start(bf16[1024,896]{1,0:T(8,128)(2,1)S(1)} %collective-permute-done.refs_0_.refs_3_) | copy-start | bytes 5505028
  21.5 30.1 %copy-start.5 = (bf16[1024]{0:T(1024)(128)(2,1)S(1)}, bf16[1024]{0:T(1024)(128)(2,1)}, u32[]{:S(2)}) copy-start(bf16[1024]{0:T(1024)(128)(2,1)} %param.42) | copy-start | bytes 6148
  51.6 15.2 %copy-start.2 = (bf16[64,256]{1,0:T(8,128)(2,1)S(1)}, bf16[64,256]{1,0:T(8,128)(2,1)}, u32[]{:S(2)}) copy-start(bf16[64,256]{1,0:T(8,128)(2,1)} %copy-done.1) | copy-start | bytes 98308
  51.6 15.2 %copy-start.3 = (bf16[64,256]{1,0:T(8,128)(2,1)S(1)}, bf16[64,256]{1,0:T(8,128)(2,1)}, u32[]{:S(2)}) copy-start(bf16[64,256]{1,0:T(8,128)(2,1)} %down_own.1) | copy-start | bytes 98308

commit v3 on v2

v3 whole, which is shorter than its diff:
```python
import functools

import jax
import jax.numpy as jnp
from jax import lax
from jax.experimental import pallas as pl
from jax.experimental.pallas import tpu as pltpu
from jax.sharding import Mesh
from jax.sharding import PartitionSpec as P


EP = ("ep_0", "ep_1", "ep_2")
FAR = ("ep_0", "ep_1")
EPSILON = 1e-06
F32, BF16 = jnp.float32, jnp.bfloat16
CAP = 2
LANES = 128
MIB = 1 << 20
ANY = pl.BlockSpec(memory_space=pl.ANY)
IN_VMEM = pl.BlockSpec(memory_space=pltpu.VMEM)
IN_SMEM = pl.BlockSpec(memory_space=pltpu.SMEM)
NT = (((1,), (1,)), ((), ()))


def at_hbm(x):
    return pltpu.with_memory_space_constraint(x, pltpu.HBM)


def at_vmem(x):
    return pltpu.with_memory_space_constraint(x, pltpu.VMEM)


def normal_rows(values, gain_row):
    mean_square = jnp.mean(values * values, axis=-1, keepdims=True)
    return values * lax.rsqrt(mean_square + EPSILON) * gain_row


def dot(a, b):
    return jnp.dot(a, b, preferred_element_type=F32)


def dot_nt(a, b):
    return lax.dot_general(a, b, NT, preferred_element_type=F32)


def rows_of(shape):
    return lax.broadcasted_iota(jnp.int32, shape, 0)


def lanes_of(shape):
    return lax.broadcasted_iota(jnp.int32, shape, 1)


def route_tables(ids, weights, taken_ref, place_ref):
    n_tp, n_core = lax.axis_size("tp"), lax.axis_size("ep_2")
    core_at, chip_at = lax.axis_index("ep_2"), lax.axis_index(FAR)
    rows, wide = taken_ref.shape[1:]
    batch = ids.shape[1]
    seqs = wide // n_tp
    each = 2 * n_tp
    cores = (core_at, 1 - core_at)
    base = (chip_at * n_core + core_at) * seqs
    ids, weights = ids[...].astype(F32), weights[...]

    own = lanes_of((wide, batch)) == base + rows_of((wide, batch)) % seqs
    padded = jnp.concatenate([ids, jnp.zeros((6, batch), F32)], axis=0).astype(BF16)
    own_ids = dot_nt(padded, jnp.where(own, 1.0, 0.0).astype(BF16)).astype(jnp.int32)
    row, lane = rows_of((rows, wide)), lanes_of((rows, wide))
    piece_fits = lane // seqs == row % n_tp
    slot = (row % each) // n_tp
    first, second = rows_of((wide, wide)), lanes_of((wide, wide))
    ahead = (first // seqs == second // seqs) & (first <= second)
    ahead = jnp.where(ahead, 1.0, 0.0).astype(BF16)
    for o in range(2):
        expert = (row // each) * n_core + cores[o]
        hit = (expert == own_ids[0:1, :]) | (expert == own_ids[1:2, :])
        rank = dot(jnp.where(hit, 1.0, 0.0).astype(BF16), ahead).astype(jnp.int32)
        taken = hit & (rank == slot + 1) & piece_fits
        taken_ref[o] = jnp.where(taken, 1.0, 0.0).astype(BF16)

    mine = lanes_of((seqs, batch)) == base + rows_of((seqs, batch))

    def column(values):
        return jnp.sum(jnp.where(mine, values, 0.0), axis=1, keepdims=True)

    lane = lanes_of((seqs, rows))
    slot = lane % each - 2 * CAP
    expert = (lane // each) * n_core + jnp.where(slot < CAP, cores[0], cores[1])
    weight = jnp.zeros((seqs, rows), F32)
    hit = jnp.zeros((seqs, rows), F32)
    for i in range(ids.shape[0]):
        fits = column(ids[i : i + 1]).astype(jnp.int32) == expert
        weight = jnp.where(fits, column(weights[i : i + 1]), weight)
        hit = jnp.where(fits, 1.0, hit)
    before = rows_of((seqs, seqs)) >= lanes_of((seqs, seqs))
    rank = dot(jnp.where(before, 1.0, 0.0).astype(BF16), hit.astype(BF16)).astype(jnp.int32)
    put = (slot >= 0) & (hit > 0.5) & (rank == slot % CAP + 1)
    weight = jnp.where(put, weight, 0.0)
    high = weight.astype(BF16).astype(F32)

    token, place_at = rows_of((seqs, rows)), lane % each
    share = seqs // n_tp
    part = share // 2

    def fits(index):
        return token == (index // part) * share + ((lane // each) % 2) * part + index % part

    first = jnp.where(fits(place_at), 1.0, 0.0)
    second = jnp.where((place_at < 2 * CAP) & fits(place_at + each), 1.0, 0.0)
    for i, table in enumerate((first, second + high, weight - high)):
        place_ref[i] = table.astype(BF16)


def prepare_kernel(ids_hbm, weights_hbm, *refs):
    dense, (taken_ref, place_ref, packed, ids, weights, sems) = refs[:3], refs[3:]
    copies = [
        pltpu.make_async_copy(ids_hbm, ids, sems.at[0]),
        pltpu.make_async_copy(weights_hbm, weights, sems.at[1]),
    ]
    at = 0
    for i, source in enumerate(dense):
        into = packed.at[:, at : at + source.shape[1]]
        copies.append(pltpu.make_async_copy(source, into, sems.at[2 + i]))
        at += source.shape[1]
    for copy in copies:
        copy.start()
    for copy in copies[:2]:
        copy.wait()
    route_tables(ids, weights, taken_ref, place_ref)
    for copy in copies[2:]:
        copy.wait()


def prepare(n_tp, chips, seqs, ids, weights, dense):
    return pl.pallas_call(
        prepare_kernel,
        name="prepare",
        out_shape=(
            pltpu.VMEM((2, chips * 2 * n_tp, n_tp * seqs), BF16),
            pltpu.VMEM((3, seqs, chips * 2 * n_tp), BF16),
            pltpu.VMEM((dense[0].shape[0], sum(w.shape[1] for w in dense)), BF16),
        ),
        in_specs=[ANY] * 5,
        out_specs=(IN_VMEM,) * 3,
        scratch_shapes=[
            pltpu.VMEM(ids.shape, ids.dtype),
            pltpu.VMEM(weights.shape, weights.dtype),
            pltpu.SemaphoreType.DMA((5,)),
        ],
        compiler_params=pltpu.CompilerParams(vmem_limit_bytes=8 * MIB),
    )(at_hbm(ids), at_hbm(weights), *[at_hbm(w) for w in dense])


def attend_kernel(chunks, forget_bias, lens_hbm, after, *refs):
    sources, out_ref, rest = refs[:11], refs[11], refs[12:]
    held, (lens, queries, keys, values, shift, scores, mixed, sems) = rest[:11], rest[11:]
    tok, gain, wq, wk, wv, wf, qg, kg, cum, wo, cache = held
    seqs, slots, pair = cache.shape
    head = qg.shape[1]
    group = wq.shape[1] // head
    copies = [pltpu.make_async_copy(sources[i], held[i], sems.at[i]) for i in range(10)]
    step = seqs // chunks
    parts = [
        pltpu.make_async_copy(
            sources[10].at[pl.ds(i * step, step)], cache.at[pl.ds(i * step, step)], sems.at[10 + i]
        )
        for i in range(chunks)
    ]
    lens_copy = pltpu.make_async_copy(lens_hbm, lens, sems.at[10 + chunks])
    lens_copy.start()
    for copy in copies[:9]:
        copy.start()
    for part in parts:
        part.start()
    copies[9].start()
    for copy in copies[:8]:
        copy.wait()

    normed = normal_rows(tok[...].astype(F32), gain[...]).astype(BF16)
    query_raw = dot(normed, wq[...])
    key_new = normal_rows(dot_nt(normed, wk[...]), kg[...]).astype(BF16).astype(F32)
    value_new = dot_nt(normed, wv[...]).astype(BF16).astype(F32)
    blank = jnp.zeros((seqs, pair - head), F32)
    key_new = jnp.concatenate([key_new, blank], axis=1)
    value_new = jnp.concatenate([blank, value_new], axis=1)
    for h in range(group):
        query = normal_rows(query_raw[:, h * head : (h + 1) * head], qg[...])
        query = jnp.concatenate([query.astype(BF16).astype(F32), blank], axis=1)
        queries[pl.ds(h, seqs, stride=group), :] = query
        keys[pl.ds(h, seqs, stride=group), :] = key_new
        values[pl.ds(h, seqs, stride=group), :] = value_new
    forget = jnp.sum(normed.astype(F32) * wf[...].astype(F32), axis=1, keepdims=True) + forget_bias[0]
    log_gate = jnp.minimum(forget, 0.0) - jnp.log1p(jnp.exp(-jnp.abs(forget)))

    lens_copy.wait()
    row = rows_of((seqs, 1))
    length = jnp.zeros((seqs, 1), jnp.int32)
    for s in range(seqs):
        length = jnp.where(row == s, lens[s], length)
    copies[8].wait()
    position = lanes_of((seqs, slots))
    summed = cum[...].reshape(seqs, slots)
    last = jnp.sum(jnp.where(position == length - 1, summed, 0.0), axis=1, keepdims=True)
    shift[...] = jnp.where(position < length, (last + log_gate) - summed, -jnp.inf)

    multiplier = head ** (-0.5)
    own_score = jnp.sum(queries[...] * keys[...], axis=1, keepdims=True) * multiplier
    tall = 2 * group
    upper = rows_of((tall, 1)) < group
    for p in range(seqs // 2):
        if (2 * p) % step == 0:
            parts[2 * p // step].wait()
        query = queries[tall * p : tall * (p + 1), :].astype(BF16)
        score = jnp.where(upper, dot_nt(query, cache[2 * p]), dot_nt(query, cache[2 * p + 1]))
        moved = jnp.where(upper, shift[2 * p : 2 * p + 1, :], shift[2 * p + 1 : 2 * p + 2, :])
        scores[tall * p : tall * (p + 1), :] = score * multiplier + moved
    score = scores[...]
    peak = jnp.maximum(jnp.max(score, axis=1, keepdims=True), own_score)
    past = jnp.exp(score - peak)
    own = jnp.exp(own_score - peak)
    whole = 1.0 / (jnp.sum(past, axis=1, keepdims=True) + own)
    scores[...] = past * whole
    own_prob = (own * whole).astype(BF16).astype(F32)
    for p in range(seqs // 2):
        prob = scores[tall * p : tall * (p + 1), :].astype(BF16)
        mixed[tall * p : tall * (p + 1), :] = jnp.where(
            upper, dot(prob, cache[2 * p]), dot(prob, cache[2 * p + 1])
        )
    mixed[...] = mixed[...] + own_prob * values[...]
    copies[9].wait()
    total = jnp.zeros((seqs, wo.shape[1]), F32)
    for h in range(group):
        mix = mixed[pl.ds(h, seqs, stride=group), :][:, pair - head :].astype(BF16)
        total = total + dot(mix, wo[h * head : (h + 1) * head, :])
    partial = total.astype(BF16)
    for t in range(out_ref.shape[0]):
        out_ref[t] = partial


def attend(n_tp, lens, forget_bias, after, *arrays):
    chunks = 6
    tok, wq, qg, cache = arrays[0], arrays[2], arrays[6], arrays[10]
    seqs, slots, pair = cache.shape
    heads = wq.shape[1] // qg.shape[1]
    rows = seqs * heads
    scratch = [pltpu.VMEM(a.shape, a.dtype) for a in arrays]
    scratch += [pltpu.SMEM(lens.shape, lens.dtype)]
    scratch += [pltpu.VMEM((rows, pair), F32)] * 3
    scratch += [pltpu.VMEM((seqs, slots), F32), pltpu.VMEM((rows, slots), F32), pltpu.VMEM((rows, pair), F32)]
    scratch += [pltpu.SemaphoreType.DMA((11 + chunks,))]
    return pl.pallas_call(
        functools.partial(attend_kernel, chunks),
        name="attend",
        out_shape=pltpu.VMEM((n_tp, *tok.shape), BF16),
        in_specs=[IN_SMEM] + [ANY] * 13,
        out_specs=IN_VMEM,
        scratch_shapes=scratch,
        compiler_params=pltpu.CompilerParams(vmem_limit_bytes=16 * MIB),
    )(forget_bias, at_hbm(lens), after, *[at_hbm(a) for a in arrays])


def send_kernel(crossed, tok, gain, taken_ref, *refs):
    message, own_residual = refs[-2:]
    n_tp = crossed.shape[0]
    seqs, width = tok.shape
    rows = message.shape[0]
    span = width // n_tp
    share = seqs // n_tp
    tp_at = lax.axis_index("tp")
    attn_out = crossed[0].astype(F32)
    for t in range(1, n_tp):
        attn_out = attn_out + crossed[t].astype(F32)
    residual = (tok[...].astype(F32) + attn_out).astype(BF16)
    residual_f = residual.astype(F32)
    kept = residual[:, :span]
    for t in range(1, n_tp):
        kept = jnp.where(tp_at == t, residual[:, t * span : (t + 1) * span], kept)
    own_residual[...] = kept
    normed = normal_rows(residual_f, gain[...])
    pieces = jnp.concatenate([normed[:, q * span : (q + 1) * span] for q in range(n_tp)], axis=0)
    pieces = pieces.astype(BF16)
    wide = n_tp * seqs
    for o in range(2):
        message[:, o * span : (o + 1) * span] = dot(taken_ref[o], pieces).astype(BF16)
    each = 2 * n_tp
    both = 2 * each
    part = share // 2
    narrow = span // 2
    row, lane = rows_of((both, wide)), lanes_of((both, wide))
    token = tp_at * share + (row // each) * part + (row % each) // n_tp
    fits = (lane // seqs == row % n_tp) & (lane % seqs == token)
    block = dot(jnp.where(fits, 1.0, 0.0).astype(BF16), pieces).astype(BF16)
    block = jnp.broadcast_to(block[None], (rows // both, both, span)).reshape(rows, span)
    message[:, 2 * span : 3 * span] = block
    pieces = jnp.concatenate([normed[:, q * narrow : (q + 1) * narrow] for q in range(each)], axis=0)
    row, lane = rows_of((both, each * seqs)), lanes_of((both, each * seqs))
    token = tp_at * share + (row // each) * part + part - 1
    fits = (lane // seqs == row % each) & (lane % seqs == token)
    block = dot(jnp.where(fits, 1.0, 0.0).astype(BF16), pieces.astype(BF16)).astype(BF16)
    block = jnp.broadcast_to(block[None], (rows // both, both, narrow)).reshape(rows, narrow)
    message[:, 3 * span :] = block


def send(crossed, tok, gain, taken, chips, swapped):
    n_tp, seqs, width = crossed.shape
    span = width // n_tp
    rows = chips * 2 * n_tp
    return pl.pallas_call(
        send_kernel,
        name="send",
        out_shape=(
            pltpu.VMEM((rows, 3 * span + span // 2), BF16),
            pltpu.VMEM((seqs, span), BF16),
        ),
        in_specs=[IN_VMEM] * 4 + [ANY] * len(swapped),
        out_specs=(IN_VMEM, IN_VMEM),
        compiler_params=pltpu.CompilerParams(vmem_limit_bytes=8 * MIB),
    )(at_vmem(crossed), tok, gain, at_vmem(taken), *swapped)


def experts_kernel(n_tp, arrived, shared, *refs):
    own, swapped, shards_of, refs = refs[:3], refs[3:6], refs[6:10], refs[10:]
    out_ref, down, spread, held, sems = refs[0], refs[1], refs[2], refs[3:6], refs[6]
    width = shared.shape[0] * shared.shape[1]
    copies = [pltpu.make_async_copy(own[i], held[i], sems.at[i]) for i in range(3)]
    for copy in copies:
        copy.start()
    rows, span = arrived.shape[0], out_ref.shape[2]
    each = 2 * n_tp
    chips = rows // each
    for j in range(spread.shape[0]):
        spread[j] = arrived[:, j * LANES : (j + 1) * LANES].astype(F32)

    def gathered(k, column):
        return jnp.concatenate(
            [
                spread[column // LANES + j, pl.ds(k * n_tp + q, chips, stride=each), :]
                for q in range(n_tp)
                for j in range(span // LANES)
            ],
            axis=1,
        )

    last = [spread[3 * span // LANES, pl.ds(i, chips, stride=each), :] for i in range(each)]
    tokens = [gathered(0, 2 * span), gathered(1, 2 * span), jnp.concatenate(last, axis=1)]
    tokens = jnp.concatenate(tokens, axis=0).astype(BF16)
    gate_row = shared[...].astype(F32)
    gate_row = jnp.concatenate([gate_row[i : i + 1] for i in range(gate_row.shape[0])], axis=1)
    gate_rows = jnp.broadcast_to(gate_row, (8, gate_row.shape[1])).astype(BF16)
    mix_gate = dot_nt(tokens, gate_rows)[:, :1]
    mix_gate = 1.0 / (1.0 + jnp.exp(-mix_gate))
    gate = dot_nt(tokens, jnp.concatenate([w[:, :width] for w in shards_of], axis=0))
    up = dot_nt(tokens, jnp.concatenate([w[:, width : 2 * width] for w in shards_of], axis=0))
    down[...] = jnp.concatenate([w[:, 2 * width :] for w in shards_of], axis=0)
    hidden = (mix_gate * (gate / (1.0 + jnp.exp(-gate)) * up)).astype(BF16)
    taken = chips * 2 * CAP
    for t in range(n_tp):
        out_ref[t, taken:, :] = hidden
    for o in (1, 0):
        tokens = [gathered(k, o * span) for k in range(CAP)]
        tokens = jnp.concatenate(tokens, axis=0).astype(BF16)
        gate_w, up_w, down_w = (held, swapped)[o]
        if o == 0:
            copies[0].wait()
        gate = dot(tokens, gate_w[...])
        if o == 0:
            copies[1].wait()
        up = dot(tokens, up_w[...])
        hidden = (gate / (1.0 + jnp.exp(-gate)) * up).astype(BF16)
        if o == 0:
            copies[2].wait()
        part = dot(hidden, down_w[...]).astype(BF16)
        for t in range(n_tp):
            out_ref[t, o * chips * CAP : (o + 1) * chips * CAP, :] = part[:, t * span : (t + 1) * span]


def experts(n_tp, span, arrived, shared, own, swapped, shards_of):
    rows = arrived.shape[0]
    chips = rows // (2 * n_tp)
    units = sum(w.shape[0] for w in shards_of)
    return pl.pallas_call(
        functools.partial(experts_kernel, n_tp),
        name="experts",
        out_shape=(
            pltpu.VMEM((n_tp, chips * 2 * CAP + chips * 3, span), BF16),
            pltpu.VMEM((units, span), BF16),
        ),
        in_specs=[IN_VMEM] * 2 + [ANY] * 3 + [IN_VMEM] * 7,
        out_specs=(IN_VMEM, IN_VMEM),
        scratch_shapes=[pltpu.VMEM((arrived.shape[1] // LANES, rows, LANES), F32)]
        + [pltpu.VMEM(w.shape, w.dtype) for w in own]
        + [pltpu.SemaphoreType.DMA((3,))],
        compiler_params=pltpu.CompilerParams(vmem_limit_bytes=16 * MIB),
    )(at_vmem(arrived), shared, *[at_hbm(w) for w in own], *[at_vmem(w) for w in (*swapped, *shards_of)])


def combine_kernel(crossed, down, out_ref, spread):
    n_tp, _, span = crossed.shape
    chips, each, _ = out_ref.shape
    block = chips * CAP
    taken = 2 * block
    total = crossed[0, :taken].astype(F32)
    for t in range(1, n_tp):
        total = total + crossed[t, :taken].astype(F32)
    parts = []
    for t in range(n_tp):
        part = dot(crossed[t, taken:], down[...])
        parts += [part[k * chips : (k + 1) * chips] for k in range(part.shape[0] // chips)]
    parts += [total[i * chips : (i + 1) * chips] for i in range(2 * CAP)]
    for i, part in enumerate(parts):
        for j in range(span // LANES):
            spread[i // each * (span // LANES) + j, pl.ds(i % each, chips, stride=each), :] = part[
                :, j * LANES : (j + 1) * LANES
            ]
    for j in range(spread.shape[0]):
        column = spread[j].astype(BF16).reshape(chips, each, LANES)
        out_ref[:, :, j * LANES : (j + 1) * LANES] = column


def combine(crossed, down, chips):
    n_tp, _, span = crossed.shape
    each = 2 * n_tp
    return pl.pallas_call(
        combine_kernel,
        name="combine",
        out_shape=pltpu.VMEM((chips, each, 2 * span), BF16),
        in_specs=[IN_VMEM] * 2,
        out_specs=IN_VMEM,
        scratch_shapes=[pltpu.VMEM((2 * span // LANES, chips * each, LANES), F32)],
        compiler_params=pltpu.CompilerParams(vmem_limit_bytes=8 * MIB),
    )(at_vmem(crossed), at_vmem(down))


def finish_kernel(arrived, place, residual, out_ref):
    span = residual.shape[1]
    left, right = arrived[:, :span], arrived[:, span:]
    total = dot(place[0], left) + (dot(place[1], right) + dot(place[2], right))
    out_ref[...] = (residual[...].astype(F32) + total).astype(BF16)


def finish(arrived, place, residual):
    return pl.pallas_call(
        finish_kernel,
        name="finish",
        out_shape=jax.ShapeDtypeStruct(residual.shape, BF16),
        in_specs=[IN_VMEM] * 3,
        out_specs=IN_VMEM,
        compiler_params=pltpu.CompilerParams(vmem_limit_bytes=8 * MIB),
    )(at_vmem(arrived), at_vmem(place), at_vmem(residual))


def shards(
    tokens,
    attn_gain,
    w_query,
    w_key,
    w_value,
    w_forget,
    forget_bias,
    query_gain,
    key_gain,
    cache_pairs,
    cache_cum,
    lengths,
    w_output,
    ffn_gain,
    expert_ids,
    route_weight,
    w_exp_gate,
    w_exp_up,
    w_exp_down,
    shared_gate,
    w_dense_gate,
    w_dense_up,
    w_dense_down,
):
    seqs, width = tokens.shape
    n_tp, chips = lax.axis_size("tp"), lax.axis_size(FAR)
    span = width // n_tp

    def other(w):
        return lax.ppermute(w, "ep_2", [(0, 1), (1, 0)])

    def neighbour(w, flip):
        axes = ("ep_1", "ep_2")
        return lax.ppermute(w, axes, [(i, i ^ flip) for i in range(lax.axis_size(axes))])

    own = [w_exp_gate[0], w_exp_up[0], w_exp_down[0]]
    swapped = [other(w) for w in own]
    taken, place, packed = prepare(
        n_tp, chips, seqs, expert_ids.T, route_weight.T, (w_dense_gate, w_dense_up, w_dense_down)
    )
    near, far, across = neighbour(packed, 2), neighbour(packed, 3), neighbour(packed, 1)
    partial = attend(
        n_tp,
        lengths,
        forget_bias,
        packed,
        tokens,
        attn_gain[None],
        w_query,
        w_key.T,
        w_value.T,
        w_forget.T,
        query_gain[None],
        key_gain[None],
        cache_cum,
        w_output,
        cache_pairs[:, 0],
    )
    crossed = lax.all_to_all(partial, "tp", 0, 0, tiled=True)
    message, own_residual = send(crossed, tokens, ffn_gain[None], taken, chips, [*swapped, near, across, far])
    arrived = lax.all_to_all(message.reshape(chips, -1, message.shape[1]), FAR, 0, 0, tiled=True)
    blocks, down = experts(
        n_tp,
        span,
        arrived.reshape(message.shape),
        shared_gate.reshape(-1, LANES),
        own,
        swapped,
        (packed, near, across, far),
    )
    crossed = lax.all_to_all(blocks, "tp", 0, 0, tiled=True)
    total = combine(crossed, down, chips)
    arrived = lax.all_to_all(total, FAR, 0, 0, tiled=True)
    return finish(arrived.reshape(-1, arrived.shape[2]), place, own_residual)


def solution(mesh):
    split = Mesh(mesh.devices.reshape(8, 4, 2, mesh.shape["tp"]), ("ep_0", "ep_1", "ep_2", "tp"))
    return jax.shard_map(
        shards,
        mesh=split,
        in_specs=(
            P(EP, None),
            P(),
            P(None, "tp"),
            P(None, "tp"),
            P(None, "tp"),
            P(None, "tp"),
            P("tp"),
            P(),
            P(),
            P(EP, "tp", None, None),
            P(EP, "tp", None),
            P(EP),
            P("tp", None),
            P(),
            P(),
            P(),
            P(EP, None, "tp"),
            P(EP, None, "tp"),
            P(EP, "tp", None),
            P(),
            P(EP, None),
            P(EP, None),
            P(EP, "tp"),
        ),
        out_specs=P(EP, "tp"),
        check_vma=False,
    )
```

time: 86.8 us -> 86.2 us (level)
  blocking collectives: 58.3 us -> 62.1 us
  starting transfers between devices: 5.89 us -> 3.87 us
  local copies, waits for them, and re-layouts: 1.91 us -> 0.02 us
  waiting for transfers between devices: 5.73 us -> 6.94 us
  Pallas kernels: 13.2 us -> 12 us
    all_to_all x1 -> x2, blocking collectives: 18.5 us -> 26.1 us  [the longest x1 15.7 us: shards(): arrived = lax.all_to_all(total, FAR, 0, 0, tiled=True)]
    ppermute x0 -> x3, waiting for transfers between devices: none -> 6.93 us  [neighbour(): lax.ppermute(w, axes, [(i, i ^ flip) for i in range(lax.axis_size(axes))])]
    all_to_all x1 -> x0, waiting for transfers between devices: 4.74 us -> none  [shards(): crossed = lax.all_to_all(partial, 'tp', 0, 0, tiled=True)]
    all_to_all x1 -> x0, starting transfers between devices: 4.3 us -> none  [shards(): crossed = lax.all_to_all(partial, 'tp', 0, 0, tiled=True)]
    all_to_all x1, blocking collectives: 29.7 us -> 25.9 us  [shards(): lax.all_to_all(message.reshape(chips, -1, message.shape[1]), FAR, 0, 0, t...]
    ppermute x0 -> x3, starting transfers between devices: none -> 3.35 us  [neighbour(): lax.ppermute(w, axes, [(i, i ^ flip) for i in range(lax.axis_size(axes))])]
    pallas_call x1 -> x3, Pallas kernels: 0.36 us -> 2.46 us  [the longest x1 1.31 us: prepare(): pl.pallas_call(prepare_kernel, name='prepare', out_shape=(pltpu.VMEM((2,...]
    unnamed x24 -> x6, local copies, waits for them, and re-layouts: 1.91 us -> 0.02 us
  transfers between devices with their start and end apart: 7 -> 6, of which waited for: 3 -> 1; matrix products, arithmetic and copies ran while one was open for 0% -> 0% of each run, Pallas kernels for 8% -> 8%
where the time goes in v3:
time: 86.2 us; the launch traced here: 85.7 us
  blocking collectives  62.1 us (72%)
  Pallas kernels  12 us (14%)
  waiting for transfers between devices  6.94 us (8%)
  starting transfers between devices  3.87 us (4%)
    all_to_all x1, blocking collectives, shards(): lax.all_to_all(message.reshape(chips, -1, message.shape[1]), FAR, 0, 0, t...  25.9 us
    all_to_all x1, blocking collectives, shards(): arrived = lax.all_to_all(total, FAR, 0, 0, tiled=True)  15.7 us
    all_to_all x1, blocking collectives, shards(): crossed = lax.all_to_all(partial, 'tp', 0, 0, tiled=True)  10.5 us
    all_to_all x1, blocking collectives, shards(): crossed = lax.all_to_all(blocks, 'tp', 0, 0, tiled=True)  10.1 us
    ppermute x3, waiting for transfers between devices, neighbour(): lax.ppermute(w, axes, [(i, i ^ flip) for i in range(lax.axis_size(axes))])  6.93 us
    pallas_call x1, Pallas kernels, attend(): pl.pallas_call(functools.partial(attend_kernel, chunks), name='attend', o...  5.47 us
    pallas_call x1, Pallas kernels, experts(): pl.pallas_call(functools.partial(experts_kernel, n_tp), name='experts', o...  3.8 us
    ppermute x3, starting transfers between devices, neighbour(): lax.ppermute(w, axes, [(i, i ^ flip) for i in range(lax.axis_size(axes))])  3.35 us
  transfers between devices with their start and end apart: 6, of which 1 were waited for; matrix products, arithmetic and copies ran while one was open for 0% of the time, Pallas kernels for 8%

profile of v3, /device:TPU:32, one launch (start us, length us, event | category | flops | bytes accessed | tf_op | source)
XLA Modules:
  0.0 85.7 jit_solution(1825470998321583150)
XLA Ops:
  0.0 0.0 collective-permute-start
  0.0 0.5 collective-permute-start.1
  0.5 0.0 collective-permute-start.2
  0.5 1.3 %prepare.1 = (bf16[2,256,96]{2,1,0:T(8,128)(2,1)S(1)}, bf16[3,24,256]{2,1,0:T(8,128)(2,1)S(1)}, bf16[64,2304]{1,0:T(8,128)(2,1)S(1)}) custom-call(s32[2,1536]{1,0:T(2,128)} %bitcast.31, f32[2,1536]{1,0:T(2,128)} %bitcast.32, bf16[64,1024]{1,0:T(8,128)(2,1)} %refs_0_.2, bf16[64,1024]{1,0:T(8,128)(2,1)} %refs_1_.1, bf16[64,256]{1,0:T(8,128)(2,1)} %refs_2_.2), custom_call_target="tpu_custom_call" | custom-call | tf_op jit(solution)/shard_map/prepare/pallas_call | solution.py:135
  1.8 1.8 %collective-permute-start.5 = (bf16[64,2304]{1,0:T(8,128)(2,1)S(1)}, bf16[64,2304]{1,0:T(8,128)(2,1)S(1)}, u32[]{:S(2)}, u32[]{:S(2)}) collective-permute-start(bf16[64,2304]{1,0:T(8,128)(2,1)S(1)} %get-tuple-element.12.after.refs_6_), channel_id=1, source_target_pairs={{0,12},{4,8},{8,4},{12,0},{16,28},{20,24},{24,20},{28,16},{1,13},{... | collective-permute-start | bytes 884744 | tf_op jit(solution)/shard_map/ppermute | solution.py:486
  3.6 0.0 collective-permute-start.4
  3.6 6.9 %collective-permute-done.5.refs_5_.refs_9_ = bf16[64,2304]{1,0:T(8,128)(2,1)S(1)} collective-permute-done((bf16[64,2304]{1,0:T(8,128)(2,1)S(1)}, bf16[64,2304]{1,0:T(8,128)(2,1)S(1)}, u32[]{:S(2)}, u32[]{:S(2)}) %collective-permute-start.5) | collective-permute-done | bytes 294944 | tf_op jit(solution)/shard_map/ppermute | solution.py:486
  10.5 1.6 %collective-permute-start.3 = (bf16[64,2304]{1,0:T(8,128)(2,1)S(1)}, bf16[64,2304]{1,0:T(8,128)(2,1)S(1)}, u32[]{:S(2)}, u32[]{:S(2)}) collective-permute-start(bf16[64,2304]{1,0:T(8,128)(2,1)S(1)} %get-tuple-element.12.after.refs_6_), channel_id=1, source_target_pairs={{0,8},{4,12},{8,0},{12,4},{16,24},{20,28},{24,16},{28,20},{1,9},{5... | collective-permute-start | bytes 884744 | tf_op jit(solution)/shard_map/ppermute | solution.py:486
  12.8 0.0 copy-start
  12.8 0.0 copy-start.1
  12.8 5.5 %attend.1 = bf16[4,24,1024]{2,1,0:T(8,128)(2,1)S(1)} custom-call(f32[1]{0:T(128)S(6)} %copy.24.forget_bias, s32[24]{0:T(128)} %lens_hbm.1, bf16[64,2304]{1,0:T(8,128)(2,1)S(1)} %get-tuple-element.12.after.refs_6_, bf16[24,1024]{1,0:T(8,128)(2,1)} %tok.1, f32[1,1024]{1,0:T(1,128)} %bitcast.33, bf16[1024,256]{1,0:T(8,128)(2,1)} %refs_2_.3, ...), custom_call_target="tpu_custom_call" | custom-call | tf_op jit(solution)/shard_map/attend/pallas_call | solution.py:251
  18.3 10.5 %all_to_all.20.crossed = bf16[4,24,1024]{2,1,0:T(8,128)(2,1)S(1)} all-to-all(bf16[4,24,1024]{2,1,0:T(8,128)(2,1)S(1)} %attend.1), channel_id=1, replica_groups=mesh['ep_0'=8,'ep_1'=4,'ep_2'=2,'tp'=4] {'tp'}, dimensions={0} | all-to-all | bytes 393216 | tf_op jit(solution)/shard_map/all_to_all | solution.py:511
  28.7 0.0 collective-permute-done.4.refs_4_.refs_8_
  28.7 0.0 collective-permute-done.3.refs_3_.refs_7_
  28.7 0.0 collective-permute-done.refs_0_.refs_3_
  28.7 0.0 collective-permute-done.1.refs_1_.refs_4_
  28.8 0.0 copy-start.2
  28.8 0.4 send.1
  29.2 25.9 %all_to_all.21 = bf16[32,8,896]{2,1,0:T(8,128)(2,1)S(1)} all-to-all(bf16[32,8,896]{2,1,0:T(8,128)(2,1)S(1)} %bitcast.19), channel_id=1, replica_groups=mesh['ep_0'=8,'ep_1'=4,'ep_2'=2,'tp'=4] {'ep_0','ep_1'}, dimensions={0} | all-to-all | bytes 917504 | tf_op jit(solution)/shard_map/all_to_all | solution.py:513
  55.0 3.8 %experts.1 = (bf16[4,224,256]{2,1,0:T(8,128)(2,1)S(1)}, bf16[256,256]{1,0:T(8,128)(2,1)S(1)}) custom-call(bf16[256,896]{1,0:T(8,128)(2,1)S(1)} %bitcast.17, bf16[8,128]{1,0:T(8,128)(2,1)S(1)} %bitcast.21, bf16[1024,896]{1,0:T(8,128)(2,1)} %bitcast.24, bf16[1024,896]{1,0:T(8,128)(2,1)} %bitcast.26, bf16[896,1024]{1,0:T(8,128)(2,1)} %bitcast.28, ...), custom_call_target="tpu_custom_call" | custom-call | tf_op jit(solution)/shard_map/experts/pallas_call | solution.py:381
  58.8 10.1 %all_to_all.22.crossed = bf16[4,224,256]{2,1,0:T(8,128)(2,1)S(1)} all-to-all(bf16[4,224,256]{2,1,0:T(8,128)(2,1)S(1)} %get-tuple-element.15), channel_id=1, replica_groups=mesh['ep_0'=8,'ep_1'=4,'ep_2'=2,'tp'=4] {'tp'}, dimensions={0} | all-to-all | bytes 917504 | tf_op jit(solution)/shard_map/all_to_all | solution.py:523
  69.0 0.3 combine.1
  69.2 15.7 %all_to_all.23 = bf16[32,8,512]{2,1,0:T(8,128)(2,1)S(1)} all-to-all(bf16[32,8,512]{2,1,0:T(8,128)(2,1)S(1)} %combine.1), channel_id=1, replica_groups=mesh['ep_0'=8,'ep_1'=4,'ep_2'=2,'tp'=4] {'ep_0','ep_1'}, dimensions={0} | all-to-all | bytes 524288 | tf_op jit(solution)/shard_map/all_to_all | solution.py:525
  84.9 0.8 finish.1
  (4 shorter events, 0.0 us)
Async XLA Ops:
  0.0 28.7 %collective-permute-start = (bf16[1024,896]{1,0:T(8,128)(2,1)}, bf16[1024,896]{1,0:T(8,128)(2,1)S(1)}, u32[]{:S(2)}, u32[]{:S(2)}) collective-permute-start(bf16[1024,896]{1,0:T(8,128)(2,1)} %bitcast.23), channel_id=1, source_target_pairs={{0,4},{4,0},{1,5},{5,1},{2,6},{6,2},{3,7},{7,3},{8,12},{12,8},{9,1... | collective-permute-start | bytes 5505032 | tf_op jit(solution)/shard_map/ppermute | solution.py:482
  0.0 28.7 %collective-permute-start.1 = (bf16[1024,896]{1,0:T(8,128)(2,1)}, bf16[1024,896]{1,0:T(8,128)(2,1)S(1)}, u32[]{:S(2)}, u32[]{:S(2)}) collective-permute-start(bf16[1024,896]{1,0:T(8,128)(2,1)} %bitcast.25), channel_id=1, source_target_pairs={{0,4},{4,0},{1,5},{5,1},{2,6},{6,2},{3,7},{7,3},{8,12},{12,8},{9,1... | collective-permute-start | bytes 5505032 | tf_op jit(solution)/shard_map/ppermute | solution.py:482
  0.5 28.2 %collective-permute-start.2 = (bf16[896,1024]{1,0:T(8,128)(2,1)}, bf16[896,1024]{1,0:T(8,128)(2,1)S(1)}, u32[]{:S(2)}, u32[]{:S(2)}) collective-permute-start(bf16[896,1024]{1,0:T(8,128)(2,1)} %bitcast.27), channel_id=1, source_target_pairs={{0,4},{4,0},{1,5},{5,1},{2,6},{6,2},{3,7},{7,3},{8,12},{12,8},{9,1... | collective-permute-start | bytes 5505032 | tf_op jit(solution)/shard_map/ppermute | solution.py:482
  1.8 8.7 %collective-permute-start.5 = (bf16[64,2304]{1,0:T(8,128)(2,1)S(1)}, bf16[64,2304]{1,0:T(8,128)(2,1)S(1)}, u32[]{:S(2)}, u32[]{:S(2)}) collective-permute-start(bf16[64,2304]{1,0:T(8,128)(2,1)S(1)} %get-tuple-element.12.after.refs_6_), channel_id=1, source_target_pairs={{0,12},{4,8},{8,4},{12,0},{16,28},{20,24},{24,20},{28,16},{1,13},{... | collective-permute-start | bytes 884744 | tf_op jit(solution)/shard_map/ppermute | solution.py:486
  3.6 25.1 %collective-permute-start.4 = (bf16[64,2304]{1,0:T(8,128)(2,1)S(1)}, bf16[64,2304]{1,0:T(8,128)(2,1)S(1)}, u32[]{:S(2)}, u32[]{:S(2)}) collective-permute-start(bf16[64,2304]{1,0:T(8,128)(2,1)S(1)} %get-tuple-element.12.after.refs_6_), channel_id=1, source_target_pairs={{0,4},{4,0},{8,12},{12,8},{16,20},{20,16},{24,28},{28,24},{1,5},{5... | collective-permute-start | bytes 884744 | tf_op jit(solution)/shard_map/ppermute | solution.py:486
  10.5 18.2 %collective-permute-start.3 = (bf16[64,2304]{1,0:T(8,128)(2,1)S(1)}, bf16[64,2304]{1,0:T(8,128)(2,1)S(1)}, u32[]{:S(2)}, u32[]{:S(2)}) collective-permute-start(bf16[64,2304]{1,0:T(8,128)(2,1)S(1)} %get-tuple-element.12.after.refs_6_), channel_id=1, source_target_pairs={{0,8},{4,12},{8,0},{12,4},{16,24},{20,28},{24,16},{28,20},{1,9},{5... | collective-permute-start | bytes 884744 | tf_op jit(solution)/shard_map/ppermute | solution.py:486
  12.8 16.0 %copy-start = (bf16[24,1024]{1,0:T(8,128)(2,1)S(1)}, bf16[24,1024]{1,0:T(8,128)(2,1)}, u32[]{:S(2)}) copy-start(bf16[24,1024]{1,0:T(8,128)(2,1)} %tok.1) | copy-start | bytes 147460
  12.8 16.0 %copy-start.1 = (f32[1024]{0:T(1024)S(1)}, f32[1024]{0:T(1024)}, u32[]{:S(2)}) copy-start(f32[1024]{0:T(1024)} %param.36) | copy-start | bytes 12292
  28.8 26.3 %copy-start.2 = (bf16[1024]{0:T(1024)(128)(2,1)S(1)}, bf16[1024]{0:T(1024)(128)(2,1)}, u32[]{:S(2)}) copy-start(bf16[1024]{0:T(1024)(128)(2,1)} %param.42) | copy-start | bytes 6148

commit v4 on v3

--- a/solution.py
+++ b/solution.py
@@ -152,7 +152,8 @@
 
 
 def attend_kernel(chunks, forget_bias, lens_hbm, after, *refs):
-    sources, out_ref, rest = refs[:11], refs[11], refs[12:]
+    ahead, refs = refs[:3], refs[3:]
+    sources, out_ref, fetched, rest = refs[:11], refs[11], refs[12:15], refs[15:]
     held, (lens, queries, keys, values, shift, scores, mixed, sems) = rest[:11], rest[11:]
     tok, gain, wq, wk, wv, wf, qg, kg, cum, wo, cache = held
     seqs, slots, pair = cache.shape
@@ -167,6 +168,7 @@
         for i in range(chunks)
     ]
     lens_copy = pltpu.make_async_copy(lens_hbm, lens, sems.at[10 + chunks])
+    fetches = [pltpu.make_async_copy(ahead[i], fetched[i], sems.at[11 + chunks + i]) for i in range(3)]
     lens_copy.start()
     for copy in copies[:9]:
         copy.start()
@@ -210,6 +212,9 @@
     for p in range(seqs // 2):
         if (2 * p) % step == 0:
             parts[2 * p // step].wait()
+            if 2 * p // step == 0:
+                for fetch in fetches:
+                    fetch.start()
         query = queries[tall * p : tall * (p + 1), :].astype(BF16)
         score = jnp.where(upper, dot_nt(query, cache[2 * p]), dot_nt(query, cache[2 * p + 1]))
         moved = jnp.where(upper, shift[2 * p : 2 * p + 1, :], shift[2 * p + 1 : 2 * p + 2, :])
@@ -235,10 +240,12 @@
     partial = total.astype(BF16)
     for t in range(out_ref.shape[0]):
         out_ref[t] = partial
-
-
-def attend(n_tp, lens, forget_bias, after, *arrays):
-    chunks = 6
+    for fetch in fetches:
+        fetch.wait()
+
+
+def attend(n_tp, lens, forget_bias, after, ahead, *arrays):
+    chunks = 3
     tok, wq, qg, cache = arrays[0], arrays[2], arrays[6], arrays[10]
     seqs, slots, pair = cache.shape
     heads = wq.shape[1] // qg.shape[1]
@@ -247,16 +254,16 @@
     scratch += [pltpu.SMEM(lens.shape, lens.dtype)]
     scratch += [pltpu.VMEM((rows, pair), F32)] * 3
     scratch += [pltpu.VMEM((seqs, slots), F32), pltpu.VMEM((rows, slots), F32), pltpu.VMEM((rows, pair), F32)]
-    scratch += [pltpu.SemaphoreType.DMA((11 + chunks,))]
+    scratch += [pltpu.SemaphoreType.DMA((14 + chunks,))]
     return pl.pallas_call(
         functools.partial(attend_kernel, chunks),
         name="attend",
-        out_shape=pltpu.VMEM((n_tp, *tok.shape), BF16),
-        in_specs=[IN_SMEM] + [ANY] * 13,
-        out_specs=IN_VMEM,
+        out_shape=(pltpu.VMEM((n_tp, *tok.shape), BF16), *(pltpu.VMEM(w.shape, BF16) for w in ahead)),
+        in_specs=[IN_SMEM] + [ANY] * 16,
+        out_specs=(IN_VMEM,) * 4,
         scratch_shapes=scratch,
         compiler_params=pltpu.CompilerParams(vmem_limit_bytes=16 * MIB),
-    )(forget_bias, at_hbm(lens), after, *[at_hbm(a) for a in arrays])
+    )(forget_bias, at_hbm(lens), after, *[at_hbm(a) for a in (*ahead, *arrays)])
 
 
 def send_kernel(crossed, tok, gain, taken_ref, *refs):
@@ -320,11 +327,8 @@
 
 def experts_kernel(n_tp, arrived, shared, *refs):
     own, swapped, shards_of, refs = refs[:3], refs[3:6], refs[6:10], refs[10:]
-    out_ref, down, spread, held, sems = refs[0], refs[1], refs[2], refs[3:6], refs[6]
+    out_ref, down, spread = refs
     width = shared.shape[0] * shared.shape[1]
-    copies = [pltpu.make_async_copy(own[i], held[i], sems.at[i]) for i in range(3)]
-    for copy in copies:
-        copy.start()
     rows, span = arrived.shape[0], out_ref.shape[2]
     each = 2 * n_tp
     chips = rows // each
@@ -356,19 +360,13 @@
     taken = chips * 2 * CAP
     for t in range(n_tp):
         out_ref[t, taken:, :] = hidden
-    for o in (1, 0):
+    for o in range(2):
         tokens = [gathered(k, o * span) for k in range(CAP)]
         tokens = jnp.concatenate(tokens, axis=0).astype(BF16)
-        gate_w, up_w, down_w = (held, swapped)[o]
-        if o == 0:
-            copies[0].wait()
+        gate_w, up_w, down_w = (own, swapped)[o]
         gate = dot(tokens, gate_w[...])
-        if o == 0:
-            copies[1].wait()
         up = dot(tokens, up_w[...])
         hidden = (gate / (1.0 + jnp.exp(-gate)) * up).astype(BF16)
-        if o == 0:
-            copies[2].wait()
         part = dot(hidden, down_w[...]).astype(BF16)
         for t in range(n_tp):
             out_ref[t, o * chips * CAP : (o + 1) * chips * CAP, :] = part[:, t * span : (t + 1) * span]
@@ -385,13 +383,11 @@
             pltpu.VMEM((n_tp, chips * 2 * CAP + chips * 3, span), BF16),
             pltpu.VMEM((units, span), BF16),
         ),
-        in_specs=[IN_VMEM] * 2 + [ANY] * 3 + [IN_VMEM] * 7,
+        in_specs=[IN_VMEM] * 12,
         out_specs=(IN_VMEM, IN_VMEM),
-        scratch_shapes=[pltpu.VMEM((arrived.shape[1] // LANES, rows, LANES), F32)]
-        + [pltpu.VMEM(w.shape, w.dtype) for w in own]
-        + [pltpu.SemaphoreType.DMA((3,))],
-        compiler_params=pltpu.CompilerParams(vmem_limit_bytes=16 * MIB),
-    )(at_vmem(arrived), shared, *[at_hbm(w) for w in own], *[at_vmem(w) for w in (*swapped, *shards_of)])
+        scratch_shapes=[pltpu.VMEM((arrived.shape[1] // LANES, rows, LANES), F32)],
+        compiler_params=pltpu.CompilerParams(vmem_limit_bytes=8 * MIB),
+    )(at_vmem(arrived), shared, *[at_vmem(w) for w in (*own, *swapped, *shards_of)])
 
 
 def combine_kernel(crossed, down, out_ref, spread):
@@ -491,11 +487,12 @@
         n_tp, chips, seqs, expert_ids.T, route_weight.T, (w_dense_gate, w_dense_up, w_dense_down)
     )
     near, far, across = neighbour(packed, 2), neighbour(packed, 3), neighbour(packed, 1)
-    partial = attend(
+    partial, *fetched = attend(
         n_tp,
         lengths,
         forget_bias,
         packed,
+        own,
         tokens,
         attn_gain[None],
         w_query,
@@ -516,7 +513,7 @@
         span,
         arrived.reshape(message.shape),
         shared_gate.reshape(-1, LANES),
-        own,
+        fetched,
         swapped,
         (packed, near, across, far),
     )

time: 86.2 us -> 84.5 us (0.980)
  Pallas kernels: 12 us -> 10.3 us
    pallas_call x1, Pallas kernels: 3.8 us -> 2.25 us  [experts(): pl.pallas_call(functools.partial(experts_kernel, n_tp), name='experts', o...]
where the time goes in v4:
time: 84.5 us; the launch traced here: 84 us
  blocking collectives  62.1 us (73%)
  Pallas kernels  10.3 us (12%)
  waiting for transfers between devices  6.94 us (8%)
  starting transfers between devices  3.87 us (5%)
    all_to_all x1, blocking collectives, shards(): lax.all_to_all(message.reshape(chips, -1, message.shape[1]), FAR, 0, 0, t...  25.9 us
    all_to_all x1, blocking collectives, shards(): arrived = lax.all_to_all(total, FAR, 0, 0, tiled=True)  15.7 us
    all_to_all x1, blocking collectives, shards(): crossed = lax.all_to_all(partial, 'tp', 0, 0, tiled=True)  10.5 us
    all_to_all x1, blocking collectives, shards(): crossed = lax.all_to_all(blocks, 'tp', 0, 0, tiled=True)  10.1 us
    ppermute x3, waiting for transfers between devices, neighbour(): lax.ppermute(w, axes, [(i, i ^ flip) for i in range(lax.axis_size(axes))])  6.93 us
    pallas_call x1, Pallas kernels, attend(): pl.pallas_call(functools.partial(attend_kernel, chunks), name='attend', o...  5.3 us
    ppermute x3, starting transfers between devices, neighbour(): lax.ppermute(w, axes, [(i, i ^ flip) for i in range(lax.axis_size(axes))])  3.35 us
    pallas_call x1, Pallas kernels, experts(): pl.pallas_call(functools.partial(experts_kernel, n_tp), name='experts', o...  2.25 us
  transfers between devices with their start and end apart: 6, of which 1 were waited for; matrix products, arithmetic and copies ran while one was open for 0% of the time, Pallas kernels for 8%

profile of v4, /device:TPU:32, one launch (start us, length us, event | category | flops | bytes accessed | tf_op | source)
XLA Modules:
  0.0 84.0 jit_solution(12238045532072169594)
XLA Ops:
  0.0 0.0 collective-permute-start
  0.0 0.5 collective-permute-start.1
  0.5 0.0 collective-permute-start.2
  0.5 1.3 %prepare.1 = (bf16[2,256,96]{2,1,0:T(8,128)(2,1)S(1)}, bf16[3,24,256]{2,1,0:T(8,128)(2,1)S(1)}, bf16[64,2304]{1,0:T(8,128)(2,1)S(1)}) custom-call(s32[2,1536]{1,0:T(2,128)} %bitcast.31, f32[2,1536]{1,0:T(2,128)} %bitcast.32, bf16[64,1024]{1,0:T(8,128)(2,1)} %refs_0_.1, bf16[64,1024]{1,0:T(8,128)(2,1)} %refs_1_.1, bf16[64,256]{1,0:T(8,128)(2,1)} %refs_2_.1), custom_call_target="tpu_custom_call" | custom-call | tf_op jit(solution)/shard_map/prepare/pallas_call | solution.py:135
  1.8 1.8 %collective-permute-start.5 = (bf16[64,2304]{1,0:T(8,128)(2,1)S(1)}, bf16[64,2304]{1,0:T(8,128)(2,1)S(1)}, u32[]{:S(2)}, u32[]{:S(2)}) collective-permute-start(bf16[64,2304]{1,0:T(8,128)(2,1)S(1)} %get-tuple-element.16.after.refs_6_), channel_id=1, source_target_pairs={{0,12},{4,8},{8,4},{12,0},{16,28},{20,24},{24,20},{28,16},{1,13},{... | collective-permute-start | bytes 884744 | tf_op jit(solution)/shard_map/ppermute | solution.py:482
  3.6 0.0 collective-permute-start.4
  3.6 6.9 %collective-permute-done.5.refs_5_.refs_9_ = bf16[64,2304]{1,0:T(8,128)(2,1)S(1)} collective-permute-done((bf16[64,2304]{1,0:T(8,128)(2,1)S(1)}, bf16[64,2304]{1,0:T(8,128)(2,1)S(1)}, u32[]{:S(2)}, u32[]{:S(2)}) %collective-permute-start.5) | collective-permute-done | bytes 294944 | tf_op jit(solution)/shard_map/ppermute | solution.py:482
  10.5 1.6 %collective-permute-start.3 = (bf16[64,2304]{1,0:T(8,128)(2,1)S(1)}, bf16[64,2304]{1,0:T(8,128)(2,1)S(1)}, u32[]{:S(2)}, u32[]{:S(2)}) collective-permute-start(bf16[64,2304]{1,0:T(8,128)(2,1)S(1)} %get-tuple-element.16.after.refs_6_), channel_id=1, source_target_pairs={{0,8},{4,12},{8,0},{12,4},{16,24},{20,28},{24,16},{28,20},{1,9},{5... | collective-permute-start | bytes 884744 | tf_op jit(solution)/shard_map/ppermute | solution.py:482
  12.8 0.0 copy-start
  12.8 0.0 copy-start.1
  12.8 5.3 %attend.1 = (bf16[4,24,1024]{2,1,0:T(8,128)(2,1)S(1)}, bf16[1024,896]{1,0:T(8,128)(2,1)S(1)}, bf16[1024,896]{1,0:T(8,128)(2,1)S(1)}, bf16[896,1024]{1,0:T(8,128)(2,1)S(1)}) custom-call(f32[1]{0:T(128)S(6)} %copy.24.forget_bias, s32[24]{0:T(128)} %lens_hbm.1, bf16[64,2304]{1,0:T(8,128)(2,1)S(1)} %get-tuple-element.16.after.refs_6_, ...), custom_call_target="tpu_custom_call" | custom-call | tf_op jit(solution)/shard_map/attend/pallas_call | solution.py:258
  18.1 10.5 %all_to_all.20.crossed = bf16[4,24,1024]{2,1,0:T(8,128)(2,1)S(1)} all-to-all(bf16[4,24,1024]{2,1,0:T(8,128)(2,1)S(1)} %get-tuple-element.17), channel_id=1, replica_groups=mesh['ep_0'=8,'ep_1'=4,'ep_2'=2,'tp'=4] {'tp'}, dimensions={0} | all-to-all | bytes 393216 | tf_op jit(solution)/shard_map/all_to_all | solution.py:508
  28.6 0.0 collective-permute-done.4.refs_4_.refs_8_
  28.6 0.0 collective-permute-done.3.refs_3_.refs_7_
  28.6 0.0 collective-permute-done.refs_0_.refs_3_
  28.6 0.0 collective-permute-done.1.refs_1_.refs_4_
  28.6 0.0 copy-start.2
  28.6 0.4 send.1
  29.0 25.9 %all_to_all.21 = bf16[32,8,896]{2,1,0:T(8,128)(2,1)S(1)} all-to-all(bf16[32,8,896]{2,1,0:T(8,128)(2,1)S(1)} %bitcast.19), channel_id=1, replica_groups=mesh['ep_0'=8,'ep_1'=4,'ep_2'=2,'tp'=4] {'ep_0','ep_1'}, dimensions={0} | all-to-all | bytes 917504 | tf_op jit(solution)/shard_map/all_to_all | solution.py:510
  54.9 2.3 %experts.1 = (bf16[4,224,256]{2,1,0:T(8,128)(2,1)S(1)}, bf16[256,256]{1,0:T(8,128)(2,1)S(1)}) custom-call(bf16[256,896]{1,0:T(8,128)(2,1)S(1)} %bitcast.17, bf16[8,128]{1,0:T(8,128)(2,1)S(1)} %bitcast.21, bf16[1024,896]{1,0:T(8,128)(2,1)S(1)} %get-tuple-element.20.refs_0_, bf16[1024,896]{1,0:T(8,128)(2,1)S(1)} %get-tuple-element.21.refs_1_, ...), custom_call_target="tpu_custom_call" | custom-call | tf_op jit(solution)/shard_map/experts/pallas_call | solution.py:379
  57.1 10.1 %all_to_all.22.crossed = bf16[4,224,256]{2,1,0:T(8,128)(2,1)S(1)} all-to-all(bf16[4,224,256]{2,1,0:T(8,128)(2,1)S(1)} %get-tuple-element.23), channel_id=1, replica_groups=mesh['ep_0'=8,'ep_1'=4,'ep_2'=2,'tp'=4] {'tp'}, dimensions={0} | all-to-all | bytes 917504 | tf_op jit(solution)/shard_map/all_to_all | solution.py:520
  67.2 0.3 combine.1
  67.5 15.7 %all_to_all.23 = bf16[32,8,512]{2,1,0:T(8,128)(2,1)S(1)} all-to-all(bf16[32,8,512]{2,1,0:T(8,128)(2,1)S(1)} %combine.1), channel_id=1, replica_groups=mesh['ep_0'=8,'ep_1'=4,'ep_2'=2,'tp'=4] {'ep_0','ep_1'}, dimensions={0} | all-to-all | bytes 524288 | tf_op jit(solution)/shard_map/all_to_all | solution.py:522
  83.2 0.8 finish.1
  (4 shorter events, 0.0 us)
Async XLA Ops:
  0.0 28.6 %collective-permute-start = (bf16[1024,896]{1,0:T(8,128)(2,1)}, bf16[1024,896]{1,0:T(8,128)(2,1)S(1)}, u32[]{:S(2)}, u32[]{:S(2)}) collective-permute-start(bf16[1024,896]{1,0:T(8,128)(2,1)} %bitcast.23), channel_id=1, source_target_pairs={{0,4},{4,0},{1,5},{5,1},{2,6},{6,2},{3,7},{7,3},{8,12},{12,8},{9,1... | collective-permute-start | bytes 5505032 | tf_op jit(solution)/shard_map/ppermute | solution.py:478
  0.0 28.6 %collective-permute-start.1 = (bf16[1024,896]{1,0:T(8,128)(2,1)}, bf16[1024,896]{1,0:T(8,128)(2,1)S(1)}, u32[]{:S(2)}, u32[]{:S(2)}) collective-permute-start(bf16[1024,896]{1,0:T(8,128)(2,1)} %bitcast.25), channel_id=1, source_target_pairs={{0,4},{4,0},{1,5},{5,1},{2,6},{6,2},{3,7},{7,3},{8,12},{12,8},{9,1... | collective-permute-start | bytes 5505032 | tf_op jit(solution)/shard_map/ppermute | solution.py:478
  0.5 28.1 %collective-permute-start.2 = (bf16[896,1024]{1,0:T(8,128)(2,1)}, bf16[896,1024]{1,0:T(8,128)(2,1)S(1)}, u32[]{:S(2)}, u32[]{:S(2)}) collective-permute-start(bf16[896,1024]{1,0:T(8,128)(2,1)} %bitcast.27), channel_id=1, source_target_pairs={{0,4},{4,0},{1,5},{5,1},{2,6},{6,2},{3,7},{7,3},{8,12},{12,8},{9,1... | collective-permute-start | bytes 5505032 | tf_op jit(solution)/shard_map/ppermute | solution.py:478
  1.8 8.7 %collective-permute-start.5 = (bf16[64,2304]{1,0:T(8,128)(2,1)S(1)}, bf16[64,2304]{1,0:T(8,128)(2,1)S(1)}, u32[]{:S(2)}, u32[]{:S(2)}) collective-permute-start(bf16[64,2304]{1,0:T(8,128)(2,1)S(1)} %get-tuple-element.16.after.refs_6_), channel_id=1, source_target_pairs={{0,12},{4,8},{8,4},{12,0},{16,28},{20,24},{24,20},{28,16},{1,13},{... | collective-permute-start | bytes 884744 | tf_op jit(solution)/shard_map/ppermute | solution.py:482
  3.6 24.9 %collective-permute-start.4 = (bf16[64,2304]{1,0:T(8,128)(2,1)S(1)}, bf16[64,2304]{1,0:T(8,128)(2,1)S(1)}, u32[]{:S(2)}, u32[]{:S(2)}) collective-permute-start(bf16[64,2304]{1,0:T(8,128)(2,1)S(1)} %get-tuple-element.16.after.refs_6_), channel_id=1, source_target_pairs={{0,4},{4,0},{8,12},{12,8},{16,20},{20,16},{24,28},{28,24},{1,5},{5... | collective-permute-start | bytes 884744 | tf_op jit(solution)/shard_map/ppermute | solution.py:482
  10.5 18.0 %collective-permute-start.3 = (bf16[64,2304]{1,0:T(8,128)(2,1)S(1)}, bf16[64,2304]{1,0:T(8,128)(2,1)S(1)}, u32[]{:S(2)}, u32[]{:S(2)}) collective-permute-start(bf16[64,2304]{1,0:T(8,128)(2,1)S(1)} %get-tuple-element.16.after.refs_6_), channel_id=1, source_target_pairs={{0,8},{4,12},{8,0},{12,4},{16,24},{20,28},{24,16},{28,20},{1,9},{5... | collective-permute-start | bytes 884744 | tf_op jit(solution)/shard_map/ppermute | solution.py:482
  12.8 15.8 %copy-start = (bf16[24,1024]{1,0:T(8,128)(2,1)S(1)}, bf16[24,1024]{1,0:T(8,128)(2,1)}, u32[]{:S(2)}) copy-start(bf16[24,1024]{1,0:T(8,128)(2,1)} %tok.1) | copy-start | bytes 147460
  12.8 15.8 %copy-start.1 = (f32[1024]{0:T(1024)S(1)}, f32[1024]{0:T(1024)}, u32[]{:S(2)}) copy-start(f32[1024]{0:T(1024)} %param.36) | copy-start | bytes 12292
  28.6 26.3 %copy-start.2 = (bf16[1024]{0:T(1024)(128)(2,1)S(1)}, bf16[1024]{0:T(1024)(128)(2,1)}, u32[]{:S(2)}) copy-start(bf16[1024]{0:T(1024)(128)(2,1)} %param.42) | copy-start | bytes 6148

commit v5 on v4

--- a/solution.py
+++ b/solution.py
@@ -16,6 +16,8 @@
 CAP = 2
 LANES = 128
 MIB = 1 << 20
+HEADS_ORDER = (1, 3, 2)
+EXPERT_ORDER = (2, 1, 3)
 ANY = pl.BlockSpec(memory_space=pl.ANY)
 IN_VMEM = pl.BlockSpec(memory_space=pltpu.VMEM)
 IN_SMEM = pl.BlockSpec(memory_space=pltpu.SMEM)
@@ -53,7 +55,7 @@
 
 def route_tables(ids, weights, taken_ref, place_ref):
     n_tp, n_core = lax.axis_size("tp"), lax.axis_size("ep_2")
-    core_at, chip_at = lax.axis_index("ep_2"), lax.axis_index(FAR)
+    core_at, chip_at, tp_at = lax.axis_index("ep_2"), lax.axis_index(FAR), lax.axis_index("tp")
     rows, wide = taken_ref.shape[1:]
     batch = ids.shape[1]
     seqs = wide // n_tp
@@ -103,7 +105,8 @@
     part = share // 2
 
     def fits(index):
-        return token == (index // part) * share + ((lane // each) % 2) * part + index % part
+        owner = (tp_at - index // part + n_tp) % n_tp
+        return token == owner * share + ((lane // each) % 2) * part + index % part
 
     first = jnp.where(fits(place_at), 1.0, 0.0)
     second = jnp.where((place_at < 2 * CAP) & fits(place_at + each), 1.0, 0.0)
@@ -111,44 +114,60 @@
         place_ref[i] = table.astype(BF16)
 
 
-def prepare_kernel(ids_hbm, weights_hbm, *refs):
-    dense, (taken_ref, place_ref, packed, ids, weights, sems) = refs[:3], refs[3:]
+def tables_kernel(ids_hbm, weights_hbm, after, taken_ref, place_ref, ids, weights, sems):
     copies = [
         pltpu.make_async_copy(ids_hbm, ids, sems.at[0]),
         pltpu.make_async_copy(weights_hbm, weights, sems.at[1]),
     ]
-    at = 0
+    for copy in copies:
+        copy.start()
+    for copy in copies:
+        copy.wait()
+    route_tables(ids, weights, taken_ref, place_ref)
+
+
+def tables(n_tp, chips, seqs, ids, weights, after):
+    return pl.pallas_call(
+        tables_kernel,
+        name="tables",
+        out_shape=(
+            pltpu.VMEM((2, chips * 2 * n_tp, n_tp * seqs), BF16),
+            pltpu.VMEM((3, seqs, chips * 2 * n_tp), BF16),
+        ),
+        in_specs=[ANY] * 3,
+        out_specs=(IN_VMEM,) * 2,
+        scratch_shapes=[
+            pltpu.VMEM(ids.shape, ids.dtype),
+            pltpu.VMEM(weights.shape, weights.dtype),
+            pltpu.SemaphoreType.DMA((2,)),
+        ],
+        compiler_params=pltpu.CompilerParams(vmem_limit_bytes=8 * MIB),
+    )(at_hbm(ids), at_hbm(weights), after)
+
+
+def pack_kernel(*refs):
+    dense, packed, sems = refs[:3], refs[3], refs[4]
+    copies, at = [], 0
     for i, source in enumerate(dense):
         into = packed.at[:, at : at + source.shape[1]]
-        copies.append(pltpu.make_async_copy(source, into, sems.at[2 + i]))
+        copies.append(pltpu.make_async_copy(source, into, sems.at[i]))
         at += source.shape[1]
     for copy in copies:
         copy.start()
-    for copy in copies[:2]:
+    for copy in copies:
         copy.wait()
-    route_tables(ids, weights, taken_ref, place_ref)
-    for copy in copies[2:]:
-        copy.wait()
-
-
-def prepare(n_tp, chips, seqs, ids, weights, dense):
-    return pl.pallas_call(
-        prepare_kernel,
-        name="prepare",
-        out_shape=(
-            pltpu.VMEM((2, chips * 2 * n_tp, n_tp * seqs), BF16),
-            pltpu.VMEM((3, seqs, chips * 2 * n_tp), BF16),
-            pltpu.VMEM((dense[0].shape[0], sum(w.shape[1] for w in dense)), BF16),
-        ),
-        in_specs=[ANY] * 5,
-        out_specs=(IN_VMEM,) * 3,
-        scratch_shapes=[
-            pltpu.VMEM(ids.shape, ids.dtype),
-            pltpu.VMEM(weights.shape, weights.dtype),
-            pltpu.SemaphoreType.DMA((5,)),
-        ],
-        compiler_params=pltpu.CompilerParams(vmem_limit_bytes=8 * MIB),
-    )(at_hbm(ids), at_hbm(weights), *[at_hbm(w) for w in dense])
+
+
+def pack(dense):
+    return pl.pallas_call(
+        pack_kernel,
+        name="pack",
+        out_shape=pltpu.VMEM((dense[0].shape[0], sum(w.shape[1] for w in dense)), BF16),
+        in_specs=[ANY] * 3,
+        out_specs=IN_VMEM,
+        scratch_shapes=[pltpu.SemaphoreType.DMA((3,))],
+        compiler_params=pltpu.CompilerParams(vmem_limit_bytes=1 * MIB),
+    )(*[at_hbm(w) for w in dense])
 
 
 def attend_kernel(chunks, forget_bias, lens_hbm, after, *refs):
@@ -238,13 +257,12 @@
         mix = mixed[pl.ds(h, seqs, stride=group), :][:, pair - head :].astype(BF16)
         total = total + dot(mix, wo[h * head : (h + 1) * head, :])
     partial = total.astype(BF16)
-    for t in range(out_ref.shape[0]):
-        out_ref[t] = partial
+    out_ref[...] = partial
     for fetch in fetches:
         fetch.wait()
 
 
-def attend(n_tp, lens, forget_bias, after, ahead, *arrays):
+def attend(lens, forget_bias, after, ahead, *arrays):
     chunks = 3
     tok, wq, qg, cache = arrays[0], arrays[2], arrays[6], arrays[10]
     seqs, slots, pair = cache.shape
@@ -258,7 +276,7 @@
     return pl.pallas_call(
         functools.partial(attend_kernel, chunks),
         name="attend",
-        out_shape=(pltpu.VMEM((n_tp, *tok.shape), BF16), *(pltpu.VMEM(w.shape, BF16) for w in ahead)),
+        out_shape=(pltpu.VMEM(tok.shape, BF16), *(pltpu.VMEM(w.shape, BF16) for w in ahead)),
         in_specs=[IN_SMEM] + [ANY] * 16,
         out_specs=(IN_VMEM,) * 4,
         scratch_shapes=scratch,
@@ -266,17 +284,16 @@
     )(forget_bias, at_hbm(lens), after, *[at_hbm(a) for a in (*ahead, *arrays)])
 
 
-def send_kernel(crossed, tok, gain, taken_ref, *refs):
-    message, own_residual = refs[-2:]
-    n_tp = crossed.shape[0]
+def send_kernel(n_tp, *refs):
+    crossed, (tok, gain, taken_ref), (message, own_residual) = refs[:n_tp], refs[n_tp : n_tp + 3], refs[-2:]
     seqs, width = tok.shape
     rows = message.shape[0]
     span = width // n_tp
     share = seqs // n_tp
     tp_at = lax.axis_index("tp")
-    attn_out = crossed[0].astype(F32)
+    attn_out = crossed[0][...].astype(F32)
     for t in range(1, n_tp):
-        attn_out = attn_out + crossed[t].astype(F32)
+        attn_out = attn_out + crossed[t][...].astype(F32)
     residual = (tok[...].astype(F32) + attn_out).astype(BF16)
     residual_f = residual.astype(F32)
     kept = residual[:, :span]
@@ -309,27 +326,29 @@
 
 
 def send(crossed, tok, gain, taken, chips, swapped):
-    n_tp, seqs, width = crossed.shape
+    n_tp = len(crossed)
+    seqs, width = tok.shape
     span = width // n_tp
     rows = chips * 2 * n_tp
     return pl.pallas_call(
-        send_kernel,
+        functools.partial(send_kernel, n_tp),
         name="send",
         out_shape=(
             pltpu.VMEM((rows, 3 * span + span // 2), BF16),
             pltpu.VMEM((seqs, span), BF16),
         ),
-        in_specs=[IN_VMEM] * 4 + [ANY] * len(swapped),
+        in_specs=[IN_VMEM] * (n_tp + 3) + [ANY] * len(swapped),
         out_specs=(IN_VMEM, IN_VMEM),
         compiler_params=pltpu.CompilerParams(vmem_limit_bytes=8 * MIB),
-    )(at_vmem(crossed), tok, gain, at_vmem(taken), *swapped)
+    )(*[at_vmem(part) for part in crossed], tok, gain, at_vmem(taken), *swapped)
 
 
 def experts_kernel(n_tp, arrived, shared, *refs):
     own, swapped, shards_of, refs = refs[:3], refs[3:6], refs[6:10], refs[10:]
-    out_ref, down, spread = refs
+    blocks, (down, spread) = refs[:n_tp], refs[n_tp:]
+    tp_at = lax.axis_index("tp")
     width = shared.shape[0] * shared.shape[1]
-    rows, span = arrived.shape[0], out_ref.shape[2]
+    rows, span = arrived.shape[0], blocks[0].shape[1]
     each = 2 * n_tp
     chips = rows // each
     for j in range(spread.shape[0]):
@@ -358,8 +377,8 @@
     down[...] = jnp.concatenate([w[:, 2 * width :] for w in shards_of], axis=0)
     hidden = (mix_gate * (gate / (1.0 + jnp.exp(-gate)) * up)).astype(BF16)
     taken = chips * 2 * CAP
-    for t in range(n_tp):
-        out_ref[t, taken:, :] = hidden
+    for block in blocks:
+        block[taken:, :] = hidden
     for o in range(2):
         tokens = [gathered(k, o * span) for k in range(CAP)]
         tokens = jnp.concatenate(tokens, axis=0).astype(BF16)
@@ -368,8 +387,12 @@
         up = dot(tokens, up_w[...])
         hidden = (gate / (1.0 + jnp.exp(-gate)) * up).astype(BF16)
         part = dot(hidden, down_w[...]).astype(BF16)
-        for t in range(n_tp):
-            out_ref[t, o * chips * CAP : (o + 1) * chips * CAP, :] = part[:, t * span : (t + 1) * span]
+        parts = [part[:, t * span : (t + 1) * span] for t in range(n_tp)]
+        for k in range(n_tp):
+            chosen = parts[k]
+            for t in range(1, n_tp):
+                chosen = jnp.where(tp_at == t, parts[(t + k) % n_tp], chosen)
+            blocks[k][o * chips * CAP : (o + 1) * chips * CAP, :] = chosen
 
 
 def experts(n_tp, span, arrived, shared, own, swapped, shards_of):
@@ -380,27 +403,28 @@
         functools.partial(experts_kernel, n_tp),
         name="experts",
         out_shape=(
-            pltpu.VMEM((n_tp, chips * 2 * CAP + chips * 3, span), BF16),
+            *[pltpu.VMEM((chips * 2 * CAP + chips * 3, span), BF16)] * n_tp,
             pltpu.VMEM((units, span), BF16),
         ),
         in_specs=[IN_VMEM] * 12,
-        out_specs=(IN_VMEM, IN_VMEM),
+        out_specs=(IN_VMEM,) * (n_tp + 1),
         scratch_shapes=[pltpu.VMEM((arrived.shape[1] // LANES, rows, LANES), F32)],
         compiler_params=pltpu.CompilerParams(vmem_limit_bytes=8 * MIB),
     )(at_vmem(arrived), shared, *[at_vmem(w) for w in (*own, *swapped, *shards_of)])
 
 
-def combine_kernel(crossed, down, out_ref, spread):
-    n_tp, _, span = crossed.shape
+def combine_kernel(n_tp, *refs):
+    crossed, (down, out_ref, spread) = refs[:n_tp], refs[n_tp:]
+    span = down.shape[1]
     chips, each, _ = out_ref.shape
     block = chips * CAP
     taken = 2 * block
-    total = crossed[0, :taken].astype(F32)
+    total = crossed[0][:taken].astype(F32)
     for t in range(1, n_tp):
-        total = total + crossed[t, :taken].astype(F32)
+        total = total + crossed[t][:taken].astype(F32)
     parts = []
     for t in range(n_tp):
-        part = dot(crossed[t, taken:], down[...])
+        part = dot(crossed[t][taken:], down[...])
         parts += [part[k * chips : (k + 1) * chips] for k in range(part.shape[0] // chips)]
     parts += [total[i * chips : (i + 1) * chips] for i in range(2 * CAP)]
     for i, part in enumerate(parts):
@@ -414,17 +438,17 @@
 
 
 def combine(crossed, down, chips):
-    n_tp, _, span = crossed.shape
+    n_tp, span = len(crossed), down.shape[1]
     each = 2 * n_tp
     return pl.pallas_call(
-        combine_kernel,
+        functools.partial(combine_kernel, n_tp),
         name="combine",
         out_shape=pltpu.VMEM((chips, each, 2 * span), BF16),
-        in_specs=[IN_VMEM] * 2,
+        in_specs=[IN_VMEM] * (n_tp + 1),
         out_specs=IN_VMEM,
         scratch_shapes=[pltpu.VMEM((2 * span // LANES, chips * each, LANES), F32)],
         compiler_params=pltpu.CompilerParams(vmem_limit_bytes=8 * MIB),
-    )(at_vmem(crossed), at_vmem(down))
+    )(*[at_vmem(block) for block in crossed], at_vmem(down))
 
 
 def finish_kernel(arrived, place, residual, out_ref):
@@ -481,14 +505,14 @@
         axes = ("ep_1", "ep_2")
         return lax.ppermute(w, axes, [(i, i ^ flip) for i in range(lax.axis_size(axes))])
 
+    def passed_on(x, k):
+        return lax.ppermute(x, "tp", [(i, (i + k) % n_tp) for i in range(n_tp)])
+
     own = [w_exp_gate[0], w_exp_up[0], w_exp_down[0]]
     swapped = [other(w) for w in own]
-    taken, place, packed = prepare(
-        n_tp, chips, seqs, expert_ids.T, route_weight.T, (w_dense_gate, w_dense_up, w_dense_down)
-    )
+    packed = pack((w_dense_gate, w_dense_up, w_dense_down))
     near, far, across = neighbour(packed, 2), neighbour(packed, 3), neighbour(packed, 1)
     partial, *fetched = attend(
-        n_tp,
         lengths,
         forget_bias,
         packed,
@@ -505,10 +529,11 @@
         w_output,
         cache_pairs[:, 0],
     )
-    crossed = lax.all_to_all(partial, "tp", 0, 0, tiled=True)
+    crossed = [partial] + [passed_on(partial, k) for k in HEADS_ORDER]
+    taken, place = tables(n_tp, chips, seqs, expert_ids.T, route_weight.T, partial)
     message, own_residual = send(crossed, tokens, ffn_gain[None], taken, chips, [*swapped, near, across, far])
     arrived = lax.all_to_all(message.reshape(chips, -1, message.shape[1]), FAR, 0, 0, tiled=True)
-    blocks, down = experts(
+    *blocks, down = experts(
         n_tp,
         span,
         arrived.reshape(message.shape),
@@ -517,7 +542,8 @@
         swapped,
         (packed, near, across, far),
     )
-    crossed = lax.all_to_all(blocks, "tp", 0, 0, tiled=True)
+    crossed = [passed_on(blocks[k], k) for k in EXPERT_ORDER]
+    crossed = [blocks[0]] + [crossed[EXPERT_ORDER.index(k)] for k in range(1, n_tp)]
     total = combine(crossed, down, chips)
     arrived = lax.all_to_all(total, FAR, 0, 0, tiled=True)
     return finish(arrived.reshape(-1, arrived.shape[2]), place, own_residual)

time: 84.5 us -> 90.9 us (1.076); the launches traced: 84 us -> 89.1 us
  blocking collectives: 62.1 us -> 42.5 us
  waiting for transfers between devices: 6.94 us -> 21 us
  starting transfers between devices: 3.87 us -> 13.5 us
  Pallas kernels: 10.3 us -> 11.3 us
    all_to_all x2 -> x0, blocking collectives: 20.6 us -> none  [the longest x1 10.5 us: shards(): crossed = lax.all_to_all(partial, 'tp', 0, 0, tiled=True)]
    ppermute x0 -> x6, waiting for transfers between devices: none -> 13.4 us  [passed_on(): return lax.ppermute(x, 'tp', [(i, (i + k) % n_tp) for i in range(n_tp)])]
    ppermute x0 -> x6, starting transfers between devices: none -> 10.8 us  [passed_on(): return lax.ppermute(x, 'tp', [(i, (i + k) % n_tp) for i in range(n_tp)])]
    ppermute x3, starting transfers between devices: 3.35 us -> 2.23 us  [neighbour(): lax.ppermute(w, axes, [(i, i ^ flip) for i in range(lax.axis_size(axes))])]
    pallas_call x3 -> x4, Pallas kernels: 1.93 us -> 2.9 us  [the longest x1 1.29 us: tables(): pl.pallas_call(tables_kernel, name='tables', out_shape=(pltpu.VMEM((2, ch...]
  transfers between devices with their start and end apart: 6 -> 12, of which waited for: 1 -> 7; matrix products, arithmetic and copies ran while one was open for 0% -> 0% of each run, Pallas kernels for 8% -> 9%
where the time goes in v5:
time: 90.9 us; the launch traced here: 89.1 us
  blocking collectives  42.5 us (47%)
  waiting for transfers between devices  21 us (23%)
  starting transfers between devices  13.5 us (15%)
  Pallas kernels  11.3 us (12%)
    all_to_all x1, blocking collectives, shards(): lax.all_to_all(message.reshape(chips, -1, message.shape[1]), FAR, 0, 0, t...  26.6 us
    all_to_all x1, blocking collectives, shards(): arrived = lax.all_to_all(total, FAR, 0, 0, tiled=True)  15.9 us
    ppermute x6, waiting for transfers between devices, passed_on(): return lax.ppermute(x, 'tp', [(i, (i + k) % n_tp) for i in range(n_tp)])  13.4 us
    ppermute x6, starting transfers between devices, passed_on(): return lax.ppermute(x, 'tp', [(i, (i + k) % n_tp) for i in range(n_tp)])  10.8 us
    ppermute x3, waiting for transfers between devices, neighbour(): lax.ppermute(w, axes, [(i, i ^ flip) for i in range(lax.axis_size(axes))])  7.67 us
    pallas_call x1, Pallas kernels, attend(): pl.pallas_call(functools.partial(attend_kernel, chunks), name='attend', o...  5.3 us
    pallas_call x1, Pallas kernels, experts(): pl.pallas_call(functools.partial(experts_kernel, n_tp), name='experts', o...  2.27 us
    ppermute x3, starting transfers between devices, neighbour(): lax.ppermute(w, axes, [(i, i ^ flip) for i in range(lax.axis_size(axes))])  2.23 us
  transfers between devices with their start and end apart: 12, of which 7 were waited for; matrix products, arithmetic and copies ran while one was open for 0% of the time, Pallas kernels for 9%

profile of v5, /device:TPU:32, one launch (start us, length us, event | category | flops | bytes accessed | tf_op | source)
XLA Modules:
  0.0 89.1 jit_solution(5699930581039718598)
XLA Ops:
  0.0 0.5 collective-permute-start.4
  0.5 1.0 %pack.1.after.refs_6_ = bf16[64,2304]{1,0:T(8,128)(2,1)S(1)} custom-call(bf16[64,1024]{1,0:T(8,128)(2,1)} %refs_0_.1, bf16[64,1024]{1,0:T(8,128)(2,1)} %refs_1_.1, bf16[64,256]{1,0:T(8,128)(2,1)} %refs_2_.1), custom_call_target="tpu_custom_call" | custom-call | tf_op jit(solution)/shard_map/pack/pallas_call | solution.py:162
  1.5 1.8 %collective-permute-start.8 = (bf16[64,2304]{1,0:T(8,128)(2,1)S(1)}, bf16[64,2304]{1,0:T(8,128)(2,1)S(1)}, u32[]{:S(2)}, u32[]{:S(2)}) collective-permute-start(bf16[64,2304]{1,0:T(8,128)(2,1)S(1)} %pack.1.after.refs_6_), channel_id=1, source_target_pairs={{0,12},{4,8},{8,4},{12,0},{16,28},{20,24},{24,20},{28,16},{1,13},{... | collective-permute-start | bytes 884744 | tf_op jit(solution)/shard_map/ppermute | solution.py:506
  4.0 5.3 %attend.1 = (bf16[24,1024]{1,0:T(8,128)(2,1)S(1)}, bf16[1024,896]{1,0:T(8,128)(2,1)S(1)}, bf16[1024,896]{1,0:T(8,128)(2,1)S(1)}, bf16[896,1024]{1,0:T(8,128)(2,1)S(1)}) custom-call(f32[1]{0:T(128)S(6)} %copy.24.forget_bias, s32[24]{0:T(128)} %lens_hbm.1, bf16[64,2304]{1,0:T(8,128)(2,1)S(1)} %pack.1.after.refs_6_, bf16[1024,896]{1,0:T(8,128)(2,1)} %bitcast.24, ...), custom_call_target="tpu_custom_call" | custom-call | tf_op jit(solution)/shard_map/attend/pallas_call | solution.py:276
  9.3 3.1 %collective-permute-start.2 = (bf16[24,1024]{1,0:T(8,128)(2,1)S(1)}, bf16[24,1024]{1,0:T(8,128)(2,1)S(1)}, u32[]{:S(2)}, u32[]{:S(2)}) collective-permute-start(bf16[24,1024]{1,0:T(8,128)(2,1)S(1)} %get-tuple-element.18.after.refs_0_), channel_id=1, source_target_pairs={{0,2},{1,3},{2,0},{3,1},{4,6},{5,7},{6,4},{7,5},{8,10},{9,11},{10,... | collective-permute-start | bytes 147464 | tf_op jit(solution)/shard_map/ppermute | solution.py:509
  12.4 2.6 %collective-permute-done.2.refs_3_ = bf16[24,1024]{1,0:T(8,128)(2,1)S(1)} collective-permute-done((bf16[24,1024]{1,0:T(8,128)(2,1)S(1)}, bf16[24,1024]{1,0:T(8,128)(2,1)S(1)}, u32[]{:S(2)}, u32[]{:S(2)}) %collective-permute-start.2) | collective-permute-done | bytes 49184 | tf_op jit(solution)/shard_map/ppermute | solution.py:509
  15.0 2.8 %collective-permute-start.1 = (bf16[24,1024]{1,0:T(8,128)(2,1)S(1)}, bf16[24,1024]{1,0:T(8,128)(2,1)S(1)}, u32[]{:S(2)}, u32[]{:S(2)}) collective-permute-start(bf16[24,1024]{1,0:T(8,128)(2,1)S(1)} %get-tuple-element.18.after.refs_0_), channel_id=1, source_target_pairs={{0,3},{1,0},{2,1},{3,2},{4,7},{5,4},{6,5},{7,6},{8,11},{9,8},{10,9... | collective-permute-start | bytes 147464 | tf_op jit(solution)/shard_map/ppermute | solution.py:509
  17.7 1.8 %collective-permute-done.1.refs_2_ = bf16[24,1024]{1,0:T(8,128)(2,1)S(1)} collective-permute-done((bf16[24,1024]{1,0:T(8,128)(2,1)S(1)}, bf16[24,1024]{1,0:T(8,128)(2,1)S(1)}, u32[]{:S(2)}, u32[]{:S(2)}) %collective-permute-start.1) | collective-permute-done | bytes 49184 | tf_op jit(solution)/shard_map/ppermute | solution.py:509
  19.5 1.1 %collective-permute-start = (bf16[24,1024]{1,0:T(8,128)(2,1)S(1)}, bf16[24,1024]{1,0:T(8,128)(2,1)S(1)}, u32[]{:S(2)}, u32[]{:S(2)}) collective-permute-start(bf16[24,1024]{1,0:T(8,128)(2,1)S(1)} %get-tuple-element.18.after.refs_0_), channel_id=1, source_target_pairs={{0,1},{1,2},{2,3},{3,0},{4,5},{5,6},{6,7},{7,4},{8,9},{9,10},{10,1... | collective-permute-start | bytes 147464 | tf_op jit(solution)/shard_map/ppermute | solution.py:509
  20.5 4.5 %collective-permute-done.refs_1_ = bf16[24,1024]{1,0:T(8,128)(2,1)S(1)} collective-permute-done((bf16[24,1024]{1,0:T(8,128)(2,1)S(1)}, bf16[24,1024]{1,0:T(8,128)(2,1)S(1)}, u32[]{:S(2)}, u32[]{:S(2)}) %collective-permute-start) | collective-permute-done | bytes 49184 | tf_op jit(solution)/shard_map/ppermute | solution.py:509
  25.1 0.5 collective-permute-start.6
  25.5 1.3 %tables.1 = (bf16[2,256,96]{2,1,0:T(8,128)(2,1)S(1)}, bf16[3,24,256]{2,1,0:T(8,128)(2,1)S(1)}) custom-call(s32[2,1536]{1,0:T(2,128)} %bitcast.31, f32[2,1536]{1,0:T(2,128)} %bitcast.32, bf16[24,1024]{1,0:T(8,128)(2,1)S(1)} %get-tuple-element.18.after.refs_0_), custom_call_target="tpu_custom_call" | custom-call | tf_op jit(solution)/shard_map/tables/pallas_call | solution.py:130
  26.9 7.7 %collective-permute-done.6.refs_10_.refs_7_ = bf16[64,2304]{1,0:T(8,128)(2,1)S(1)} collective-permute-done((bf16[64,2304]{1,0:T(8,128)(2,1)S(1)}, bf16[64,2304]{1,0:T(8,128)(2,1)S(1)}, u32[]{:S(2)}, u32[]{:S(2)}) %collective-permute-start.6) | collective-permute-done | bytes 294944 | tf_op jit(solution)/shard_map/ppermute | solution.py:506
  34.6 0.4 send.1
  34.9 26.6 %all_to_all.10 = bf16[32,8,896]{2,1,0:T(8,128)(2,1)S(1)} all-to-all(bf16[32,8,896]{2,1,0:T(8,128)(2,1)S(1)} %bitcast.19), channel_id=1, replica_groups=mesh['ep_0'=8,'ep_1'=4,'ep_2'=2,'tp'=4] {'ep_0','ep_1'}, dimensions={0} | all-to-all | bytes 917504 | tf_op jit(solution)/shard_map/all_to_all | solution.py:535
  61.6 2.3 %experts.1 = (bf16[224,256]{1,0:T(8,128)(2,1)S(1)}, bf16[224,256]{1,0:T(8,128)(2,1)S(1)}, bf16[224,256]{1,0:T(8,128)(2,1)S(1)}, bf16[224,256]{1,0:T(8,128)(2,1)S(1)}, bf16[256,256]{1,0:T(8,128)(2,1)S(1)}) custom-call(bf16[256,896]{1,0:T(8,128)(2,1)S(1)} %bitcast.17, bf16[8,128]{1,0:T(8,128)(2,1)S(1)} %bitcast.21, ...), custom_call_target="tpu_custom_call" | custom-call | tf_op jit(solution)/shard_map/experts/pallas_call | solution.py:402
  63.9 3.5 %collective-permute-start.10 = (bf16[224,256]{1,0:T(8,128)(2,1)S(1)}, bf16[224,256]{1,0:T(8,128)(2,1)S(1)}, u32[]{:S(2)}, u32[]{:S(2)}) collective-permute-start(bf16[224,256]{1,0:T(8,128)(2,1)S(1)} %get-tuple-element.26), channel_id=1, source_target_pairs={{0,2},{1,3},{2,0},{3,1},{4,6},{5,7},{6,4},{7,5},{8,10},{9,11},{10,... | collective-permute-start | bytes 344072 | tf_op jit(solution)/shard_map/ppermute | solution.py:509
  67.4 0.3 collective-permute-start.11
  67.7 2.2 %collective-permute-done.9.refs_1_ = bf16[224,256]{1,0:T(8,128)(2,1)S(1)} collective-permute-done((bf16[224,256]{1,0:T(8,128)(2,1)S(1)}, bf16[224,256]{1,0:T(8,128)(2,1)S(1)}, u32[]{:S(2)}, u32[]{:S(2)}) %collective-permute-start.9) | collective-permute-done | bytes 114720 | tf_op jit(solution)/shard_map/ppermute | solution.py:509
  69.9 1.5 %collective-permute-done.10.refs_2_ = bf16[224,256]{1,0:T(8,128)(2,1)S(1)} collective-permute-done((bf16[224,256]{1,0:T(8,128)(2,1)S(1)}, bf16[224,256]{1,0:T(8,128)(2,1)S(1)}, u32[]{:S(2)}, u32[]{:S(2)}) %collective-permute-start.10) | collective-permute-done | bytes 114720 | tf_op jit(solution)/shard_map/ppermute | solution.py:509
  71.4 0.8 collective-permute-done.11.refs_3_
  72.2 0.3 combine.1
  72.5 15.9 %all_to_all.11 = bf16[32,8,512]{2,1,0:T(8,128)(2,1)S(1)} all-to-all(bf16[32,8,512]{2,1,0:T(8,128)(2,1)S(1)} %combine.1), channel_id=1, replica_groups=mesh['ep_0'=8,'ep_1'=4,'ep_2'=2,'tp'=4] {'ep_0','ep_1'}, dimensions={0} | all-to-all | bytes 524288 | tf_op jit(solution)/shard_map/all_to_all | solution.py:548
  88.3 0.8 finish.1
  (15 shorter events, 0.1 us)
Async XLA Ops:
  0.0 34.5 %collective-permute-start.3 = (bf16[1024,896]{1,0:T(8,128)(2,1)}, bf16[1024,896]{1,0:T(8,128)(2,1)S(1)}, u32[]{:S(2)}, u32[]{:S(2)}) collective-permute-start(bf16[1024,896]{1,0:T(8,128)(2,1)} %bitcast.23), channel_id=1, source_target_pairs={{0,4},{4,0},{1,5},{5,1},{2,6},{6,2},{3,7},{7,3},{8,12},{12,8},{9,1... | collective-permute-start | bytes 5505032 | tf_op jit(solution)/shard_map/ppermute | solution.py:502
  0.0 34.5 %collective-permute-start.4 = (bf16[1024,896]{1,0:T(8,128)(2,1)}, bf16[1024,896]{1,0:T(8,128)(2,1)S(1)}, u32[]{:S(2)}, u32[]{:S(2)}) collective-permute-start(bf16[1024,896]{1,0:T(8,128)(2,1)} %bitcast.25), channel_id=1, source_target_pairs={{0,4},{4,0},{1,5},{5,1},{2,6},{6,2},{3,7},{7,3},{8,12},{12,8},{9,1... | collective-permute-start | bytes 5505032 | tf_op jit(solution)/shard_map/ppermute | solution.py:502
  0.5 34.0 %collective-permute-start.5 = (bf16[896,1024]{1,0:T(8,128)(2,1)}, bf16[896,1024]{1,0:T(8,128)(2,1)S(1)}, u32[]{:S(2)}, u32[]{:S(2)}) collective-permute-start(bf16[896,1024]{1,0:T(8,128)(2,1)} %bitcast.27), channel_id=1, source_target_pairs={{0,4},{4,0},{1,5},{5,1},{2,6},{6,2},{3,7},{7,3},{8,12},{12,8},{9,1... | collective-permute-start | bytes 5505032 | tf_op jit(solution)/shard_map/ppermute | solution.py:502
  1.5 23.6 %collective-permute-start.8 = (bf16[64,2304]{1,0:T(8,128)(2,1)S(1)}, bf16[64,2304]{1,0:T(8,128)(2,1)S(1)}, u32[]{:S(2)}, u32[]{:S(2)}) collective-permute-start(bf16[64,2304]{1,0:T(8,128)(2,1)S(1)} %pack.1.after.refs_6_), channel_id=1, source_target_pairs={{0,12},{4,8},{8,4},{12,0},{16,28},{20,24},{24,20},{28,16},{1,13},{... | collective-permute-start | bytes 884744 | tf_op jit(solution)/shard_map/ppermute | solution.py:506
  3.9 30.6 %copy-start = (bf16[24,1024]{1,0:T(8,128)(2,1)S(1)}, bf16[24,1024]{1,0:T(8,128)(2,1)}, u32[]{:S(2)}) copy-start(bf16[24,1024]{1,0:T(8,128)(2,1)} %refs_4_.1) | copy-start | bytes 147460
  4.0 30.6 %copy-start.1 = (f32[1024]{0:T(1024)S(1)}, f32[1024]{0:T(1024)}, u32[]{:S(2)}) copy-start(f32[1024]{0:T(1024)} %param.36) | copy-start | bytes 12292
  9.3 5.7 %collective-permute-start.2 = (bf16[24,1024]{1,0:T(8,128)(2,1)S(1)}, bf16[24,1024]{1,0:T(8,128)(2,1)S(1)}, u32[]{:S(2)}, u32[]{:S(2)}) collective-permute-start(bf16[24,1024]{1,0:T(8,128)(2,1)S(1)} %get-tuple-element.18.after.refs_0_), channel_id=1, source_target_pairs={{0,2},{1,3},{2,0},{3,1},{4,6},{5,7},{6,4},{7,5},{8,10},{9,11},{10,... | collective-permute-start | bytes 147464 | tf_op jit(solution)/shard_map/ppermute | solution.py:509
  15.0 4.5 %collective-permute-start.1 = (bf16[24,1024]{1,0:T(8,128)(2,1)S(1)}, bf16[24,1024]{1,0:T(8,128)(2,1)S(1)}, u32[]{:S(2)}, u32[]{:S(2)}) collective-permute-start(bf16[24,1024]{1,0:T(8,128)(2,1)S(1)} %get-tuple-element.18.after.refs_0_), channel_id=1, source_target_pairs={{0,3},{1,0},{2,1},{3,2},{4,7},{5,4},{6,5},{7,6},{8,11},{9,8},{10,9... | collective-permute-start | bytes 147464 | tf_op jit(solution)/shard_map/ppermute | solution.py:509
  19.5 5.6 %collective-permute-start = (bf16[24,1024]{1,0:T(8,128)(2,1)S(1)}, bf16[24,1024]{1,0:T(8,128)(2,1)S(1)}, u32[]{:S(2)}, u32[]{:S(2)}) collective-permute-start(bf16[24,1024]{1,0:T(8,128)(2,1)S(1)} %get-tuple-element.18.after.refs_0_), channel_id=1, source_target_pairs={{0,1},{1,2},{2,3},{3,0},{4,5},{5,6},{6,7},{7,4},{8,9},{9,10},{10,1... | collective-permute-start | bytes 147464 | tf_op jit(solution)/shard_map/ppermute | solution.py:509
  25.1 1.8 %collective-permute-start.7 = (bf16[64,2304]{1,0:T(8,128)(2,1)S(1)}, bf16[64,2304]{1,0:T(8,128)(2,1)S(1)}, u32[]{:S(2)}, u32[]{:S(2)}) collective-permute-start(bf16[64,2304]{1,0:T(8,128)(2,1)S(1)} %pack.1.after.refs_6_), channel_id=1, source_target_pairs={{0,4},{4,0},{8,12},{12,8},{16,20},{20,16},{24,28},{28,24},{1,5},{5... | collective-permute-start | bytes 884744 | tf_op jit(solution)/shard_map/ppermute | solution.py:506
  25.1 9.4 %collective-permute-start.6 = (bf16[64,2304]{1,0:T(8,128)(2,1)S(1)}, bf16[64,2304]{1,0:T(8,128)(2,1)S(1)}, u32[]{:S(2)}, u32[]{:S(2)}) collective-permute-start(bf16[64,2304]{1,0:T(8,128)(2,1)S(1)} %pack.1.after.refs_6_), channel_id=1, source_target_pairs={{0,8},{4,12},{8,0},{12,4},{16,24},{20,28},{24,16},{28,20},{1,9},{5... | collective-permute-start | bytes 884744 | tf_op jit(solution)/shard_map/ppermute | solution.py:506
  34.5 27.0 %copy-start.2 = (bf16[1024]{0:T(1024)(128)(2,1)S(1)}, bf16[1024]{0:T(1024)(128)(2,1)}, u32[]{:S(2)}) copy-start(bf16[1024]{0:T(1024)(128)(2,1)} %param.42) | copy-start | bytes 6148
  63.8 6.1 %collective-permute-start.9 = (bf16[224,256]{1,0:T(8,128)(2,1)S(1)}, bf16[224,256]{1,0:T(8,128)(2,1)S(1)}, u32[]{:S(2)}, u32[]{:S(2)}) collective-permute-start(bf16[224,256]{1,0:T(8,128)(2,1)S(1)} %get-tuple-element.25), channel_id=1, source_target_pairs={{0,1},{1,2},{2,3},{3,0},{4,5},{5,6},{6,7},{7,4},{8,9},{9,10},{10,1... | collective-permute-start | bytes 344072 | tf_op jit(solution)/shard_map/ppermute | solution.py:509
  63.9 7.5 %collective-permute-start.10 = (bf16[224,256]{1,0:T(8,128)(2,1)S(1)}, bf16[224,256]{1,0:T(8,128)(2,1)S(1)}, u32[]{:S(2)}, u32[]{:S(2)}) collective-permute-start(bf16[224,256]{1,0:T(8,128)(2,1)S(1)} %get-tuple-element.26), channel_id=1, source_target_pairs={{0,2},{1,3},{2,0},{3,1},{4,6},{5,7},{6,4},{7,5},{8,10},{9,11},{10,... | collective-permute-start | bytes 344072 | tf_op jit(solution)/shard_map/ppermute | solution.py:509
  67.4 4.8 %collective-permute-start.11 = (bf16[224,256]{1,0:T(8,128)(2,1)S(1)}, bf16[224,256]{1,0:T(8,128)(2,1)S(1)}, u32[]{:S(2)}, u32[]{:S(2)}) collective-permute-start(bf16[224,256]{1,0:T(8,128)(2,1)S(1)} %get-tuple-element.27), channel_id=1, source_target_pairs={{0,3},{1,0},{2,1},{3,2},{4,7},{5,4},{6,5},{7,6},{8,11},{9,8},{10,9... | collective-permute-start | bytes 344072 | tf_op jit(solution)/shard_map/ppermute | solution.py:509

commit v6 on v5

--- a/solution.py
+++ b/solution.py
@@ -16,8 +16,8 @@
 CAP = 2
 LANES = 128
 MIB = 1 << 20
-HEADS_ORDER = (1, 3, 2)
-EXPERT_ORDER = (2, 1, 3)
+HEADS_ORDER = (2, 1, 3)
+EXPERT_ORDER = (1, 3, 2)
 ANY = pl.BlockSpec(memory_space=pl.ANY)
 IN_VMEM = pl.BlockSpec(memory_space=pltpu.VMEM)
 IN_SMEM = pl.BlockSpec(memory_space=pltpu.SMEM)
@@ -263,7 +263,7 @@
 
 
 def attend(lens, forget_bias, after, ahead, *arrays):
-    chunks = 3
+    chunks = 4
     tok, wq, qg, cache = arrays[0], arrays[2], arrays[6], arrays[10]
     seqs, slots, pair = cache.shape
     heads = wq.shape[1] // qg.shape[1]

time: 90.9 us -> 90.9 us (level)
  starting transfers between devices: 13.5 us -> 11.6 us
  waiting for transfers between devices: 21 us -> 22.9 us
    ppermute x6, starting transfers between devices: 10.8 us -> 8.9 us  [passed_on(): return lax.ppermute(x, 'tp', [(i, (i + k) % n_tp) for i in range(n_tp)])]
    ppermute x6, waiting for transfers between devices: 13.4 us -> 15.2 us  [passed_on(): return lax.ppermute(x, 'tp', [(i, (i + k) % n_tp) for i in range(n_tp)])]
where the time goes in v6:
time: 90.9 us; the launch traced here: 89.1 us
  blocking collectives  42.5 us (47%)
  waiting for transfers between devices  22.9 us (25%)
  starting transfers between devices  11.6 us (13%)
  Pallas kernels  11.3 us (12%)
    all_to_all x1, blocking collectives, shards(): lax.all_to_all(message.reshape(chips, -1, message.shape[1]), FAR, 0, 0, t...  26.6 us
    all_to_all x1, blocking collectives, shards(): arrived = lax.all_to_all(total, FAR, 0, 0, tiled=True)  15.9 us
    ppermute x6, waiting for transfers between devices, passed_on(): return lax.ppermute(x, 'tp', [(i, (i + k) % n_tp) for i in range(n_tp)])  15.2 us
    ppermute x6, starting transfers between devices, passed_on(): return lax.ppermute(x, 'tp', [(i, (i + k) % n_tp) for i in range(n_tp)])  8.9 us
    ppermute x3, waiting for transfers between devices, neighbour(): lax.ppermute(w, axes, [(i, i ^ flip) for i in range(lax.axis_size(axes))])  7.67 us
    pallas_call x1, Pallas kernels, attend(): pl.pallas_call(functools.partial(attend_kernel, chunks), name='attend', o...  5.31 us
    pallas_call x1, Pallas kernels, experts(): pl.pallas_call(functools.partial(experts_kernel, n_tp), name='experts', o...  2.27 us
    ppermute x3, starting transfers between devices, neighbour(): lax.ppermute(w, axes, [(i, i ^ flip) for i in range(lax.axis_size(axes))])  2.23 us
  transfers between devices with their start and end apart: 12, of which 7 were waited for; matrix products, arithmetic and copies ran while one was open for 0% of the time, Pallas kernels for 9%

profile of v6, /device:TPU:32, one launch (start us, length us, event | category | flops | bytes accessed | tf_op | source)
XLA Modules:
  0.0 89.1 jit_solution(3427074180119114298)
XLA Ops:
  0.0 0.5 collective-permute-start.4
  0.5 1.0 %pack.1.after.refs_6_ = bf16[64,2304]{1,0:T(8,128)(2,1)S(1)} custom-call(bf16[64,1024]{1,0:T(8,128)(2,1)} %refs_0_.1, bf16[64,1024]{1,0:T(8,128)(2,1)} %refs_1_.1, bf16[64,256]{1,0:T(8,128)(2,1)} %refs_2_.1), custom_call_target="tpu_custom_call" | custom-call | tf_op jit(solution)/shard_map/pack/pallas_call | solution.py:162
  1.5 1.8 %collective-permute-start.8 = (bf16[64,2304]{1,0:T(8,128)(2,1)S(1)}, bf16[64,2304]{1,0:T(8,128)(2,1)S(1)}, u32[]{:S(2)}, u32[]{:S(2)}) collective-permute-start(bf16[64,2304]{1,0:T(8,128)(2,1)S(1)} %pack.1.after.refs_6_), channel_id=1, source_target_pairs={{0,12},{4,8},{8,4},{12,0},{16,28},{20,24},{24,20},{28,16},{1,13},{... | collective-permute-start | bytes 884744 | tf_op jit(solution)/shard_map/ppermute | solution.py:506
  4.0 5.3 %attend.1 = (bf16[24,1024]{1,0:T(8,128)(2,1)S(1)}, bf16[1024,896]{1,0:T(8,128)(2,1)S(1)}, bf16[1024,896]{1,0:T(8,128)(2,1)S(1)}, bf16[896,1024]{1,0:T(8,128)(2,1)S(1)}) custom-call(f32[1]{0:T(128)S(6)} %copy.24.forget_bias, s32[24]{0:T(128)} %lens_hbm.1, bf16[64,2304]{1,0:T(8,128)(2,1)S(1)} %pack.1.after.refs_6_, bf16[1024,896]{1,0:T(8,128)(2,1)} %bitcast.24, ...), custom_call_target="tpu_custom_call" | custom-call | tf_op jit(solution)/shard_map/attend/pallas_call | solution.py:276
  9.3 2.8 %collective-permute-start.2 = (bf16[24,1024]{1,0:T(8,128)(2,1)S(1)}, bf16[24,1024]{1,0:T(8,128)(2,1)S(1)}, u32[]{:S(2)}, u32[]{:S(2)}) collective-permute-start(bf16[24,1024]{1,0:T(8,128)(2,1)S(1)} %get-tuple-element.18.after.refs_0_), channel_id=1, source_target_pairs={{0,3},{1,0},{2,1},{3,2},{4,7},{5,4},{6,5},{7,6},{8,11},{9,8},{10,9... | collective-permute-start | bytes 147464 | tf_op jit(solution)/shard_map/ppermute | solution.py:509
  12.1 1.8 %collective-permute-done.2.refs_3_ = bf16[24,1024]{1,0:T(8,128)(2,1)S(1)} collective-permute-done((bf16[24,1024]{1,0:T(8,128)(2,1)S(1)}, bf16[24,1024]{1,0:T(8,128)(2,1)S(1)}, u32[]{:S(2)}, u32[]{:S(2)}) %collective-permute-start.2) | collective-permute-done | bytes 49184 | tf_op jit(solution)/shard_map/ppermute | solution.py:509
  13.9 1.1 %collective-permute-start.1 = (bf16[24,1024]{1,0:T(8,128)(2,1)S(1)}, bf16[24,1024]{1,0:T(8,128)(2,1)S(1)}, u32[]{:S(2)}, u32[]{:S(2)}) collective-permute-start(bf16[24,1024]{1,0:T(8,128)(2,1)S(1)} %get-tuple-element.18.after.refs_0_), channel_id=1, source_target_pairs={{0,1},{1,2},{2,3},{3,0},{4,5},{5,6},{6,7},{7,4},{8,9},{9,10},{10,1... | collective-permute-start | bytes 147464 | tf_op jit(solution)/shard_map/ppermute | solution.py:509
  14.9 4.5 %collective-permute-done.1.refs_2_ = bf16[24,1024]{1,0:T(8,128)(2,1)S(1)} collective-permute-done((bf16[24,1024]{1,0:T(8,128)(2,1)S(1)}, bf16[24,1024]{1,0:T(8,128)(2,1)S(1)}, u32[]{:S(2)}, u32[]{:S(2)}) %collective-permute-start.1) | collective-permute-done | bytes 49184 | tf_op jit(solution)/shard_map/ppermute | solution.py:509
  19.5 1.1 %collective-permute-start = (bf16[24,1024]{1,0:T(8,128)(2,1)S(1)}, bf16[24,1024]{1,0:T(8,128)(2,1)S(1)}, u32[]{:S(2)}, u32[]{:S(2)}) collective-permute-start(bf16[24,1024]{1,0:T(8,128)(2,1)S(1)} %get-tuple-element.18.after.refs_0_), channel_id=1, source_target_pairs={{0,2},{1,3},{2,0},{3,1},{4,6},{5,7},{6,4},{7,5},{8,10},{9,11},{10,... | collective-permute-start | bytes 147464 | tf_op jit(solution)/shard_map/ppermute | solution.py:509
  20.6 4.4 %collective-permute-done.refs_1_ = bf16[24,1024]{1,0:T(8,128)(2,1)S(1)} collective-permute-done((bf16[24,1024]{1,0:T(8,128)(2,1)S(1)}, bf16[24,1024]{1,0:T(8,128)(2,1)S(1)}, u32[]{:S(2)}, u32[]{:S(2)}) %collective-permute-start) | collective-permute-done | bytes 49184 | tf_op jit(solution)/shard_map/ppermute | solution.py:509
  25.1 0.5 collective-permute-start.6
  25.5 1.3 %tables.1 = (bf16[2,256,96]{2,1,0:T(8,128)(2,1)S(1)}, bf16[3,24,256]{2,1,0:T(8,128)(2,1)S(1)}) custom-call(s32[2,1536]{1,0:T(2,128)} %bitcast.31, f32[2,1536]{1,0:T(2,128)} %bitcast.32, bf16[24,1024]{1,0:T(8,128)(2,1)S(1)} %get-tuple-element.18.after.refs_0_), custom_call_target="tpu_custom_call" | custom-call | tf_op jit(solution)/shard_map/tables/pallas_call | solution.py:130
  26.9 7.7 %collective-permute-done.6.refs_10_.refs_7_ = bf16[64,2304]{1,0:T(8,128)(2,1)S(1)} collective-permute-done((bf16[64,2304]{1,0:T(8,128)(2,1)S(1)}, bf16[64,2304]{1,0:T(8,128)(2,1)S(1)}, u32[]{:S(2)}, u32[]{:S(2)}) %collective-permute-start.6) | collective-permute-done | bytes 294944 | tf_op jit(solution)/shard_map/ppermute | solution.py:506
  34.6 0.4 send.1
  34.9 26.6 %all_to_all.10 = bf16[32,8,896]{2,1,0:T(8,128)(2,1)S(1)} all-to-all(bf16[32,8,896]{2,1,0:T(8,128)(2,1)S(1)} %bitcast.19), channel_id=1, replica_groups=mesh['ep_0'=8,'ep_1'=4,'ep_2'=2,'tp'=4] {'ep_0','ep_1'}, dimensions={0} | all-to-all | bytes 917504 | tf_op jit(solution)/shard_map/all_to_all | solution.py:535
  61.6 2.3 %experts.1 = (bf16[224,256]{1,0:T(8,128)(2,1)S(1)}, bf16[224,256]{1,0:T(8,128)(2,1)S(1)}, bf16[224,256]{1,0:T(8,128)(2,1)S(1)}, bf16[224,256]{1,0:T(8,128)(2,1)S(1)}, bf16[256,256]{1,0:T(8,128)(2,1)S(1)}) custom-call(bf16[256,896]{1,0:T(8,128)(2,1)S(1)} %bitcast.17, bf16[8,128]{1,0:T(8,128)(2,1)S(1)} %bitcast.21, ...), custom_call_target="tpu_custom_call" | custom-call | tf_op jit(solution)/shard_map/experts/pallas_call | solution.py:402
  63.9 3.5 %collective-permute-start.10 = (bf16[224,256]{1,0:T(8,128)(2,1)S(1)}, bf16[224,256]{1,0:T(8,128)(2,1)S(1)}, u32[]{:S(2)}, u32[]{:S(2)}) collective-permute-start(bf16[224,256]{1,0:T(8,128)(2,1)S(1)} %get-tuple-element.26), channel_id=1, source_target_pairs={{0,2},{1,3},{2,0},{3,1},{4,6},{5,7},{6,4},{7,5},{8,10},{9,11},{10,... | collective-permute-start | bytes 344072 | tf_op jit(solution)/shard_map/ppermute | solution.py:509
  67.4 0.3 collective-permute-start.11
  67.7 2.2 %collective-permute-done.9.refs_1_ = bf16[224,256]{1,0:T(8,128)(2,1)S(1)} collective-permute-done((bf16[224,256]{1,0:T(8,128)(2,1)S(1)}, bf16[224,256]{1,0:T(8,128)(2,1)S(1)}, u32[]{:S(2)}, u32[]{:S(2)}) %collective-permute-start.9) | collective-permute-done | bytes 114720 | tf_op jit(solution)/shard_map/ppermute | solution.py:509
  69.9 1.5 %collective-permute-done.10.refs_2_ = bf16[224,256]{1,0:T(8,128)(2,1)S(1)} collective-permute-done((bf16[224,256]{1,0:T(8,128)(2,1)S(1)}, bf16[224,256]{1,0:T(8,128)(2,1)S(1)}, u32[]{:S(2)}, u32[]{:S(2)}) %collective-permute-start.10) | collective-permute-done | bytes 114720 | tf_op jit(solution)/shard_map/ppermute | solution.py:509
  71.4 0.8 collective-permute-done.11.refs_3_
  72.2 0.3 combine.1
  72.5 15.9 %all_to_all.11 = bf16[32,8,512]{2,1,0:T(8,128)(2,1)S(1)} all-to-all(bf16[32,8,512]{2,1,0:T(8,128)(2,1)S(1)} %combine.1), channel_id=1, replica_groups=mesh['ep_0'=8,'ep_1'=4,'ep_2'=2,'tp'=4] {'ep_0','ep_1'}, dimensions={0} | all-to-all | bytes 524288 | tf_op jit(solution)/shard_map/all_to_all | solution.py:548
  88.3 0.8 finish.1
  (15 shorter events, 0.1 us)
Async XLA Ops:
  0.0 34.5 %collective-permute-start.3 = (bf16[1024,896]{1,0:T(8,128)(2,1)}, bf16[1024,896]{1,0:T(8,128)(2,1)S(1)}, u32[]{:S(2)}, u32[]{:S(2)}) collective-permute-start(bf16[1024,896]{1,0:T(8,128)(2,1)} %bitcast.23), channel_id=1, source_target_pairs={{0,4},{4,0},{1,5},{5,1},{2,6},{6,2},{3,7},{7,3},{8,12},{12,8},{9,1... | collective-permute-start | bytes 5505032 | tf_op jit(solution)/shard_map/ppermute | solution.py:502
  0.0 34.5 %collective-permute-start.4 = (bf16[1024,896]{1,0:T(8,128)(2,1)}, bf16[1024,896]{1,0:T(8,128)(2,1)S(1)}, u32[]{:S(2)}, u32[]{:S(2)}) collective-permute-start(bf16[1024,896]{1,0:T(8,128)(2,1)} %bitcast.25), channel_id=1, source_target_pairs={{0,4},{4,0},{1,5},{5,1},{2,6},{6,2},{3,7},{7,3},{8,12},{12,8},{9,1... | collective-permute-start | bytes 5505032 | tf_op jit(solution)/shard_map/ppermute | solution.py:502
  0.5 34.0 %collective-permute-start.5 = (bf16[896,1024]{1,0:T(8,128)(2,1)}, bf16[896,1024]{1,0:T(8,128)(2,1)S(1)}, u32[]{:S(2)}, u32[]{:S(2)}) collective-permute-start(bf16[896,1024]{1,0:T(8,128)(2,1)} %bitcast.27), channel_id=1, source_target_pairs={{0,4},{4,0},{1,5},{5,1},{2,6},{6,2},{3,7},{7,3},{8,12},{12,8},{9,1... | collective-permute-start | bytes 5505032 | tf_op jit(solution)/shard_map/ppermute | solution.py:502
  1.5 23.6 %collective-permute-start.8 = (bf16[64,2304]{1,0:T(8,128)(2,1)S(1)}, bf16[64,2304]{1,0:T(8,128)(2,1)S(1)}, u32[]{:S(2)}, u32[]{:S(2)}) collective-permute-start(bf16[64,2304]{1,0:T(8,128)(2,1)S(1)} %pack.1.after.refs_6_), channel_id=1, source_target_pairs={{0,12},{4,8},{8,4},{12,0},{16,28},{20,24},{24,20},{28,16},{1,13},{... | collective-permute-start | bytes 884744 | tf_op jit(solution)/shard_map/ppermute | solution.py:506
  3.9 30.6 %copy-start = (bf16[24,1024]{1,0:T(8,128)(2,1)S(1)}, bf16[24,1024]{1,0:T(8,128)(2,1)}, u32[]{:S(2)}) copy-start(bf16[24,1024]{1,0:T(8,128)(2,1)} %refs_4_.1) | copy-start | bytes 147460
  4.0 30.6 %copy-start.1 = (f32[1024]{0:T(1024)S(1)}, f32[1024]{0:T(1024)}, u32[]{:S(2)}) copy-start(f32[1024]{0:T(1024)} %param.36) | copy-start | bytes 12292
  9.3 4.6 %collective-permute-start.2 = (bf16[24,1024]{1,0:T(8,128)(2,1)S(1)}, bf16[24,1024]{1,0:T(8,128)(2,1)S(1)}, u32[]{:S(2)}, u32[]{:S(2)}) collective-permute-start(bf16[24,1024]{1,0:T(8,128)(2,1)S(1)} %get-tuple-element.18.after.refs_0_), channel_id=1, source_target_pairs={{0,3},{1,0},{2,1},{3,2},{4,7},{5,4},{6,5},{7,6},{8,11},{9,8},{10,9... | collective-permute-start | bytes 147464 | tf_op jit(solution)/shard_map/ppermute | solution.py:509
  13.9 5.6 %collective-permute-start.1 = (bf16[24,1024]{1,0:T(8,128)(2,1)S(1)}, bf16[24,1024]{1,0:T(8,128)(2,1)S(1)}, u32[]{:S(2)}, u32[]{:S(2)}) collective-permute-start(bf16[24,1024]{1,0:T(8,128)(2,1)S(1)} %get-tuple-element.18.after.refs_0_), channel_id=1, source_target_pairs={{0,1},{1,2},{2,3},{3,0},{4,5},{5,6},{6,7},{7,4},{8,9},{9,10},{10,1... | collective-permute-start | bytes 147464 | tf_op jit(solution)/shard_map/ppermute | solution.py:509
  19.5 5.6 %collective-permute-start = (bf16[24,1024]{1,0:T(8,128)(2,1)S(1)}, bf16[24,1024]{1,0:T(8,128)(2,1)S(1)}, u32[]{:S(2)}, u32[]{:S(2)}) collective-permute-start(bf16[24,1024]{1,0:T(8,128)(2,1)S(1)} %get-tuple-element.18.after.refs_0_), channel_id=1, source_target_pairs={{0,2},{1,3},{2,0},{3,1},{4,6},{5,7},{6,4},{7,5},{8,10},{9,11},{10,... | collective-permute-start | bytes 147464 | tf_op jit(solution)/shard_map/ppermute | solution.py:509
  25.1 1.8 %collective-permute-start.7 = (bf16[64,2304]{1,0:T(8,128)(2,1)S(1)}, bf16[64,2304]{1,0:T(8,128)(2,1)S(1)}, u32[]{:S(2)}, u32[]{:S(2)}) collective-permute-start(bf16[64,2304]{1,0:T(8,128)(2,1)S(1)} %pack.1.after.refs_6_), channel_id=1, source_target_pairs={{0,4},{4,0},{8,12},{12,8},{16,20},{20,16},{24,28},{28,24},{1,5},{5... | collective-permute-start | bytes 884744 | tf_op jit(solution)/shard_map/ppermute | solution.py:506
  25.1 9.4 %collective-permute-start.6 = (bf16[64,2304]{1,0:T(8,128)(2,1)S(1)}, bf16[64,2304]{1,0:T(8,128)(2,1)S(1)}, u32[]{:S(2)}, u32[]{:S(2)}) collective-permute-start(bf16[64,2304]{1,0:T(8,128)(2,1)S(1)} %pack.1.after.refs_6_), channel_id=1, source_target_pairs={{0,8},{4,12},{8,0},{12,4},{16,24},{20,28},{24,16},{28,20},{1,9},{5... | collective-permute-start | bytes 884744 | tf_op jit(solution)/shard_map/ppermute | solution.py:506
  34.5 27.0 %copy-start.2 = (bf16[1024]{0:T(1024)(128)(2,1)S(1)}, bf16[1024]{0:T(1024)(128)(2,1)}, u32[]{:S(2)}) copy-start(bf16[1024]{0:T(1024)(128)(2,1)} %param.42) | copy-start | bytes 6148
  63.8 6.1 %collective-permute-start.9 = (bf16[224,256]{1,0:T(8,128)(2,1)S(1)}, bf16[224,256]{1,0:T(8,128)(2,1)S(1)}, u32[]{:S(2)}, u32[]{:S(2)}) collective-permute-start(bf16[224,256]{1,0:T(8,128)(2,1)S(1)} %get-tuple-element.25), channel_id=1, source_target_pairs={{0,1},{1,2},{2,3},{3,0},{4,5},{5,6},{6,7},{7,4},{8,9},{9,10},{10,1... | collective-permute-start | bytes 344072 | tf_op jit(solution)/shard_map/ppermute | solution.py:509
  63.9 7.5 %collective-permute-start.10 = (bf16[224,256]{1,0:T(8,128)(2,1)S(1)}, bf16[224,256]{1,0:T(8,128)(2,1)S(1)}, u32[]{:S(2)}, u32[]{:S(2)}) collective-permute-start(bf16[224,256]{1,0:T(8,128)(2,1)S(1)} %get-tuple-element.26), channel_id=1, source_target_pairs={{0,2},{1,3},{2,0},{3,1},{4,6},{5,7},{6,4},{7,5},{8,10},{9,11},{10,... | collective-permute-start | bytes 344072 | tf_op jit(solution)/shard_map/ppermute | solution.py:509
  67.4 4.8 %collective-permute-start.11 = (bf16[224,256]{1,0:T(8,128)(2,1)S(1)}, bf16[224,256]{1,0:T(8,128)(2,1)S(1)}, u32[]{:S(2)}, u32[]{:S(2)}) collective-permute-start(bf16[224,256]{1,0:T(8,128)(2,1)S(1)} %get-tuple-element.27), channel_id=1, source_target_pairs={{0,3},{1,0},{2,1},{3,2},{4,7},{5,4},{6,5},{7,6},{8,11},{9,8},{10,9... | collective-permute-start | bytes 344072 | tf_op jit(solution)/shard_map/ppermute | solution.py:509
